TPU v7x, 128 devices: a whole 4x4x4 slice. The times are simulated.
128 devices in a mesh: sp: 64 (over z, y, x), tp: 2 (over core).
Axes of the slice: x: 4, y: 4, z: 4, core: 2. Of those that a mesh axis runs over, the one named last changes fastest.
Arguments:
- residual: bfloat16 [16384, 2048], P(('sp', 'tp')), may hold values from -6 to 6
- queries: bfloat16 [16384, 1152], P('sp', 'tp'), may hold values from -800 to 800
- latent: bfloat16 [16384, 256], P('sp'), may hold values from -6 to 6
- rope_key: bfloat16 [16384, 32], P('sp'), may hold values from -6 to 6
- doc_ids: int32 [16384], P('sp'), may hold values from 0 to 5, never falling along the last dimension, each value on 1 to 8192 neighbouring positions
- latent_to_key: bfloat16 [256, 768], P(None, 'tp'), may hold values from -0.375 to 0.375
- latent_to_value: bfloat16 [256, 768], P(None, 'tp'), may hold values from -0.375 to 0.375
- out_proj: bfloat16 [768, 2048], replicated, may hold values from -0.21875 to 0.21875
- mix_gain: float32 [2048], replicated, may hold values from 0.1 to 1.9
- moe_gain: float32 [2048], replicated, may hold values from 0.1 to 1.9
- expert_ids: int32 [16384, 2], P(('sp', 'tp')), may hold values from 0 to 63, as said below
- route_weight: float32 [16384, 2], P(('sp', 'tp')), may hold values from 0.1 to 1
- gate_weight: bfloat16 [64, 2048, 1024], P('sp', None, 'tp'), may hold values from -0.125 to 0.125
- up_weight: bfloat16 [64, 2048, 1024], P('sp', None, 'tp'), may hold values from -0.125 to 0.125
- down_weight: bfloat16 [64, 1024, 2048], P('sp', 'tp'), may hold values from -0.1875 to 0.1875
Outputs:
- output: bfloat16 [16384, 2048], P(('sp', 'tp'))
Inputs may be any that keep to these rules, and one draw needn't show every extreme that they name: `expert_ids`: each row names 2 different experts of one group of 16 consecutive numbers; in each aligned block of 128 rows (the rows of one device) no expert is named more than 8 times, and some expert exactly 8 times.
All inputs are finite; a program needn't handle non-finite values.
Results may differ from a plain program's by a relative error of at most 0.013.
Values may be sent and summed in bfloat16 or wider, within the bound.
No kernel may reach another device: no remote copies, remote signals or barrier semaphores. Data moves between devices by JAX's collectives and lax.ppermute only.
A program may use at most 64 MiB of HBM per device.

v0:
```python
import math

import jax
import jax.numpy as jnp
from jax import lax
from jax.sharding import PartitionSpec as P

D = 2048
UNROTATED_DIM = 64
ROPE = 32
VALUE_ENTRIES = 64
GROUPS = 4


rope_base = 10000.0
epsilon = 1e-06


def in_order(pieces, dim):
    pieces = jnp.moveaxis(pieces, 0, dim)
    lengths = pieces.shape
    return pieces.reshape(*lengths[:dim], lengths[dim] * lengths[dim + 1], *lengths[dim + 2 :])


def sent_to_all(x, axis):
    size = lax.axis_size(axis)
    return lax.all_to_all(jnp.broadcast_to(x[None], (size, *x.shape)), axis, 0, 0, tiled=True)


def collect(x, axis, dim):
    return in_order(sent_to_all(x, axis), dim)


def cut_along(x, dim, size):
    before, after = (x.shape[:dim], x.shape[dim + 1 :])
    return jnp.moveaxis(x.reshape(*before, size, -1, *after), dim, 0)


def sum_at_owner(x, axis, dim):
    pieces = cut_along(x, dim, lax.axis_size(axis))
    arrived = lax.all_to_all(pieces, axis, split_axis=0, concat_axis=0, tiled=True)
    return arrived.astype(jnp.float32).sum(axis=0)


def rotate(source, positions):
    half_width = source.shape[-1] // 2
    frequency = rope_base ** (-jnp.arange(half_width, dtype=jnp.float32) / half_width)
    angles = positions.astype(jnp.float32)[:, None] * frequency[None, :]
    if source.ndim == 3:
        angles = angles[:, None, :]
    cosine = jnp.cos(angles)
    sine_part = jnp.sin(angles)
    upper_half = source[..., :half_width].astype(jnp.float32)
    lower_half = source[..., half_width:].astype(jnp.float32)
    turned = jnp.concatenate(
        [
            upper_half * cosine - lower_half * sine_part,
            lower_half * cosine + upper_half * sine_part,
        ],
        axis=-1,
    )
    return turned.astype(jnp.bfloat16)


def rms_scale(source, gain):
    return source * lax.rsqrt(jnp.mean(source * source, axis=-1, keepdims=True) + epsilon) * gain


def attend_keys(
    running,
    query_nope,
    query_rot,
    query_pos,
    query_docs,
    key_nope,
    key_rot,
    value_rows,
    key_pos,
    key_docs,
):
    row_max, row_total, weighted = running
    score_scale = (UNROTATED_DIM + ROPE) ** (-0.5)
    scores = (
        jnp.einsum("qhd,khd->qhk", query_nope, key_nope, preferred_element_type=jnp.float32)
        + jnp.einsum("qhr,kr->qhk", query_rot, key_rot, preferred_element_type=jnp.float32)
    ) * score_scale
    allowed = (
        (key_pos[None, :] <= query_pos[:, None]) & (key_docs[None, :] == query_docs[:, None])
    )[:, None, :]
    new_max = jnp.maximum(row_max, jnp.max(jnp.where(allowed, scores, -1e30), axis=-1))
    weights = jnp.where(allowed, jnp.exp(scores - new_max[..., None]), 0.0)
    factor = jnp.exp(row_max - new_max)
    row_total = row_total * factor + jnp.sum(weights, axis=-1)
    weighted = weighted * factor[..., None] + jnp.einsum(
        "qhk,khd->qhd", weights.astype(jnp.bfloat16), value_rows, preferred_element_type=jnp.float32
    )
    return (new_max, row_total, weighted)


def local(
    residual,
    queries,
    latent,
    rope_key,
    doc_ids,
    latent_to_key,
    latent_to_value,
    out_proj,
    mix_gain,
    moe_gain,
    expert_ids,
    route_weight,
    gate_weight,
    up_weight,
    down_weight,
):
    local_rows = queries.shape[0]
    local_heads = queries.shape[1] // (UNROTATED_DIM + ROPE)
    query_pos = lax.axis_index("sp") * local_rows + jnp.arange(local_rows, dtype=jnp.int32)
    shaped = queries.reshape(local_rows, local_heads, UNROTATED_DIM + ROPE)
    query_nope = shaped[..., :UNROTATED_DIM]
    query_rot = rotate(shaped[..., UNROTATED_DIM:], query_pos)
    key_rot = rotate(rope_key, query_pos)
    initial = (
        jnp.full((local_rows, local_heads), -1e30, jnp.float32),
        jnp.zeros((local_rows, local_heads), jnp.float32),
        jnp.zeros((local_rows, local_heads, VALUE_ENTRIES), jnp.float32),
    )
    pieces = (
        lax.all_gather(latent, "sp", axis=0, tiled=True),
        lax.all_gather(key_rot, "sp", axis=0, tiled=True),
        lax.all_gather(doc_ids, "sp", axis=0, tiled=True),
    )
    row_count = pieces[0].shape[0]
    block_rows = math.gcd(row_count, 512)

    def one_block(number, current):
        first_row = number * block_rows
        sliced = [lax.dynamic_slice_in_dim(member, first_row, block_rows, 0) for member in pieces]
        key_pos = first_row + jnp.arange(block_rows, dtype=jnp.int32)
        active = (first_row <= query_pos[-1]) & (sliced[-1][-1] >= doc_ids[0])

        def compute(carried):
            key_nope = jnp.dot(sliced[0], latent_to_key, preferred_element_type=jnp.float32).astype(
                jnp.bfloat16
            )
            value_rows = jnp.dot(
                sliced[0], latent_to_value, preferred_element_type=jnp.float32
            ).astype(jnp.bfloat16)
            key_part = sliced[1]
            return attend_keys(
                carried,
                query_nope,
                query_rot,
                query_pos,
                doc_ids,
                key_nope.reshape(block_rows, local_heads, UNROTATED_DIM),
                key_part,
                value_rows.reshape(block_rows, local_heads, VALUE_ENTRIES),
                key_pos,
                sliced[-1],
            )

        return lax.cond(active, compute, lambda carried: carried, current)

    running = lax.fori_loop(0, row_count // block_rows, one_block, initial)
    attended = (running[2] / running[1][..., None]).astype(jnp.bfloat16)
    attended = attended.reshape(local_rows, local_heads * VALUE_ENTRIES)
    gathered = lax.all_to_all(attended, "tp", split_axis=0, concat_axis=1, tiled=True)
    mix = jnp.dot(gathered, out_proj, preferred_element_type=jnp.float32)
    branch = rms_scale(mix, mix_gain)
    middle = lax.optimization_barrier((residual.astype(jnp.float32) + branch).astype(jnp.bfloat16))
    normed = rms_scale(middle.astype(jnp.float32), moe_gain).astype(jnp.bfloat16)
    row_count = normed.shape[0]
    top_count = expert_ids.shape[1]
    expert_count = lax.axis_size("sp")
    capacity = row_count // (expert_count // GROUPS)
    flat_ids = expert_ids.reshape(-1)
    onehot = (flat_ids[:, None] == jnp.arange(expert_count, dtype=jnp.int32)[None, :]).astype(
        jnp.int32
    )
    earlier = jnp.cumsum(onehot, axis=0) - onehot
    slot_rank = jnp.sum(earlier * onehot, axis=1)
    slot_ids = (flat_ids * capacity + slot_rank).reshape(row_count, top_count)
    chooser = jnp.any(
        jnp.arange(expert_count * capacity, dtype=jnp.int32)[:, None, None] == slot_ids[None],
        axis=2,
    ).astype(jnp.bfloat16)
    buffer = jnp.dot(chooser, normed, preferred_element_type=jnp.float32).astype(jnp.bfloat16)
    buffer = buffer.reshape(expert_count, capacity, D)
    arrived = lax.all_to_all(buffer, "sp", split_axis=0, concat_axis=0, tiled=True)
    model_width = arrived.shape[2]
    both_halves = collect(arrived, "tp", 0)
    flat_rows = both_halves.reshape(-1, model_width)
    gate_out = jnp.dot(flat_rows, gate_weight[0], preferred_element_type=jnp.float32)
    upward = jnp.dot(flat_rows, up_weight[0], preferred_element_type=jnp.float32)
    hidden = (jax.nn.silu(gate_out) * upward).astype(jnp.bfloat16)
    partial_value = jnp.dot(hidden, down_weight[0], preferred_element_type=jnp.float32).reshape(
        both_halves.shape
    )
    summed = sum_at_owner(partial_value.astype(jnp.bfloat16), "tp", 0).astype(jnp.bfloat16)
    returned = lax.all_to_all(summed, "sp", split_axis=0, concat_axis=0, tiled=True)
    picked = returned.reshape(-1, D)[slot_ids.reshape(-1)].astype(jnp.float32)
    expert_mix = jnp.sum(
        (picked * route_weight.reshape(-1)[:, None]).reshape(row_count, top_count, D), axis=1
    )
    return (middle.astype(jnp.float32) + expert_mix).astype(jnp.bfloat16)


def solution(mesh):
    in_specs = (
        P(("sp", "tp"), None),
        P("sp", "tp"),
        P("sp", None),
        P("sp", None),
        P("sp"),
        P(None, "tp"),
        P(None, "tp"),
        P(),
        P(),
        P(),
        P(("sp", "tp"), None),
        P(("sp", "tp"), None),
        P("sp", None, "tp"),
        P("sp", None, "tp"),
        P("sp", "tp", None),
    )
    out_specs = P(("sp", "tp"), None)
    return jax.shard_map(local, mesh=mesh, in_specs=in_specs, out_specs=out_specs, check_vma=False)
```

profile of v0, /device:TPU:0, one launch (start us, length us, event | category | flops | bytes accessed | tf_op | source)
XLA Modules:
  0.0 631.5 jit_solution(9027320513454528965)
XLA Ops:
  10.0 1.6 slice.54
  13.5 186.6 %all-gather = s32[64,1,256]{2,1,0:T(1,128)} all-gather(s32[1,1,256]{2,1,0:T(1,128)} %bitcast.92), channel_id=1, replica_groups=mesh['sp'=64,'tp'=2] {'sp'}, dimensions={0}, use_global_device_ids=true | all-gather | bytes 66560 | tf_op jit(solution)/shard_map/all_gather | solution.py:132
  202.9 216.7 %while.17 = (s32[]{:T(128)}, f32[256,6]{0,1:T(8,128)S(1)}, f32[256,6]{0,1:T(8,128)S(1)}, f32[256,6,64]{0,2,1:T(8,128)S(1)}, s32[256]{0:T(256)}, /*index=5*/s32[1...) while((s32[]{:T(128)}, f32[256,6]{0,1:T(8,128)S(1)}, ...), condition=%wide.region_5.6_spmd, body=%wide.region_0.5_spmd.sunk | while | flops 461835776 | bytes 21579896 | solution.py:166
  205.0 1.2 slice.72
  207.4 1.3 slice.70
  209.5 7.0 %conditional.2 = ((f32[256,6]{0,1:T(8,128)S(1)}, f32[256,6]{0,1:T(8,128)S(1)}, f32[256,6,64]{0,2,1:T(8,128)S(1)})) conditional(s32[]{:T(128)} %convert_element_type.177, (f32[256,6]{0,1:T(8,128)S(1)}, f32[256,6]{0,1:T(8,128)S(1)}, f32[256,6,64]{0,2,1:T(8,128)S(1)}) %tuple.50, (s32[]{:T(128)}, s32[512]{0:T(512)}, s32[256]{0:T(256)}, s32[512]{0:T(512)}, ...), branch_computations={%region_1.0_spmd, %region_2.4_spmd} | conditional | flops 461835776 | bytes 21565132 | solution.py:164
  209.5 1.3 convolution_convert_fusion.1
  210.9 1.5 fusion.16
  214.5 1.2 convolution_convert_fusion
  218.5 1.2 slice.72
  221.0 1.3 slice.70
  225.1 1.2 slice.72
  227.5 1.3 slice.70
  231.6 1.2 slice.72
  234.1 1.3 slice.70
  238.2 1.2 slice.72
  240.6 1.3 slice.70
  244.7 1.2 slice.72
  247.2 1.3 slice.70
  251.3 1.2 slice.72
  253.7 1.3 slice.70
  257.8 1.2 slice.72
  260.3 1.3 slice.70
  264.4 1.2 slice.72
  266.8 1.3 slice.70
  270.9 1.2 slice.72
  273.4 1.3 slice.70
  277.5 1.2 slice.72
  279.9 1.3 slice.70
  286.5 1.3 slice.70
  293.1 1.3 slice.70
  299.6 1.3 slice.70
  306.2 1.3 slice.70
  312.7 1.3 slice.70
  319.3 1.3 slice.70
  325.9 1.3 slice.70
  332.4 1.3 slice.70
  339.0 1.3 slice.70
  345.5 1.3 slice.70
  352.1 1.3 slice.70
  358.6 1.3 slice.70
  365.2 1.3 slice.70
  371.7 1.3 slice.70
  378.3 1.3 slice.70
  384.8 1.3 slice.70
  391.4 1.3 slice.70
  398.0 1.3 slice.70
  404.5 1.3 slice.70
  411.1 1.3 slice.70
  417.6 1.3 slice.70
  421.4 4.0 all_to_all.39
  428.0 118.8 %all_to_all.40 = bf16[64,8,2048]{2,1,0:T(8,128)(2,1)S(1)} all-to-all(bf16[64,8,2048]{2,1,0:T(8,128)(2,1)S(1)} %fusion.23), channel_id=1, replica_groups=mesh['sp'=64,'tp'=2] {'sp'}, dimensions={0} | all-to-all | bytes 4194304 | tf_op jit(solution)/shard_map/all_to_all | solution.py:191
  547.3 7.2 %all_to_all.41 = bf16[2,64,8,2048]{3,2,1,0:T(8,128)(2,1)S(1)} all-to-all(bf16[2,64,8,2048]{3,2,1,0:T(8,128)(2,1)S(1)} %broadcast_in_dim.63), channel_id=1, replica_groups=mesh['sp'=64,'tp'=2] {'tp'}, dimensions={0} | all-to-all | bytes 8388608 | tf_op jit(solution)/shard_map/all_to_all | solution.py:27
  554.6 2.3 fusion.25
  556.9 2.6 fusion.31
  559.6 2.4 convolution_convert_fusion.2
  562.5 8.2 %all_to_all.42 = bf16[2,64,8,2048]{3,1,2,0:T(8,128)(2,1)} all-to-all(bf16[2,64,8,2048]{3,1,2,0:T(8,128)(2,1)S(1)} %copy.65), channel_id=1, replica_groups=mesh['sp'=64,'tp'=2] {'tp'}, dimensions={0} | all-to-all | bytes 8388608 | tf_op jit(solution)/shard_map/all_to_all | solution.py:41
  570.7 3.5 reduce_sum.67
  574.2 2.5 copy.67
  576.7 6.1 all-to-all-start.4
  583.1 29.9 %all-to-all-done.4 = bf16[64,8,2048]{2,1,0:T(8,128)(2,1)S(1)} async-done(((bf16[64,8,2048]{2,1,0:T(8,128)(2,1)}), bf16[64,8,2048]{2,1,0:T(8,128)(2,1)S(1)}, u32[]{:S(2)}, u32[]{:S(2)}) %all-to-all-start.4) | async-done | bytes 2097184 | tf_op jit(solution)/shard_map/all_to_all | solution.py:202
  612.9 2.3 gather_fusion
  615.3 3.5 reshape.226
  618.8 4.9 multiply_reduce_fusion
  (307 shorter events, 107.1 us)
Async XLA Ops:
  6.5 418.9 %copy-start = (bf16[768,2048]{1,0:T(8,128)(2,1)S(1)}, bf16[768,2048]{1,0:T(8,128)(2,1)}, u32[]{:S(2)}) copy-start(bf16[768,2048]{1,0:T(8,128)(2,1)} %param.26) | copy-start | bytes 9437188
  6.5 196.3 %all-gather.6.cloned.1.call-start = ((), (), s32[]{:S(2)}) async-start(), calls=%async_computation.6 | async-start | bytes 1064960 | tf_op jit(solution)/shard_map/all_gather | solution.py:131
  8.2 194.6 %all-gather.4.cloned.1.call-start = ((), (), s32[]{:S(2)}) async-start(), calls=%async_computation.5 | async-start | bytes 8519680 | tf_op jit(solution)/shard_map/all_gather | solution.py:130
  12.6 190.2 %copy-start.14 = (s32[256]{0:T(256)}, s32[256]{0:T(256)S(1)}, u32[]{:S(2)}) copy-start(s32[256]{0:T(256)S(1)} %fusion.49) | copy-start | bytes 3076
  203.7 0.6 copy-start.9
  209.5 2.9 copy-start.11
  209.5 2.9 copy-start.10
  209.5 2.9 copy-start.12
  209.5 2.9 copy-start.13
  209.5 3.1 copy-start.4
  213.5 0.9 copy-start.5
  217.2 0.6 copy-start.9
  223.8 0.6 copy-start.9
  230.4 0.6 copy-start.9
  236.9 0.6 copy-start.9
  243.5 0.6 copy-start.9
  250.0 0.6 copy-start.9
  256.6 0.6 copy-start.9
  263.1 0.6 copy-start.9
  269.7 0.6 copy-start.9
  276.2 0.6 copy-start.9
  282.8 0.6 copy-start.9
  289.3 0.6 copy-start.9
  295.9 0.6 copy-start.9
  302.5 0.6 copy-start.9
  309.0 0.6 copy-start.9
  315.6 0.6 copy-start.9
  322.1 0.6 copy-start.9
  328.7 0.6 copy-start.9
  335.3 0.6 copy-start.9
  341.8 0.6 copy-start.9
  348.4 0.6 copy-start.9
  354.9 0.6 copy-start.9
  361.5 0.6 copy-start.9
  368.0 0.6 copy-start.9
  374.6 0.6 copy-start.9
  381.1 0.6 copy-start.9
  387.7 0.6 copy-start.9
  394.2 0.6 copy-start.9
  400.8 0.6 copy-start.9
  407.3 0.6 copy-start.9
  413.9 0.6 copy-start.9
  419.7 6.5 %copy-start.16 = (f32[2048]{0:T(1024)S(1)}, f32[2048]{0:T(1024)}, u32[]{:S(2)}) copy-start(f32[2048]{0:T(1024)} %param.27) | copy-start | bytes 24580
  421.4 4.8 copy-start.6
  425.5 1.7 copy-start.7
  425.5 1.7 copy-start.17
  426.4 0.8 copy-start.2
  547.3 7.2 %copy-start.19 = (bf16[1,2048,512]{2,1,0:T(8,128)(2,1)S(1)}, bf16[1,2048,512]{2,1,0:T(8,128)(2,1)}, u32[]{:S(2)}) copy-start(bf16[1,2048,512]{2,1,0:T(8,128)(2,1)} %param.32) | copy-start | bytes 6291460
  554.6 2.3 copy-start.20
  556.9 2.7 copy-start.21
  576.7 6.1 copy-start.8
  576.7 6.2 copy-start.18
  576.7 6.4 %copy-start.15 = (s32[256]{0:T(256)S(1)}, s32[256]{0:T(256)}, u32[]{:S(2)}) copy-start(s32[256]{0:T(256)} %copy-done.14) | copy-start | bytes 3076
  576.7 36.2 %all-to-all-start.4 = ((bf16[64,8,2048]{2,1,0:T(8,128)(2,1)}), bf16[64,8,2048]{2,1,0:T(8,128)(2,1)S(1)}, u32[]{:S(2)}, u32[]{:S(2)}) async-start(bf16[64,8,2048]{2,1,0:T(8,128)(2,1)} %copy.67), calls=%async_computation.4 | async-start | bytes 4194304 | tf_op jit(solution)/shard_map/all_to_all | solution.py:202
  615.3 9.3 %copy-start.1 = (bf16[768,2048]{1,0:T(8,128)(2,1)S(1)}, bf16[768,2048]{1,0:T(8,128)(2,1)}, u32[]{:S(2)}) copy-start(bf16[768,2048]{1,0:T(8,128)(2,1)} %param.26) | copy-start | bytes 9437188
  618.8 4.9 copy-start.3
Sparse Core Ops, SparseCore 0:
  10.0 66.1 all-gather.5
  79.0 76.5 all-gather.3
where the time goes:
time: 639 us; the launch traced here: 631 us
  blocking collectives  325 us (51%)
  local copies, waits for them, and re-layouts  160 us (25%)
  loops' own time  64.4 us (10%)
  waiting for transfers between devices  30.6 us (5%)
  other arithmetic  17 us (3%)
  matrix products  14.5 us (2%)
  between operations  13.7 us (2%)
    all_gather x1, blocking collectives, local(): lax.all_gather(doc_ids, 'sp', axis=0, tiled=True)  187 us
    all_to_all x1, blocking collectives, local(): lax.all_to_all(buffer, 'sp', split_axis=0, concat_axis=0, tiled=True)  119 us
    slice x96, local copies, waits for them, and re-layouts, one_block(): active = (first_row <= query_pos[-1]) & (sliced[-1][-1] >= doc_ids[0])  102 us
    another operation x1, loops' own time, local(): running = lax.fori_loop(0, row_count // block_rows, one_block, initial)  63.9 us
    all_to_all x1, waiting for transfers between devices, local(): lax.all_to_all(summed, 'sp', split_axis=0, concat_axis=0, tiled=True)  29.9 us
    dynamic_slice x32, local copies, waits for them, and re-layouts, one_block(): lax.dynamic_slice_in_dim(member, first_row, block_rows, 0)  24.2 us
    iota x32, local copies, waits for them, and re-layouts, one_block(): key_pos = first_row + jnp.arange(block_rows, dtype=jnp.int32)  19.1 us
  transfers between devices with their start and end apart: 3, of which 1 were waited for; matrix products, arithmetic and copies ran while one was open for 1% of the time, Pallas kernels for 0%

commit v1 on v0

v1 whole, which is shorter than its diff:
```python
import math

import jax
import jax.numpy as jnp
from jax import lax
from jax.experimental import pallas as pl
from jax.experimental.pallas import tpu as pltpu
from jax.sharding import PartitionSpec as P

D = 2048
NOPE = 64
ROPE = 32
HALF = 128
BLOCK = 256
HEADS = 12
LOCAL_HEADS = 6
PLANE = 16
ROWS = 304
CAPACITY = 8
EXPERTS = 64
SLOTS = EXPERTS * CAPACITY
QW = LOCAL_HEADS * 128
KW = 512
VW = 384
PACK = QW + KW + VW
epsilon = 1e-06
LOW = -1e30
SCALE = (NOPE + ROPE) ** -0.5 * math.log2(math.e)
f32 = jnp.float32
bf16 = jnp.bfloat16


def vmem():
    return pl.BlockSpec(memory_space=pltpu.VMEM)


def smem():
    return pl.BlockSpec(memory_space=pltpu.SMEM)


def params(mib=48):
    return pltpu.CompilerParams(vmem_limit_bytes=mib * 1024 * 1024)


def lanes(rows):
    return lax.broadcasted_iota(jnp.int32, (rows, 128), 1)


def turn(x, cosine, sine, lane):
    other = jnp.where(lane < 80, -pltpu.roll(x, 112, 1), pltpu.roll(x, 16, 1))
    return x * cosine + other * sine


def prep_kernel(q_ref, lat_ref, rope_ref, doc_ref, wk_ref, wv_ref, cos_ref, sin_ref, pay_ref, pack_ref):
    half = lax.axis_index("tp")
    lane = lanes(BLOCK)
    cosine, sine = cos_ref[...], sin_ref[...]
    for head in range(LOCAL_HEADS):
        start = head * (NOPE + ROPE)
        panel, off = start // 128, start % 128
        x = q_ref[:, panel * 128 : panel * 128 + 128].astype(f32)
        if off:
            x = pltpu.roll(x, 128 - off, 1)
        if off + NOPE + ROPE > 128:
            width = min(128, q_ref.shape[1] - (panel + 1) * 128)
            y = q_ref[:, (panel + 1) * 128 : (panel + 1) * 128 + width].astype(f32)
            if width < 128:
                y = jnp.concatenate([y, jnp.zeros((BLOCK, 128 - width), f32)], axis=1)
            x = jnp.where(lane < 128 - off, x, pltpu.roll(y, 128 - off, 1))
        x = jnp.where(lane < NOPE + ROPE, x, 0.0)
        pack_ref[:, head * 128 : head * 128 + 128] = turn(x, cosine, sine, lane).astype(bf16)
    w0 = wk_ref[:, 0:128]
    w1 = wk_ref[:, 128:256].astype(f32)
    w2 = wk_ref[:, 256:384].astype(f32)
    r1, r2 = pltpu.roll(w1, 64, 1), pltpu.roll(w2, 64, 1)
    pack_ref[:, QW : QW + 128] = w0
    pack_ref[:, QW + 128 : QW + 256] = jnp.where(lane < 64, w1, 0.0).astype(bf16)
    pack_ref[:, QW + 256 : QW + 384] = jnp.where(lane < 64, r1, r2).astype(bf16)
    pack_ref[:, QW + 384 : QW + 512] = jnp.where(lane < 64, r2, 0.0).astype(bf16)
    pack_ref[:, QW + KW : PACK] = wv_ref[...]
    first = pl.multiple_of(half * HALF, HALF)
    mine = pl.ds(first, HALF)
    pay_ref[0:128, :] = lat_ref[mine, 0:128]
    pay_ref[128:256, :] = lat_ref[mine, 128:256]
    rope = jnp.concatenate([rope_ref[mine, :].astype(f32), jnp.zeros((HALF, 96), f32)], axis=1)
    small = lanes(HALF)
    turned = turn(pltpu.roll(rope, 64, 1), cos_ref[mine, :], sin_ref[mine, :], small)
    turned = jnp.where((small >= 64) & (small < 96), turned, 0.0)
    packed = jnp.zeros((32, 128), f32)
    for c in range(4):
        piece = turned[32 * c : 32 * c + 32, :]
        shift = (32 * c + 64) % 128
        packed = packed + (pltpu.roll(piece, shift, 1) if shift else piece)
    pay_ref[256:288, :] = packed.astype(bf16)
    docs = doc_ref[pl.ds(half, 1), :].astype(f32)
    pay_ref[288:304, :] = jnp.broadcast_to(docs, (16, 128)).astype(bf16)


def attend_kernel(
    arr_ref, ext_ref, own_ref, oth_ref, qdoc_ref, doc_ref, mine_ref, theirs_ref, q_s, k_s, v_s, m_s, l_s, a_s, bias_s, full_s
):
    half = lax.axis_index("tp")
    seat = lax.axis_index("sp")
    plane, spot = seat // PLANE, seat % PLANE
    doc_first = doc_ref[0].astype(f32)
    doc_last = doc_ref[BLOCK - 1].astype(f32)
    lane = lanes(BLOCK)
    for head in range(HEADS):
        src = own_ref if head < LOCAL_HEADS else oth_ref
        local = head % LOCAL_HEADS
        x = src[:, local * 128 : local * 128 + 128].astype(f32)
        if head % 3 == 2:
            lo, hi = jnp.zeros_like(x), x
        else:
            lo, hi = jnp.where(lane < 64, x, 0.0), jnp.where(lane < 64, 0.0, x)
            if head % 3 == 1:
                lo = pltpu.roll(lo, 64, 1)
        q_s[head, :, 0:128] = lo.astype(bf16)
        q_s[head, :, 128:256] = hi.astype(bf16)
    m_s[...] = jnp.full(m_s.shape, LOW, f32)
    l_s[...] = jnp.zeros(l_s.shape, f32)
    a_s[...] = jnp.zeros(a_s.shape, f32)

    def heads(count, masked):
        panels = count // 128
        for head in range(HEADS):
            group = head // 3
            s = lax.dot_general(
                q_s[head],
                k_s[:count, group * 256 : group * 256 + 256],
                (((1,), (1,)), ((), ())),
                preferred_element_type=f32,
            )
            parts = [s[:, 128 * b : 128 * b + 128] for b in range(panels)]
            if masked:
                parts = [part + bias_s[:, 128 * b : 128 * b + 128] for b, part in enumerate(parts)]
            top = parts[0]
            for part in parts[1:]:
                top = jnp.maximum(top, part)
            old = m_s[head]
            new = jnp.maximum(old, jnp.max(top, axis=1, keepdims=True))
            keep = jnp.exp2((old - new) * SCALE)
            weights = [jnp.exp2((part - new) * SCALE) for part in parts]
            total = weights[0]
            for w in weights[1:]:
                total = total + w
            l_s[head] = l_s[head] * keep + total
            m_s[head] = new
            rounded = jnp.concatenate([w.astype(bf16) for w in weights], axis=1) if panels > 1 else weights[0].astype(bf16)
            pair = head // 2
            a_s[head] = a_s[head] * keep + jnp.dot(
                rounded, v_s[:count, pair * 128 : pair * 128 + 128], preferred_element_type=f32
            )

    def tile(load, bases, own_flags):
        panels = len(bases)
        count = panels * 128
        rows = [load(b, 288, 304).astype(f32) for b in range(panels)]
        seen = [jnp.where(base >= 0, row, -1.0) for base, row in zip(bases, rows)]
        high, low = seen[0], seen[0]
        for row in seen[1:]:
            high, low = jnp.maximum(high, row), jnp.minimum(low, row)
        high, low = jnp.max(high), jnp.min(low)
        has_own = own_flags[0]
        for flag in own_flags[1:]:
            has_own = has_own | flag
        active = high >= doc_first
        plain = (low == doc_last) & jnp.logical_not(has_own)

        @pl.when(active)
        def _():
            lat = jnp.concatenate(
                [
                    jnp.concatenate([load(b, 0, 128) for b in range(panels)], axis=0),
                    jnp.concatenate([load(b, 128, 256) for b in range(panels)], axis=0),
                ],
                axis=1,
            )
            turned = []
            for b in range(panels):
                r = load(b, 256, 288).astype(f32)
                turned += [pltpu.roll(r, 64, 1), pltpu.roll(r, 32, 1), r, pltpu.roll(r, 96, 1)]
            turned = jnp.concatenate(turned, axis=0)
            wide = lanes(count)
            turned = jnp.where((wide >= 64) & (wide < 96), turned, 0.0)
            for side, src in enumerate((own_ref, oth_ref)):
                keys = jnp.dot(lat, src[:, QW : QW + KW], preferred_element_type=f32)
                for g in range(2):
                    at = side * 512 + g * 256
                    k_s[:count, at : at + 128] = keys[:, g * 256 : g * 256 + 128].astype(bf16)
                    k_s[:count, at + 128 : at + 256] = (keys[:, g * 256 + 128 : g * 256 + 256] + turned).astype(bf16)
                v_s[:count, side * 384 : side * 384 + 384] = jnp.dot(
                    lat, src[:, QW + KW : PACK], preferred_element_type=f32
                ).astype(bf16)

        @pl.when(active & plain)
        def _():
            heads(count, False)

        @pl.when(active & jnp.logical_not(plain))
        def _():
            at_query = seat * BLOCK + lax.broadcasted_iota(jnp.int32, (BLOCK, 128), 0)
            for b in range(panels):
                at_key = jnp.where(bases[b] >= 0, bases[b], 1 << 20) + lane
                allowed = (at_key <= at_query) & (rows[b][0:1, :] == qdoc_ref[...])
                bias_s[:, 128 * b : 128 * b + 128] = jnp.where(allowed, 0.0, LOW)
            heads(count, True)

    def place(block):
        return jnp.where(block >= 0, block * BLOCK + half * HALF, -1)

    tile(lambda b, lo, hi: ext_ref[lo:hi, :], [place((plane - 2) * PLANE + spot)], [jnp.bool_(False)])

    def step(number, carried):
        kind, quad = number // 4, number % 4
        bases, flags = [], []
        for b in range(4):
            i = quad * 4 + b
            late = (plane - jnp.where(i <= spot, 0, 2)) * PLANE + i
            block = jnp.where(kind == 0, (plane - 1) * PLANE + i, late)
            bases.append(place(block))
            flags.append(block == seat)
        tile(lambda b, lo, hi: arr_ref[quad * 4 + b, kind, lo:hi, :], bases, flags)
        return carried

    lax.fori_loop(0, 8, step, 0)

    stats = jnp.zeros((BLOCK, 128), f32)
    for head in range(HEADS):
        at = head + jnp.where(half == 0, 0, LOCAL_HEADS if head < LOCAL_HEADS else -LOCAL_HEADS)
        stats = jnp.where(lane == at, m_s[head], stats)
        stats = jnp.where(lane == at + 16, jnp.sum(l_s[head], axis=1, keepdims=True), stats)
    full_s[:, 768:896] = stats
    for pair in range(6):
        both = jnp.where(lane < 64, a_s[2 * pair], a_s[2 * pair + 1])

        @pl.when(half == 0)
        def _():
            full_s[:, pair * 128 : pair * 128 + 128] = both

        @pl.when(half == 1)
        def _():
            at = (pair + 3) % 6
            full_s[:, at * 128 : at * 128 + 128] = both

    mine_ref[...] = full_s[pl.ds(pl.multiple_of(half * HALF, HALF), HALF), :]
    theirs_ref[...] = full_s[pl.ds(pl.multiple_of((1 - half) * HALF, HALF), HALF), :]


def slots_of(ids):
    expert = lax.broadcasted_iota(jnp.int32, (HALF, EXPERTS), 1)
    named = [(ids[:, k : k + 1] == expert) for k in range(2)]
    counts = named[0].astype(f32) + named[1].astype(f32)
    row = lax.broadcasted_iota(jnp.int32, (HALF, HALF), 0)
    col = lax.broadcasted_iota(jnp.int32, (HALF, HALF), 1)
    earlier = jnp.dot((col < row).astype(f32).astype(bf16), counts.astype(bf16), preferred_element_type=f32)
    slot = lax.broadcasted_iota(jnp.int32, (HALF, SLOTS), 1)
    picks = []
    for k in range(2):
        rank = jnp.sum(jnp.where(named[k], earlier, 0.0), axis=1, keepdims=True)
        at = ids[:, k : k + 1] * CAPACITY + rank.astype(jnp.int32)
        picks.append((slot == at).astype(f32).astype(bf16))
    return picks


def norm_of(x):
    return lax.rsqrt(jnp.mean(x * x, axis=-1, keepdims=True) + epsilon)


def mix_kernel(mine_ref, theirs_ref, proj_ref, res_ref, mixg_ref, moeg_ref, ids_ref, mid_ref, buf_ref):
    lane = lanes(HALF)
    sm, st = mine_ref[:, 768:896], theirs_ref[:, 768:896]
    top = jnp.maximum(sm, st)
    wm = jnp.exp2((sm - top) * SCALE)
    wt = jnp.exp2((st - top) * SCALE)
    panels = []
    for pair in range(6):
        fm, ft, total = [], [], []
        for head in (2 * pair, 2 * pair + 1):
            a, b = wm[:, head : head + 1], wt[:, head : head + 1]
            fm.append(a)
            ft.append(b)
            total.append(a * sm[:, 16 + head : 17 + head] + b * st[:, 16 + head : 17 + head])
        cols = slice(pair * 128, pair * 128 + 128)
        value = mine_ref[:, cols] * jnp.where(lane < 64, fm[0], fm[1]) + theirs_ref[:, cols] * jnp.where(lane < 64, ft[0], ft[1])
        panels.append((value / jnp.where(lane < 64, total[0], total[1])).astype(bf16))
    attended = jnp.concatenate(panels, axis=1)
    mix = jnp.dot(attended, proj_ref[...], preferred_element_type=f32)
    branch = mix * norm_of(mix) * mixg_ref[...]
    middle = (res_ref[...].astype(f32) + branch).astype(bf16)
    mid_ref[...] = middle
    wide = middle.astype(f32)
    normed = (wide * norm_of(wide) * moeg_ref[...]).astype(bf16)
    picks = slots_of(ids_ref[...])
    buf_ref[...] = lax.dot_general(
        picks[0] + picks[1], normed, (((0,), (0,)), ((), ())), preferred_element_type=f32
    ).astype(bf16)


def pick_kernel(back_ref, mid_ref, ids_ref, weight_ref, out_ref):
    picks = slots_of(ids_ref[...])
    total = mid_ref[...].astype(f32)
    for k in range(2):
        rows = jnp.dot(picks[k], back_ref[...], preferred_element_type=f32)
        total = total + rows * weight_ref[:, k : k + 1]
    out_ref[...] = total.astype(bf16)


def local(
    residual,
    queries,
    latent,
    rope_key,
    doc_ids,
    latent_to_key,
    latent_to_value,
    out_proj,
    mix_gain,
    moe_gain,
    expert_ids,
    route_weight,
    gate_weight,
    up_weight,
    down_weight,
):
    sp = lax.axis_size("sp")
    seat = lax.axis_index("sp")
    spot = seat % PLANE
    swap = [(0, 1), (1, 0)]
    lane = jnp.arange(128, dtype=jnp.int32)
    frequency = jnp.where(
        (lane >= 64) & (lane < 96), 10000.0 ** (-(lane % 16).astype(f32) / 16), 0.0
    )
    positions = seat * BLOCK + jnp.arange(BLOCK, dtype=jnp.int32)
    angles = positions.astype(f32)[:, None] * frequency[None, :]
    payload, pack = pl.pallas_call(
        prep_kernel,
        out_shape=(jax.ShapeDtypeStruct((ROWS, 128), bf16), jax.ShapeDtypeStruct((BLOCK, PACK), bf16)),
        in_specs=[vmem()] * 8,
        out_specs=(vmem(), vmem()),
        compiler_params=params(),
        name="prep",
    )(queries, latent, rope_key, doc_ids.reshape(2, 128), latent_to_key, latent_to_value, jnp.cos(angles), jnp.sin(angles))
    before = [lax.ppermute(payload, "sp", [(i, i + PLANE * k) for i in range(sp - PLANE * k)]) for k in (1, 2)]
    other = lax.ppermute(pack, "tp", swap)
    target = jnp.arange(PLANE, dtype=jnp.int32)[:, None, None]
    sent = jnp.stack(
        [jnp.broadcast_to(before[0][None], (PLANE, ROWS, 128)), jnp.where(spot <= target, payload[None], before[1][None])],
        axis=1,
    )
    groups = [[z * PLANE + i for i in range(PLANE)] for z in range(sp // PLANE)]
    arrived = lax.all_to_all(sent, "sp", 0, 0, axis_index_groups=groups, tiled=True)
    query_docs = jnp.broadcast_to(doc_ids.astype(f32)[:, None], (BLOCK, 128))
    stat = jax.ShapeDtypeStruct((HALF, 896), f32)
    mine, theirs = pl.pallas_call(
        attend_kernel,
        out_shape=(stat, stat),
        in_specs=[vmem()] * 5 + [smem()],
        out_specs=(vmem(), vmem()),
        scratch_shapes=[
            pltpu.VMEM((HEADS, BLOCK, 256), bf16),
            pltpu.VMEM((512, 1024), bf16),
            pltpu.VMEM((512, 768), bf16),
            pltpu.VMEM((HEADS, BLOCK, 128), f32),
            pltpu.VMEM((HEADS, BLOCK, 128), f32),
            pltpu.VMEM((HEADS, BLOCK, 128), f32),
            pltpu.VMEM((BLOCK, 512), f32),
            pltpu.VMEM((BLOCK, 896), f32),
        ],
        compiler_params=params(),
        name="attend",
    )(arrived, before[1], pack, other, query_docs, doc_ids)
    theirs = lax.ppermute(theirs, "tp", swap)
    middle, buffer = pl.pallas_call(
        mix_kernel,
        out_shape=(jax.ShapeDtypeStruct((HALF, D), bf16), jax.ShapeDtypeStruct((SLOTS, D), bf16)),
        in_specs=[vmem()] * 7,
        out_specs=(vmem(), vmem()),
        compiler_params=params(),
        name="mix",
    )(mine, theirs, out_proj, residual, mix_gain[None], moe_gain[None], expert_ids)
    rows = lax.all_to_all(buffer.reshape(EXPERTS, CAPACITY, D), "sp", 0, 0, tiled=True).reshape(SLOTS, D)
    own = (gate_weight[0], up_weight[0], down_weight[0])
    swapped = tuple(lax.ppermute(w, "tp", swap) for w in own)
    result = 0.0
    for gate, up, down in (own, swapped):
        gated = jnp.dot(rows, gate, preferred_element_type=f32)
        upward = jnp.dot(rows, up, preferred_element_type=f32)
        hidden = (jax.nn.silu(gated) * upward).astype(bf16)
        part = lax.optimization_barrier(jnp.dot(hidden, down, preferred_element_type=f32).astype(bf16))
        result = result + part.astype(f32)
    result = result.astype(bf16).reshape(EXPERTS, CAPACITY, D)
    back = lax.all_to_all(result, "sp", 0, 0, tiled=True).reshape(SLOTS, D)
    return pl.pallas_call(
        pick_kernel,
        out_shape=jax.ShapeDtypeStruct((HALF, D), bf16),
        in_specs=[vmem()] * 4,
        out_specs=vmem(),
        compiler_params=params(),
        name="pick",
    )(back, middle, expert_ids, route_weight)


def solution(mesh):
    in_specs = (
        P(("sp", "tp"), None),
        P("sp", "tp"),
        P("sp", None),
        P("sp", None),
        P("sp"),
        P(None, "tp"),
        P(None, "tp"),
        P(),
        P(),
        P(),
        P(("sp", "tp"), None),
        P(("sp", "tp"), None),
        P("sp", None, "tp"),
        P("sp", None, "tp"),
        P("sp", "tp", None),
    )
    out_specs = P(("sp", "tp"), None)
    return jax.shard_map(local, mesh=mesh, in_specs=in_specs, out_specs=out_specs, check_vma=False)
```

time: 639 us -> 216 us (0.34)
  blocking collectives: 325 us -> 0 us
  local copies, waits for them, and re-layouts: 160 us -> 10.8 us
  waiting for transfers between devices: 30.6 us -> 96.5 us
  loops' own time: 64.4 us -> 0 us
  starting transfers between devices: 6.12 us -> 61.3 us
  Pallas kernels: 0 us -> 17.4 us
  between operations: 13.7 us -> 0.19 us
  other arithmetic: 17 us -> 6.07 us
  matrix products: 14.5 us -> 21.7 us
    all_gather x1 -> x0, blocking collectives: 187 us -> none  [local(): lax.all_gather(doc_ids, 'sp', axis=0, tiled=True)]
    all_to_all x4 -> x0, blocking collectives: 138 us -> none  [the longest x1 119 us: local(): lax.all_to_all(buffer, 'sp', split_axis=0, concat_axis=0, tiled=True)]
    slice x97 -> x0, local copies, waits for them, and re-layouts: 104 us -> none  [the longest x96 102 us: one_block(): active = (first_row <= query_pos[-1]) & (sliced[-1][-1] >= doc_ids[0])]
    another operation x33 -> x0, loops' own time: 64.4 us -> none  [the longest x1 63.9 us: local(): running = lax.fori_loop(0, row_count // block_rows, one_block, initial)]
    all_to_all x1 -> x3, waiting for transfers between devices: 29.9 us -> 90.9 us  [the longest x1 31.1 us: local(): lax.all_to_all(sent, 'sp', 0, 0, axis_index_groups=groups, tiled=True)]
    all_to_all x1 -> x3, starting transfers between devices: 6.07 us -> 51.3 us  [the longest x1 38.4 us: local(): lax.all_to_all(buffer.reshape(EXPERTS, CAPACITY, D), 'sp', 0, 0, tiled=True)]
    dynamic_slice x32 -> x0, local copies, waits for them, and re-layouts: 24.2 us -> none  [one_block(): lax.dynamic_slice_in_dim(member, first_row, block_rows, 0)]
    iota x32 -> x0, local copies, waits for them, and re-layouts: 19.1 us -> none  [one_block(): key_pos = first_row + jnp.arange(block_rows, dtype=jnp.int32)]
  transfers between devices with their start and end apart: 3 -> 10, of which waited for: 1 -> 6; matrix products, arithmetic and copies ran while one was open for 1% -> 2% of each run, Pallas kernels for 0% -> 3%
where the time goes in v1:
time: 216 us; the launch traced here: 214 us
  waiting for transfers between devices  96.5 us (45%)
  starting transfers between devices  61.3 us (28%)
  matrix products  21.7 us (10%)
  Pallas kernels  17.4 us (8%)
  local copies, waits for them, and re-layouts  10.8 us (5%)
  other arithmetic  6.07 us (3%)
    all_to_all x1, starting transfers between devices, local(): lax.all_to_all(buffer.reshape(EXPERTS, CAPACITY, D), 'sp', 0, 0, tiled=True)  38.4 us
    all_to_all x1, waiting for transfers between devices, local(): lax.all_to_all(sent, 'sp', 0, 0, axis_index_groups=groups, tiled=True)  31.1 us
    all_to_all x1, waiting for transfers between devices, local(): lax.all_to_all(buffer.reshape(EXPERTS, CAPACITY, D), 'sp', 0, 0, tiled=True)  30.1 us
    all_to_all x1, waiting for transfers between devices, local(): back = lax.all_to_all(result, 'sp', 0, 0, tiled=True).reshape(SLOTS, D)  29.7 us
    dot_general x2, matrix products, local(): jnp.dot(hidden, down, preferred_element_type=f32).astype(bf16)  12.6 us
    unnamed x34, local copies, waits for them, and re-layouts  10.6 us
    ppermute x2, starting transfers between devices, local(): lax.ppermute(payload, 'sp', [(i, i + PLANE * k) for i in range(sp - PLANE...  8.83 us
    pallas_call x1, Pallas kernels, local(): pl.pallas_call(attend_kernel, out_shape=(stat, stat), in_specs=[vmem()] *...  8.8 us
  transfers between devices with their start and end apart: 10, of which 6 were waited for; matrix products, arithmetic and copies ran while one was open for 2% of the time, Pallas kernels for 3%

profile of v1, /device:TPU:0, one launch (start us, length us, event | category | flops | bytes accessed | tf_op | source)
XLA Modules:
  0.0 214.0 jit_solution(17100973637207463421)
XLA Ops:
  0.0 1.2 copy.16.q_ref
  1.2 0.8 copy.17.rope_ref
  2.0 0.5 multiply_sine_fusion
  2.6 0.0 copy-start.5
  2.6 0.9 copy-done.5
  3.5 0.0 copy-start.6
  3.5 0.9 copy-done.6
  4.4 0.0 copy-start.7
  4.4 0.9 copy-done.7
  5.3 0.0 copy-start.8
  5.3 0.7 copy-done.8
  6.0 0.8 prep.1
  6.8 5.9 %collective-permute-start.1 = (bf16[304,128]{1,0:T(8,128)(2,1)S(1)}, bf16[304,128]{1,0:T(8,128)(2,1)S(1)}, u32[]{:S(2)}, u32[]{:S(2)}) collective-permute-start(bf16[304,128]{1,0:T(8,128)(2,1)S(1)} %get-tuple-element.11), channel_id=1, source_target_pairs={{0,64},{2,66},{4,68},{6,70},{8,72},{10,74},{12,76},{14,78},{16,80}... | collective-permute-start | bytes 233480 | tf_op jit(solution)/shard_map/ppermute | solution.py:344
  12.7 2.9 %collective-permute-start = (bf16[304,128]{1,0:T(8,128)(2,1)S(1)}, bf16[304,128]{1,0:T(8,128)(2,1)S(1)}, u32[]{:S(2)}, u32[]{:S(2)}) collective-permute-start(bf16[304,128]{1,0:T(8,128)(2,1)S(1)} %get-tuple-element.11), channel_id=1, source_target_pairs={{0,32},{2,34},{4,36},{6,38},{8,40},{10,42},{12,44},{14,46},{16,48}... | collective-permute-start | bytes 233480 | tf_op jit(solution)/shard_map/ppermute | solution.py:344
  15.7 0.0 collective-permute-done.1.ext_ref
  15.7 0.2 broadcast_select_fusion
  15.9 1.8 collective-permute-done
  17.7 0.2 stack_broadcast_in_dim.2
  17.8 1.7 pad_maximum_fusion
  19.5 0.0 copy-start.9
  19.5 7.2 %all-to-all-start = ((bf16[16,2,304,128]{3,2,1,0:T(8,128)(2,1)}), bf16[16,2,304,128]{3,2,1,0:T(8,128)(2,1)S(1)}, u32[]{:S(2)}, u32[]{:S(2)}) async-start(bf16[16,2,304,128]{3,2,1,0:T(8,128)(2,1)} %pad_maximum_fusion), calls=%async_computation | async-start | bytes 4980736 | tf_op jit(solution)/shard_map/all_to_all | solution.py:352
  26.7 0.1 collective-permute-start.2
  26.8 0.0 copy-done.9
  26.8 2.3 %collective-permute-done.2.oth_ref = bf16[256,1664]{1,0:T(8,128)(2,1)S(1)} collective-permute-done((bf16[256,1664]{1,0:T(8,128)(2,1)S(1)}, bf16[256,1664]{1,0:T(8,128)(2,1)S(1)}, u32[]{:S(2)}, u32[]{:S(2)}) %collective-permute-start.2) | collective-permute-done | bytes 852000 | tf_op jit(solution)/shard_map/ppermute | solution.py:345
  29.1 0.0 copy-start
  29.1 0.9 copy-done
  30.1 31.1 %all-to-all-done.arr_ref = bf16[16,2,304,128]{3,2,1,0:T(8,128)(2,1)S(1)} async-done(((bf16[16,2,304,128]{3,2,1,0:T(8,128)(2,1)}), bf16[16,2,304,128]{3,2,1,0:T(8,128)(2,1)S(1)}, u32[]{:S(2)}, u32[]{:S(2)}) %all-to-all-start) | async-done | bytes 2490400 | tf_op jit(solution)/shard_map/all_to_all | solution.py:352
  61.2 0.1 broadcast_in_dim.50.qdoc_ref
  61.3 0.0 copy-start.1
  61.3 1.2 copy-done.1
  62.4 0.0 copy-start.13
  62.4 0.0 copy-start.10
  62.4 0.0 copy-start.11
  62.4 8.8 %attend.1 = (f32[128,896]{1,0:T(8,128)S(1)}, f32[128,896]{1,0:T(8,128)}) custom-call(bf16[16,2,304,128]{3,2,1,0:T(8,128)(2,1)S(1)} %all-to-all-done.arr_ref, bf16[304,128]{1,0:T(8,128)(2,1)S(1)} %collective-permute-done.1.ext_ref, bf16[256,1664]{1,0:T(8,128)(2,1)S(1)} %get-tuple-element.12.own_ref, bf16[256,1664]{1,0:T(8,128)(2,1)S(1)} %copy-done.1, ...), custom_call_target="tpu_custom_call" | custom-call | tf_op jit(solution)/shard_map/attend/pallas_call | solution.py:355
  71.2 0.0 copy-start.3
  71.3 0.8 copy-done.3
  72.0 0.0 collective-permute-start.3
  72.0 0.5 collective-permute-start.5
  72.5 0.0 copy-done.13
  72.5 0.1 copy.18.ids_ref
  72.7 1.4 collective-permute-done.3.theirs_ref
  74.1 0.0 copy-done.10
  74.1 0.0 copy-done.11
  74.1 1.0 copy-done.2
  75.1 1.0 copy-done.4
  76.1 5.9 %mix.1 = (bf16[128,2048]{1,0:T(8,128)(2,1)S(1)}, bf16[512,2048]{1,0:T(8,128)(2,1)}) custom-call(f32[128,896]{1,0:T(8,128)S(1)} %copy-done.4, f32[128,896]{1,0:T(8,128)S(1)} %collective-permute-done.3.theirs_ref, bf16[768,2048]{1,0:T(8,128)(2,1)} %proj_ref.1, bf16[128,2048]{1,0:T(8,128)(2,1)S(1)} %copy-done.2, f32[1,2048]{1,0:T(1,128)S(1)} %bitcast.41, ...), custom_call_target="tpu_custom_call" | custom-call | tf_op jit(solution)/shard_map/mix/pallas_call | solution.py:374
  82.0 38.4 %all-to-all-start.1 = ((bf16[64,8,2048]{2,1,0:T(8,128)(2,1)}), bf16[64,8,2048]{2,1,0:T(8,128)(2,1)S(1)}, u32[]{:S(2)}, u32[]{:S(2)}) async-start(bf16[64,8,2048]{2,1,0:T(8,128)(2,1)} %bitcast.3), calls=%async_computation.1 | async-start | bytes 4194304 | tf_op jit(solution)/shard_map/all_to_all | solution.py:382
  120.4 0.2 collective-permute-start.6
  120.6 0.4 collective-permute-start.4
  121.0 0.0 collective-permute-done.5
  121.0 30.1 %all-to-all-done.1 = bf16[64,8,2048]{2,1,0:T(8,128)(2,1)S(1)} async-done(((bf16[64,8,2048]{2,1,0:T(8,128)(2,1)}), bf16[64,8,2048]{2,1,0:T(8,128)(2,1)S(1)}, u32[]{:S(2)}, u32[]{:S(2)}) %all-to-all-start.1) | async-done | bytes 2097184 | tf_op jit(solution)/shard_map/all_to_all | solution.py:382
  151.1 4.6 %fusion.1 = f32[512,512]{1,0:T(8,128)} fusion(bf16[2048,512]{1,0:T(8,128)(2,1)} %collective-permute-done.5, bf16[64,8,2048]{2,1,0:T(8,128)(2,1)S(1)} %all-to-all-done.1), kind=kOutput, calls=%fused_computation.5 | convolution fusion | flops 1073741824 | bytes 5242880 | tf_op jit(solution)/shard_map/dot_general | solution.py:388
  155.8 0.0 copy-done.12
  155.8 0.0 collective-permute-done.6
  155.8 0.0 collective-permute-done.4
  155.8 5.7 %convolution_convert_fusion = bf16[512,2048]{1,0:T(8,128)(2,1)S(1)} fusion(bf16[512,2048]{1,0:T(8,128)(2,1)} %collective-permute-done.6, f32[512,512]{1,0:T(8,128)} %fusion.1, bf16[2048,512]{1,0:T(8,128)(2,1)} %collective-permute-done.4, bf16[64,8,2048]{2,1,0:T(8,128)(2,1)} %copy-done.12), kind=kOutput, calls=%fused_computation.1 | convolution fusion | flops 2150105088 | bytes 9437184 | tf_op jit(solution)/shard_map/dot_general | solution.py:390
  161.4 4.5 %fusion.7 = f32[512,512]{1,0:T(8,128)} fusion(bf16[64,8,2048]{2,1,0:T(8,128)(2,1)} %copy-done.12, bf16[1,2048,512]{2,1,0:T(8,128)(2,1)} %param.27), kind=kOutput, calls=%fused_computation.11 | convolution fusion | flops 1073741824 | bytes 5242880 | tf_op jit(solution)/shard_map/dot_general | solution.py:387
  165.9 6.9 %convolution_convert_fusion.1 = bf16[512,2048]{1,0:T(8,128)(2,1)} fusion(bf16[64,8,2048]{2,1,0:T(8,128)(2,1)} %copy-done.12, f32[512,512]{1,0:T(8,128)} %fusion.7, bf16[1,512,2048]{2,1,0:T(8,128)(2,1)} %param.29, bf16[1,2048,512]{2,1,0:T(8,128)(2,1)} %param.28), kind=kOutput, calls=%fused_computation.2 | convolution fusion | flops 2150105088 | bytes 9437184 | tf_op jit(solution)/shard_map/dot_general | solution.py:390
  172.9 3.7 %fusion = bf16[64,8,2048]{2,1,0:T(8,128)(2,1)} fusion(bf16[512,2048]{1,0:T(8,128)(2,1)S(1)} %convolution_convert_fusion, bf16[512,2048]{1,0:T(8,128)(2,1)} %convolution_convert_fusion.1), kind=kLoop, calls=%fused_computation.4 | loop fusion | flops 4194304 | bytes 6291456 | tf_op jit(solution)/shard_map/reshape | solution.py:392
  176.5 5.7 %all-to-all-start.2 = ((bf16[64,8,2048]{2,1,0:T(8,128)(2,1)}), bf16[64,8,2048]{2,1,0:T(8,128)(2,1)S(1)}, u32[]{:S(2)}, u32[]{:S(2)}) async-start(bf16[64,8,2048]{2,1,0:T(8,128)(2,1)} %fusion), calls=%async_computation.2 | async-start | bytes 4194304 | tf_op jit(solution)/shard_map/all_to_all | solution.py:393
  182.2 0.0 copy-done.14
  182.2 0.1 copy.20.weight_ref
  182.3 29.7 %all-to-all-done.2 = bf16[64,8,2048]{2,1,0:T(8,128)(2,1)S(1)} async-done(((bf16[64,8,2048]{2,1,0:T(8,128)(2,1)}), bf16[64,8,2048]{2,1,0:T(8,128)(2,1)S(1)}, u32[]{:S(2)}, u32[]{:S(2)}) %all-to-all-start.2) | async-done | bytes 2097184 | tf_op jit(solution)/shard_map/all_to_all | solution.py:393
  212.1 1.9 pick.1
  (8 shorter events, 0.0 us)
Async XLA Ops:
  2.6 0.9 copy-start.5
  3.5 0.9 copy-start.6
  4.4 0.9 copy-start.7
  5.3 0.7 copy-start.8
  6.8 8.9 %collective-permute-start.1 = (bf16[304,128]{1,0:T(8,128)(2,1)S(1)}, bf16[304,128]{1,0:T(8,128)(2,1)S(1)}, u32[]{:S(2)}, u32[]{:S(2)}) collective-permute-start(bf16[304,128]{1,0:T(8,128)(2,1)S(1)} %get-tuple-element.11), channel_id=1, source_target_pairs={{0,64},{2,66},{4,68},{6,70},{8,72},{10,74},{12,76},{14,78},{16,80}... | collective-permute-start | bytes 233480 | tf_op jit(solution)/shard_map/ppermute | solution.py:344
  12.7 4.9 %collective-permute-start = (bf16[304,128]{1,0:T(8,128)(2,1)S(1)}, bf16[304,128]{1,0:T(8,128)(2,1)S(1)}, u32[]{:S(2)}, u32[]{:S(2)}) collective-permute-start(bf16[304,128]{1,0:T(8,128)(2,1)S(1)} %get-tuple-element.11), channel_id=1, source_target_pairs={{0,32},{2,34},{4,36},{6,38},{8,40},{10,42},{12,44},{14,46},{16,48}... | collective-permute-start | bytes 233480 | tf_op jit(solution)/shard_map/ppermute | solution.py:344
  19.5 7.3 %copy-start.9 = (s32[256]{0:T(256)S(1)}, s32[256]{0:T(256)}, u32[]{:S(2)}) copy-start(s32[256]{0:T(256)} %doc_ref.1) | copy-start | bytes 3076
  19.5 41.7 %all-to-all-start = ((bf16[16,2,304,128]{3,2,1,0:T(8,128)(2,1)}), bf16[16,2,304,128]{3,2,1,0:T(8,128)(2,1)S(1)}, u32[]{:S(2)}, u32[]{:S(2)}) async-start(bf16[16,2,304,128]{3,2,1,0:T(8,128)(2,1)} %pad_maximum_fusion), calls=%async_computation | async-start | bytes 4980736 | tf_op jit(solution)/shard_map/all_to_all | solution.py:352
  26.7 2.5 %collective-permute-start.2 = (bf16[256,1664]{1,0:T(8,128)(2,1)S(1)}, bf16[256,1664]{1,0:T(8,128)(2,1)S(1)}, u32[]{:S(2)}, u32[]{:S(2)}) collective-permute-start(bf16[256,1664]{1,0:T(8,128)(2,1)S(1)} %get-tuple-element.12.own_ref), channel_id=1, source_target_pairs={{0,1},{1,0},{2,3},{3,2},{4,5},{5,4},{6,7},{7,6},{8,9},{9,8},{10,11... | collective-permute-start | bytes 2555912 | tf_op jit(solution)/shard_map/ppermute | solution.py:345
  29.1 0.9 copy-start
  61.3 1.2 copy-start.1
  62.4 10.1 %copy-start.13 = (s32[128,2]{0,1:T(2,128)S(1)}, s32[128,2]{0,1:T(2,128)}, u32[]{:S(2)}) copy-start(s32[128,2]{0,1:T(2,128)} %param.25) | copy-start | bytes 3076
  62.4 11.6 %copy-start.10 = (f32[2048]{0:T(1024)S(1)}, f32[2048]{0:T(1024)}, u32[]{:S(2)}) copy-start(f32[2048]{0:T(1024)} %param.23) | copy-start | bytes 24580
  62.4 11.6 %copy-start.11 = (f32[2048]{0:T(1024)S(1)}, f32[2048]{0:T(1024)}, u32[]{:S(2)}) copy-start(f32[2048]{0:T(1024)} %param.24) | copy-start | bytes 24580
  71.2 0.8 copy-start.3
  72.0 2.0 collective-permute-start.3
  72.0 49.0 %collective-permute-start.5 = (bf16[2048,512]{1,0:T(8,128)(2,1)}, bf16[2048,512]{1,0:T(8,128)(2,1)}, u32[]{:S(2)}, u32[]{:S(2)}) collective-permute-start(bf16[2048,512]{1,0:T(8,128)(2,1)} %bitcast.6), channel_id=1, source_target_pairs={{0,1},{1,0},{2,3},{3,2},{4,5},{5,4},{6,7},{7,6},{8,9},{9,8},{10,11... | collective-permute-start | bytes 6291464 | tf_op jit(solution)/shard_map/ppermute | solution.py:384
  74.1 1.0 copy-start.2
  75.1 1.0 copy-start.4
  82.0 69.1 %all-to-all-start.1 = ((bf16[64,8,2048]{2,1,0:T(8,128)(2,1)}), bf16[64,8,2048]{2,1,0:T(8,128)(2,1)S(1)}, u32[]{:S(2)}, u32[]{:S(2)}) async-start(bf16[64,8,2048]{2,1,0:T(8,128)(2,1)} %bitcast.3), calls=%async_computation.1 | async-start | bytes 4194304 | tf_op jit(solution)/shard_map/all_to_all | solution.py:382
  120.4 35.3 %collective-permute-start.6 = (bf16[512,2048]{1,0:T(8,128)(2,1)}, bf16[512,2048]{1,0:T(8,128)(2,1)}, u32[]{:S(2)}, u32[]{:S(2)}) collective-permute-start(bf16[512,2048]{1,0:T(8,128)(2,1)} %bitcast.44), channel_id=1, source_target_pairs={{0,1},{1,0},{2,3},{3,2},{4,5},{5,4},{6,7},{7,6},{8,9},{9,8},{10,11... | collective-permute-start | bytes 6291464 | tf_op jit(solution)/shard_map/ppermute | solution.py:384
  120.6 35.1 %collective-permute-start.4 = (bf16[2048,512]{1,0:T(8,128)(2,1)}, bf16[2048,512]{1,0:T(8,128)(2,1)}, u32[]{:S(2)}, u32[]{:S(2)}) collective-permute-start(bf16[2048,512]{1,0:T(8,128)(2,1)} %bitcast.43), channel_id=1, source_target_pairs={{0,1},{1,0},{2,3},{3,2},{4,5},{5,4},{6,7},{7,6},{8,9},{9,8},{10,11... | collective-permute-start | bytes 6291464 | tf_op jit(solution)/shard_map/ppermute | solution.py:384
  151.1 4.6 %copy-start.12 = (bf16[64,8,2048]{2,1,0:T(8,128)(2,1)}, bf16[64,8,2048]{2,1,0:T(8,128)(2,1)S(1)}, u32[]{:S(2)}) copy-start(bf16[64,8,2048]{2,1,0:T(8,128)(2,1)S(1)} %all-to-all-done.1) | copy-start | bytes 6291460
  176.5 5.7 %copy-start.14 = (f32[128,2]{0,1:T(2,128)S(1)}, f32[128,2]{0,1:T(2,128)}, u32[]{:S(2)}) copy-start(f32[128,2]{0,1:T(2,128)} %param.26) | copy-start | bytes 3076
  176.5 35.5 %all-to-all-start.2 = ((bf16[64,8,2048]{2,1,0:T(8,128)(2,1)}), bf16[64,8,2048]{2,1,0:T(8,128)(2,1)S(1)}, u32[]{:S(2)}, u32[]{:S(2)}) async-start(bf16[64,8,2048]{2,1,0:T(8,128)(2,1)} %fusion), calls=%async_computation.2 | async-start | bytes 4194304 | tf_op jit(solution)/shard_map/all_to_all | solution.py:393

commit v2 on v1

v2 whole, which is shorter than its diff:
```python
import functools
import math

import jax
import jax.numpy as jnp
from jax import lax
from jax.experimental import pallas as pl
from jax.experimental.pallas import tpu as pltpu
from jax.sharding import PartitionSpec as P

D = 2048
NOPE = 64
ROPE = 32
HALF = 128
BLOCK = 256
HEADS = 12
LOCAL_HEADS = 6
PLANE = 16
ROWS = 304
CAPACITY = 8
EXPERTS = 64
SLOTS = EXPERTS * CAPACITY
QW = LOCAL_HEADS * 128
KW = 512
VW = 384
PACK = QW + KW + VW
epsilon = 1e-06
ATTEND_MIB = 24
LOW = -1e30
SCALE = (NOPE + ROPE) ** -0.5 * math.log2(math.e)
f32 = jnp.float32
bf16 = jnp.bfloat16


def vmem():
    return pl.BlockSpec(memory_space=pltpu.VMEM)


def smem():
    return pl.BlockSpec(memory_space=pltpu.SMEM)


def hbm():
    return pl.BlockSpec(memory_space=pltpu.HBM)


def far(x):
    return pltpu.with_memory_space_constraint(x, pltpu.HBM)


def params(mib):
    return pltpu.CompilerParams(vmem_limit_bytes=mib * 1024 * 1024)


def lanes(rows):
    return lax.broadcasted_iota(jnp.int32, (rows, 128), 1)


def turn(first, second, cosine, sine):
    return first * cosine - second * sine, second * cosine + first * sine


def prep_kernel(*refs):
    inputs, (pay_ref, pack_ref) = refs[:8], refs[8:10]
    held, sems = refs[10:18], refs[18]
    copies = [pltpu.make_async_copy(src, dst, sems.at[i]) for i, (src, dst) in enumerate(zip(inputs, held))]
    for copy in copies:
        copy.start()
    for copy in copies:
        copy.wait()
    q_ref, lat_ref, rope_ref, doc_ref, wk_ref, wv_ref, cos_ref, sin_ref = held
    half = lax.axis_index("tp")
    cosine, sine = cos_ref[...], sin_ref[...]
    mine = pl.ds(pl.multiple_of(half * HALF, HALF), HALF)
    pay_ref[0:128, :] = lat_ref[mine, 0:128]
    pay_ref[128:256, :] = lat_ref[mine, 128:256]
    rope = rope_ref[...].astype(f32)
    turned = jnp.concatenate(turn(rope[:16], rope[16:], cosine, sine), axis=0)
    turned = jnp.where(half == 0, turned[:, :128], turned[:, 128:])
    turned = jnp.concatenate([turned, jnp.zeros((96, 128), f32)], axis=0).T
    packed = turned[0:32, :]
    for c in range(1, 4):
        packed = packed + pltpu.roll(turned[32 * c : 32 * c + 32, :], 32 * c, 1)
    pay_ref[256:288, :] = packed.astype(bf16)
    docs = doc_ref[pl.ds(half, 1), :].astype(f32)
    pay_ref[288:304, :] = jnp.broadcast_to(docs, (16, 128)).astype(bf16)
    lane = lanes(BLOCK)
    for head in range(LOCAL_HEADS):
        start = head * (NOPE + ROPE)
        plain = q_ref[start : start + NOPE, :].astype(f32)
        rot = q_ref[start + NOPE : start + NOPE + ROPE, :].astype(f32)
        x = jnp.concatenate([plain, *turn(rot[:16], rot[16:], cosine, sine), jnp.zeros((32, BLOCK), f32)], axis=0)
        pack_ref[:, head * 128 : head * 128 + 128] = x.T.astype(bf16)
    w0 = wk_ref[:, 0:128]
    w1 = wk_ref[:, 128:256].astype(f32)
    w2 = wk_ref[:, 256:384].astype(f32)
    r1, r2 = pltpu.roll(w1, 64, 1), pltpu.roll(w2, 64, 1)
    pack_ref[:, QW : QW + 128] = w0
    pack_ref[:, QW + 128 : QW + 256] = jnp.where(lane < 64, w1, 0.0).astype(bf16)
    pack_ref[:, QW + 256 : QW + 384] = jnp.where(lane < 64, r1, r2).astype(bf16)
    pack_ref[:, QW + 384 : QW + 512] = jnp.where(lane < 64, r2, 0.0).astype(bf16)
    pack_ref[:, QW + KW : PACK] = wv_ref[...]


def spread_kernel(own_ref, oth_ref, q_ref):
    lane = lanes(BLOCK)
    for head in range(HEADS):
        src = own_ref if head < LOCAL_HEADS else oth_ref
        local = head % LOCAL_HEADS
        x = src[:, local * 128 : local * 128 + 128].astype(f32)
        if head % 3 == 2:
            lo, hi = jnp.zeros_like(x), x
        else:
            lo, hi = jnp.where(lane < 64, x, 0.0), jnp.where(lane < 64, 0.0, x)
            if head % 3 == 1:
                lo = pltpu.roll(lo, 64, 1)
        q_ref[head, :, 0:128] = lo.astype(bf16)
        q_ref[head, :, 128:256] = hi.astype(bf16)


def attend_kernel(late, *refs):
    if late:
        ext_ref, refs = refs[0], refs[1:]
    src_ref, q_ref, own_ref, oth_ref, qdoc_ref, doc_ref, mine_ref, theirs_ref = refs[:8]
    k_s, v_s, m_s, a_s, bias_s, full_s, arr_ref, sem = refs[8:]
    fetch = pltpu.make_async_copy(src_ref, arr_ref, sem)
    fetch.start()
    half = lax.axis_index("tp")
    seat = lax.axis_index("sp")
    plane, spot = seat // PLANE, seat % PLANE
    doc_first = doc_ref[0].astype(f32)
    doc_last = doc_ref[BLOCK - 1].astype(f32)
    lane = lanes(BLOCK)
    m_s[...] = jnp.full(m_s.shape, LOW, f32)
    a_s[...] = jnp.zeros(a_s.shape, f32)
    fetch.wait()

    def block_of(i):
        if not late:
            return (plane - 1) * PLANE + i
        return (plane - jnp.where(i <= spot, 0, 2)) * PLANE + i

    def place(block):
        return jnp.where(block >= 0, block * BLOCK + half * HALF, -1)

    groups = [[(arr_ref, 8 * t + b, block_of(8 * t + b)) for b in range(8)] for t in range(2)]
    if late:
        groups.append([(ext_ref, None, (plane - 2) * PLANE + spot)])
    row_lane = lax.broadcasted_iota(jnp.int32, (1, 128), 1)
    code = jnp.zeros((1, 128), f32)
    for t, group in enumerate(groups):
        high = low = None
        for ref, i, block in group:
            docs = (ref[288:304, :] if i is None else ref[i, 288:304, :]).astype(f32)[0:1, :]
            seen = jnp.where(block >= 0, docs, -1.0)
            bound = jnp.where(block == seat, -1.0, seen)
            high = seen if high is None else jnp.maximum(high, seen)
            low = bound if low is None else jnp.minimum(low, bound)
        code = code + jnp.where((row_lane == 127) & (high >= doc_first), float(2 ** (2 * t)), 0.0)
        code = code + jnp.where((row_lane == 0) & (low == doc_last), float(2 ** (2 * t + 1)), 0.0)
    code = jnp.sum(code).astype(jnp.int32)

    def heads(count, masked):
        panels = count // 128

        def side(number, carried):
            first = number * LOCAL_HEADS

            def score(head):
                return lax.dot_general(
                    q_ref[first + head],
                    k_s[2 * number + head // 3, :count, :],
                    (((1,), (1,)), ((), ())),
                    preferred_element_type=f32,
                )

            following = score(0)
            for head in range(LOCAL_HEADS):
                s = following
                if head + 1 < LOCAL_HEADS:
                    following = score(head + 1)
                at = first + head
                parts = [s[:, 128 * b : 128 * b + 128] for b in range(panels)]
                if masked:
                    parts = [part + bias_s[:, 128 * b : 128 * b + 128] for b, part in enumerate(parts)]
                top = parts[0]
                for part in parts[1:]:
                    top = jnp.maximum(top, part)
                old = m_s[at]
                new = jnp.maximum(old, jnp.max(top, axis=1, keepdims=True))
                keep = jnp.exp2((old - new) * SCALE)
                m_s[at] = new
                weights = [jnp.exp2((part - new) * SCALE).astype(bf16) for part in parts]
                rounded = jnp.concatenate(weights, axis=1) if panels > 1 else weights[0]
                a_s[at] = a_s[at] * keep + jnp.dot(rounded, v_s[at, :count, :], preferred_element_type=f32)
            return carried

        lax.fori_loop(0, 2, side, 0)

    def tile(load, blocks, flags):
        panels = len(blocks)
        count = panels * 128
        active = (flags & 1) == 1
        plain = (flags & 2) == 2

        @pl.when(active)
        def _():
            lat = jnp.concatenate(
                [
                    jnp.concatenate([load(b, 0, 128) for b in range(panels)], axis=0),
                    jnp.concatenate([load(b, 128, 256) for b in range(panels)], axis=0),
                ],
                axis=1,
            )
            turned = []
            for b in range(panels):
                r = load(b, 256, 288).astype(f32)
                turned += [pltpu.roll(r, 64, 1), pltpu.roll(r, 32, 1), r, pltpu.roll(r, 96, 1)]
            turned = jnp.concatenate(turned, axis=0)
            wide = lanes(count)
            turned = jnp.where((wide >= 64) & (wide < 96), turned, 0.0)
            for side, src in enumerate((own_ref, oth_ref)):
                keys = jnp.dot(lat, src[:, QW : QW + KW], preferred_element_type=f32)
                for g in range(2):
                    at = side * 2 + g
                    k_s[at, :count, 0:128] = keys[:, g * 256 : g * 256 + 128].astype(bf16)
                    k_s[at, :count, 128:256] = (keys[:, g * 256 + 128 : g * 256 + 256] + turned).astype(bf16)
                rows = jnp.dot(lat, src[:, QW + KW : PACK], preferred_element_type=f32)
                for pair in range(3):
                    both = rows[:, pair * 128 : pair * 128 + 128]
                    at = side * LOCAL_HEADS + pair * 2
                    v_s[at, :count, :] = jnp.where(wide < 64, both, 1.0).astype(bf16)
                    v_s[at + 1, :count, :] = jnp.where(wide < 64, 1.0, both).astype(bf16)

        if panels > 1:

            @pl.when(active & plain)
            def _():
                heads(count, False)

        @pl.when(active & jnp.logical_not(plain) if panels > 1 else active)
        def _():
            at_query = seat * BLOCK + lax.broadcasted_iota(jnp.int32, (BLOCK, 128), 0)
            for b in range(panels):
                base = place(blocks[b])
                at_key = jnp.where(base >= 0, base, 1 << 20) + lane
                docs = load(b, 288, 304).astype(f32)[0:1, :]
                allowed = (at_key <= at_query) & (docs == qdoc_ref[...])
                bias_s[:, 128 * b : 128 * b + 128] = jnp.where(allowed, 0.0, LOW)
            heads(count, True)

    if late:
        tile(lambda b, lo, hi: ext_ref[lo:hi, :], [groups[2][0][2]], code >> 4)

    def step(number, carried):
        blocks = [block_of(number * 8 + b) for b in range(8)]
        tile(lambda b, lo, hi: arr_ref[number * 8 + b, lo:hi, :], blocks, code >> (2 * number))
        return carried

    lax.fori_loop(0, 2, step, 0)

    stats = jnp.zeros((BLOCK, 128), f32)
    for head in range(HEADS):
        at = head + jnp.where(half == 0, 0, LOCAL_HEADS if head < LOCAL_HEADS else -LOCAL_HEADS)
        stats = jnp.where(lane == at, m_s[head], stats)
        spare = 64 if head % 2 == 0 else 0
        stats = jnp.where(lane == at + 16, a_s[head, :, spare : spare + 1], stats)
    full_s[:, 768:896] = stats
    for pair in range(6):
        both = jnp.where(lane < 64, a_s[2 * pair], a_s[2 * pair + 1])

        @pl.when(half == 0)
        def _():
            full_s[:, pair * 128 : pair * 128 + 128] = both

        @pl.when(half == 1)
        def _():
            at = (pair + 3) % 6
            full_s[:, at * 128 : at * 128 + 128] = both

    mine_ref[...] = full_s[pl.ds(pl.multiple_of(half * HALF, HALF), HALF), :]
    theirs_ref[...] = full_s[pl.ds(pl.multiple_of((1 - half) * HALF, HALF), HALF), :]


def slots_of(ids):
    expert = lax.broadcasted_iota(jnp.int32, (EXPERTS, HALF), 0)
    named = [(ids[k : k + 1, :] == expert) for k in range(2)]
    counts = named[0].astype(f32) + named[1].astype(f32)
    row = lax.broadcasted_iota(jnp.int32, (HALF, HALF), 0)
    col = lax.broadcasted_iota(jnp.int32, (HALF, HALF), 1)
    earlier = jnp.dot(counts.astype(bf16), (row < col).astype(f32).astype(bf16), preferred_element_type=f32)
    slot = lax.broadcasted_iota(jnp.int32, (SLOTS, HALF), 0)
    picks = []
    for k in range(2):
        rank = jnp.sum(jnp.where(named[k], earlier, 0.0), axis=0, keepdims=True)
        at = ids[k : k + 1, :] * CAPACITY + rank.astype(jnp.int32)
        picks.append((slot == at).astype(f32).astype(bf16))
    return picks


def norm_of(x):
    return lax.rsqrt(jnp.mean(x * x, axis=-1, keepdims=True) + epsilon)


def mix_kernel(*refs):
    parts, (proj_ref, res_ref, mixg_ref, moeg_ref, ids_ref, mid_ref, buf_ref) = refs[:4], refs[4:]
    lane = lanes(HALF)
    stats = [part[:, 768:896] for part in parts]
    top = jnp.maximum(jnp.maximum(stats[0], stats[1]), jnp.maximum(stats[2], stats[3]))
    shares = [jnp.exp2((s - top) * SCALE) for s in stats]
    panels = []
    for pair in range(6):
        cols = slice(pair * 128, pair * 128 + 128)
        value, total = 0.0, 0.0
        for part, s, share in zip(parts, stats, shares):
            even, odd = share[:, 2 * pair : 2 * pair + 1], share[:, 2 * pair + 1 : 2 * pair + 2]
            scale = jnp.where(lane < 64, even, odd)
            value = value + part[:, cols] * scale
            total = total + scale * jnp.where(lane < 64, s[:, 16 + 2 * pair : 17 + 2 * pair], s[:, 17 + 2 * pair : 18 + 2 * pair])
        panels.append((value / total).astype(bf16))
    attended = jnp.concatenate(panels, axis=1)
    mix = jnp.dot(attended, proj_ref[...], preferred_element_type=f32)
    branch = mix * norm_of(mix) * mixg_ref[...]
    middle = (res_ref[...].astype(f32) + branch).astype(bf16)
    mid_ref[...] = middle
    wide = middle.astype(f32)
    normed = (wide * norm_of(wide) * moeg_ref[...]).astype(bf16)
    picks = slots_of(ids_ref[...])
    buf_ref[...] = jnp.dot(picks[0] + picks[1], normed, preferred_element_type=f32).astype(bf16)


def expert_kernel(rows_ref, *refs):
    weights, out_ref, held, first_s, sems = refs[:6], refs[6], refs[7:13], refs[13], refs[14]
    copies = [pltpu.make_async_copy(src, dst, sems.at[i]) for i, (src, dst) in enumerate(zip(weights, held))]
    for copy in copies:
        copy.start()
    rows = rows_ref[...]
    for side in range(2):
        gate, up, down = held[3 * side : 3 * side + 3]
        copies[3 * side].wait()
        gated = jnp.dot(rows, gate[...], preferred_element_type=f32)
        copies[3 * side + 1].wait()
        upward = jnp.dot(rows, up[...], preferred_element_type=f32)
        hidden = (gated / (1.0 + jnp.exp(-gated)) * upward).astype(bf16)
        copies[3 * side + 2].wait()
        part = jnp.dot(hidden, down[...], preferred_element_type=f32).astype(bf16)
        if side == 0:
            first_s[...] = part
        else:
            out_ref[...] = (first_s[...].astype(f32) + part.astype(f32)).astype(bf16)


def pick_kernel(back_ref, mid_ref, ids_ref, weight_ref, out_ref):
    picks = slots_of(ids_ref[...])
    total = mid_ref[...].astype(f32)
    for k in range(2):
        rows = lax.dot_general(picks[k], back_ref[...], (((0,), (0,)), ((), ())), preferred_element_type=f32)
        column = jnp.broadcast_to(weight_ref[k : k + 1, :], (HALF, HALF)).T
        total = total + rows * column[:, 0:1]
    out_ref[...] = total.astype(bf16)


def local(
    residual,
    queries,
    latent,
    rope_key,
    doc_ids,
    latent_to_key,
    latent_to_value,
    out_proj,
    mix_gain,
    moe_gain,
    expert_ids,
    route_weight,
    gate_weight,
    up_weight,
    down_weight,
):
    sp = lax.axis_size("sp")
    seat = lax.axis_index("sp")
    spot = seat % PLANE
    swap = [(0, 1), (1, 0)]
    frequency = 10000.0 ** (-jnp.arange(16, dtype=f32) / 16)
    positions = seat * BLOCK + jnp.arange(BLOCK, dtype=jnp.int32)
    angles = positions.astype(f32)[None, :] * frequency[:, None]
    inputs = (queries.T, latent, rope_key.T, doc_ids.reshape(2, 128), latent_to_key, latent_to_value, jnp.cos(angles), jnp.sin(angles))
    payload, pack = pl.pallas_call(
        prep_kernel,
        out_shape=(jax.ShapeDtypeStruct((ROWS, 128), bf16), jax.ShapeDtypeStruct((BLOCK, PACK), bf16)),
        in_specs=[hbm()] * 8,
        out_specs=(vmem(), vmem()),
        scratch_shapes=[pltpu.VMEM(x.shape, x.dtype) for x in inputs] + [pltpu.SemaphoreType.DMA((8,))],
        compiler_params=params(8),
        name="prep",
    )(*map(far, inputs))
    before = [lax.ppermute(payload, "sp", [(i, i + PLANE * k) for i in range(sp - PLANE * k)]) for k in (1, 2)]
    other = lax.ppermute(pack, "tp", swap)
    target = jnp.arange(PLANE, dtype=jnp.int32)[:, None, None]
    groups = [[z * PLANE + i for i in range(PLANE)] for z in range(sp // PLANE)]
    late = lax.all_to_all(
        jnp.where(spot <= target, payload[None], before[1][None]), "sp", 0, 0, axis_index_groups=groups, tiled=True
    )
    early = lax.all_to_all(
        jnp.broadcast_to(before[0][None], (PLANE, ROWS, 128)), "sp", 0, 0, axis_index_groups=groups, tiled=True
    )
    query_docs = jnp.broadcast_to(doc_ids.astype(f32)[:, None], (BLOCK, 128))
    spread = pl.pallas_call(
        spread_kernel,
        out_shape=jax.ShapeDtypeStruct((HEADS, BLOCK, 256), bf16),
        in_specs=[vmem()] * 2,
        out_specs=vmem(),
        compiler_params=params(6),
        name="spread",
    )(pack, other)
    stat = jax.ShapeDtypeStruct((HALF, 896), f32)

    def attend(is_late, *operands):
        mine, theirs = pl.pallas_call(
            functools.partial(attend_kernel, is_late),
            out_shape=(pltpu.HBM((HALF, 896), f32),) * 2 if is_late else (stat, stat),
            in_specs=[vmem()] * (len(operands) - 1) + [hbm()] + [vmem()] * 4 + [smem()],
            out_specs=(vmem(), vmem()),
            scratch_shapes=[
                pltpu.VMEM((4, 1024, 256), bf16),
                pltpu.VMEM((HEADS, 1024, 128), bf16),
                pltpu.VMEM((HEADS, BLOCK, 128), f32),
                pltpu.VMEM((HEADS, BLOCK, 128), f32),
                pltpu.VMEM((BLOCK, 1024), f32),
                pltpu.VMEM((BLOCK, 896), f32),
                pltpu.VMEM((PLANE, ROWS, 128), bf16),
                pltpu.SemaphoreType.DMA(()),
            ],
            compiler_params=params(ATTEND_MIB),
            name="attend_late" if is_late else "attend_early",
        )(*operands[:-1], far(operands[-1]), spread, pack, other, query_docs, doc_ids)
        return mine, lax.ppermute(theirs, "tp", swap)

    parts = attend(True, before[1], late) + attend(False, early)
    middle, buffer = pl.pallas_call(
        mix_kernel,
        out_shape=(jax.ShapeDtypeStruct((HALF, D), bf16), pltpu.HBM((SLOTS, D), bf16)),
        in_specs=[vmem()] * 9,
        out_specs=(vmem(), vmem()),
        compiler_params=params(16),
        name="mix",
    )(*parts, out_proj, residual, mix_gain[None], moe_gain[None], expert_ids.T)
    rows = lax.all_to_all(buffer.reshape(EXPERTS, CAPACITY, D), "sp", 0, 0, tiled=True).reshape(SLOTS, D)
    own = (gate_weight[0], up_weight[0], down_weight[0])
    swapped = tuple(lax.ppermute(w, "tp", swap) for w in own)
    result = pl.pallas_call(
        expert_kernel,
        out_shape=jax.ShapeDtypeStruct((SLOTS, D), bf16),
        in_specs=[vmem()] + [hbm()] * 6,
        out_specs=vmem(),
        scratch_shapes=[pltpu.VMEM(w.shape, bf16) for w in own * 2]
        + [pltpu.VMEM((SLOTS, D), bf16), pltpu.SemaphoreType.DMA((6,))],
        compiler_params=params(32),
        name="experts",
    )(rows, *map(far, own + swapped)).reshape(EXPERTS, CAPACITY, D)
    back = lax.all_to_all(result, "sp", 0, 0, tiled=True).reshape(SLOTS, D)
    return pl.pallas_call(
        pick_kernel,
        out_shape=jax.ShapeDtypeStruct((HALF, D), bf16),
        in_specs=[vmem()] * 4,
        out_specs=vmem(),
        compiler_params=params(10),
        name="pick",
    )(back, middle, expert_ids.T, route_weight.T)


def solution(mesh):
    in_specs = (
        P(("sp", "tp"), None),
        P("sp", "tp"),
        P("sp", None),
        P("sp", None),
        P("sp"),
        P(None, "tp"),
        P(None, "tp"),
        P(),
        P(),
        P(),
        P(("sp", "tp"), None),
        P(("sp", "tp"), None),
        P("sp", None, "tp"),
        P("sp", None, "tp"),
        P("sp", "tp", None),
    )
    out_specs = P(("sp", "tp"), None)
    return jax.shard_map(local, mesh=mesh, in_specs=in_specs, out_specs=out_specs, check_vma=False)
```

time: 216 us -> 175 us (0.81)
  waiting for transfers between devices: 96.5 us -> 56.3 us
  blocking collectives: 0 us -> 35.4 us
  matrix products: 21.7 us -> 0 us
  starting transfers between devices: 61.3 us -> 46 us
  Pallas kernels: 17.4 us -> 31.6 us
  local copies, waits for them, and re-layouts: 10.8 us -> 1.45 us
  other arithmetic: 6.07 us -> 1.98 us
    all_to_all x2, waiting for transfers between devices: 60.8 us -> 19 us  [the longest x1 14 us: local(): lax.all_to_all(jnp.where(spot <= target, payload[None], before[1][None]),...]
    all_to_all x0 -> x1, blocking collectives: none -> 35.4 us  [local(): back = lax.all_to_all(result, 'sp', 0, 0, tiled=True).reshape(SLOTS, D)]
    dot_general x4 -> x0, matrix products: 21.7 us -> none  [the longest x2 12.6 us: local(): jnp.dot(hidden, down, preferred_element_type=f32).astype(bf16)]
    all_to_all x1, starting transfers between devices: 38.4 us -> 24.2 us  [local(): lax.all_to_all(buffer.reshape(EXPERTS, CAPACITY, D), 'sp', 0, 0, tiled=True)]
    pallas_call x1 -> x4, Pallas kernels: 8.8 us -> 22.1 us  [the longest x2 12.5 us: attend(): pl.pallas_call(functools.partial(attend_kernel, is_late), out_shape=(pltp...]
    unnamed x34 -> x18, local copies, waits for them, and re-layouts: 10.6 us -> 0.05 us
    reshape x1 -> x0, other arithmetic: 3.68 us -> none  [local(): result = result.astype(bf16).reshape(EXPERTS, CAPACITY, D)]
    ppermute x2, waiting for transfers between devices: 1.8 us -> 3.97 us  [local(): lax.ppermute(payload, 'sp', [(i, i + PLANE * k) for i in range(sp - PLANE...]
  transfers between devices with their start and end apart: 10 -> 11, of which waited for: 6 -> 7; matrix products, arithmetic and copies ran while one was open for 2% -> 0% of each run, Pallas kernels for 3% -> 11%
where the time goes in v2:
time: 175 us; the launch traced here: 173 us
  waiting for transfers between devices  56.3 us (32%)
  starting transfers between devices  46 us (26%)
  blocking collectives  35.4 us (20%)
  Pallas kernels  31.6 us (18%)
  other arithmetic  1.98 us (1%)
    all_to_all x1, blocking collectives, local(): back = lax.all_to_all(result, 'sp', 0, 0, tiled=True).reshape(SLOTS, D)  35.4 us
    all_to_all x1, waiting for transfers between devices, local(): lax.all_to_all(buffer.reshape(EXPERTS, CAPACITY, D), 'sp', 0, 0, tiled=True)  30.1 us
    all_to_all x1, starting transfers between devices, local(): lax.all_to_all(buffer.reshape(EXPERTS, CAPACITY, D), 'sp', 0, 0, tiled=True)  24.2 us
    all_to_all x1, waiting for transfers between devices, local(): lax.all_to_all(jnp.where(spot <= target, payload[None], before[1][None]),...  14 us
    pallas_call x2, Pallas kernels, attend(): pl.pallas_call(functools.partial(attend_kernel, is_late), out_shape=(pltp...  12.5 us
    pallas_call x1, Pallas kernels, local(): pl.pallas_call(expert_kernel, out_shape=jax.ShapeDtypeStruct((SLOTS, D),...  9.33 us
    ppermute x2, starting transfers between devices, local(): lax.ppermute(payload, 'sp', [(i, i + PLANE * k) for i in range(sp - PLANE...  8.83 us
    all_to_all x1, starting transfers between devices, local(): lax.all_to_all(jnp.where(spot <= target, payload[None], before[1][None]),...  7.03 us
  transfers between devices with their start and end apart: 11, of which 7 were waited for; matrix products, arithmetic and copies ran while one was open for 0% of the time, Pallas kernels for 11%

profile of v2, /device:TPU:0, one launch (start us, length us, event | category | flops | bytes accessed | tf_op | source)
XLA Modules:
  0.0 172.9 jit_solution(6291921069098176672)
XLA Ops:
  0.0 0.8 multiply_sine_fusion
  0.8 1.6 prep.1
  2.4 5.9 %collective-permute-start = (bf16[304,128]{1,0:T(8,128)(2,1)S(1)}, bf16[304,128]{1,0:T(8,128)(2,1)S(1)}, u32[]{:S(2)}, u32[]{:S(2)}) collective-permute-start(bf16[304,128]{1,0:T(8,128)(2,1)S(1)} %get-tuple-element.13), channel_id=1, source_target_pairs={{0,64},{2,66},{4,68},{6,70},{8,72},{10,74},{12,76},{14,78},{16,80}... | collective-permute-start | bytes 233480 | tf_op jit(solution)/shard_map/ppermute | solution.py:397
  8.3 2.0 %collective-permute-done.refs_0_ = bf16[304,128]{1,0:T(8,128)(2,1)S(1)} collective-permute-done((bf16[304,128]{1,0:T(8,128)(2,1)S(1)}, bf16[304,128]{1,0:T(8,128)(2,1)S(1)}, u32[]{:S(2)}, u32[]{:S(2)}) %collective-permute-start) | collective-permute-done | bytes 77856 | tf_op jit(solution)/shard_map/ppermute | solution.py:397
  10.3 1.2 broadcast_select_fusion
  11.5 7.0 %all-to-all-start = ((bf16[16,304,128]{2,1,0:T(8,128)(2,1)}), bf16[16,304,128]{2,1,0:T(8,128)(2,1)S(1)}, u32[]{:S(2)}, u32[]{:S(2)}) async-start(bf16[16,304,128]{2,1,0:T(8,128)(2,1)} %broadcast_select_fusion), calls=%async_computation | async-start | bytes 2490368 | tf_op jit(solution)/shard_map/all_to_all | solution.py:401
  18.5 0.0 copy-start.3
  18.5 2.9 %collective-permute-start.3 = (bf16[304,128]{1,0:T(8,128)(2,1)S(1)}, bf16[304,128]{1,0:T(8,128)(2,1)S(1)}, u32[]{:S(2)}, u32[]{:S(2)}) collective-permute-start(bf16[304,128]{1,0:T(8,128)(2,1)S(1)} %get-tuple-element.13), channel_id=1, source_target_pairs={{0,32},{2,34},{4,36},{6,38},{8,40},{10,42},{12,44},{14,46},{16,48}... | collective-permute-start | bytes 233480 | tf_op jit(solution)/shard_map/ppermute | solution.py:397
  21.5 2.0 %collective-permute-done.3 = bf16[304,128]{1,0:T(8,128)(2,1)S(1)} collective-permute-done((bf16[304,128]{1,0:T(8,128)(2,1)S(1)}, bf16[304,128]{1,0:T(8,128)(2,1)S(1)}, u32[]{:S(2)}, u32[]{:S(2)}) %collective-permute-start.3) | collective-permute-done | bytes 77856 | tf_op jit(solution)/shard_map/ppermute | solution.py:397
  23.5 14.0 %all-to-all-done.refs_1_ = bf16[16,304,128]{2,1,0:T(8,128)(2,1)S(1)} async-done(((bf16[16,304,128]{2,1,0:T(8,128)(2,1)}), bf16[16,304,128]{2,1,0:T(8,128)(2,1)S(1)}, u32[]{:S(2)}, u32[]{:S(2)}) %all-to-all-start) | async-done | bytes 1245216 | tf_op jit(solution)/shard_map/all_to_all | solution.py:401
  37.5 0.0 copy-start.8
  37.5 1.3 broadcast_in_dim.51
  38.8 4.4 %all-to-all-start.1 = ((bf16[16,304,128]{2,1,0:T(8,128)(2,1)}), bf16[16,304,128]{2,1,0:T(8,128)(2,1)}, u32[]{:S(2)}, u32[]{:S(2)}) async-start(bf16[16,304,128]{2,1,0:T(8,128)(2,1)} %broadcast_in_dim.51), calls=%async_computation.1 | async-start | bytes 2490368 | tf_op jit(solution)/shard_map/all_to_all | solution.py:404
  43.2 0.1 collective-permute-start.1
  43.3 0.0 copy-done.3
  43.3 0.0 copy-done.8
  43.3 2.3 %collective-permute-done.1.oth_ref.refs_4_.refs_3_ = bf16[256,1664]{1,0:T(8,128)(2,1)S(1)} collective-permute-done((bf16[256,1664]{1,0:T(8,128)(2,1)S(1)}, bf16[256,1664]{1,0:T(8,128)(2,1)S(1)}, u32[]{:S(2)}, u32[]{:S(2)}) %collective-permute-start.1) | collective-permute-done | bytes 852000 | tf_op jit(solution)/shard_map/ppermute | solution.py:398
  45.6 0.3 spread.1.refs_2_.refs_1_
  45.9 0.1 broadcast_in_dim.50.refs_5_.refs_4_
  46.0 9.4 %attend_late.1 = (f32[128,896]{1,0:T(8,128)}, f32[128,896]{1,0:T(8,128)}) custom-call(bf16[304,128]{1,0:T(8,128)(2,1)S(1)} %collective-permute-done.refs_0_, bf16[16,304,128]{2,1,0:T(8,128)(2,1)} %copy-done.8, bf16[12,256,256]{2,1,0:T(8,128)(2,1)S(1)} %spread.1.refs_2_.refs_1_, bf16[256,1664]{1,0:T(8,128)(2,1)S(1)} %get-tuple-element.14.own_ref.refs_3_.refs_2_, ...), custom_call_target="tpu_custom_call" | custom-call | tf_op jit(solution)/shard_map/attend_late/pallas_call | solution.py:419
  55.5 0.0 copy-start.4
  55.5 0.0 copy-start.5
  55.5 0.0 copy-start.6
  55.5 0.4 collective-permute-start.2
  55.9 5.0 %all-to-all-done.1.refs_0_ = bf16[16,304,128]{2,1,0:T(8,128)(2,1)} async-done(((bf16[16,304,128]{2,1,0:T(8,128)(2,1)}), bf16[16,304,128]{2,1,0:T(8,128)(2,1)}, u32[]{:S(2)}, u32[]{:S(2)}) %all-to-all-start.1) | async-done | bytes 1245216 | tf_op jit(solution)/shard_map/all_to_all | solution.py:404
  60.9 0.0 copy-start
  60.9 0.0 copy-start.1
  60.9 0.0 copy-start.2
  60.9 3.0 %attend_early.1 = (f32[128,896]{1,0:T(8,128)S(1)}, f32[128,896]{1,0:T(8,128)S(1)}) custom-call(bf16[16,304,128]{2,1,0:T(8,128)(2,1)} %all-to-all-done.1.refs_0_, bf16[12,256,256]{2,1,0:T(8,128)(2,1)S(1)} %spread.1.refs_2_.refs_1_, bf16[256,1664]{1,0:T(8,128)(2,1)S(1)} %get-tuple-element.14.own_ref.refs_3_.refs_2_, ...), custom_call_target="tpu_custom_call" | custom-call | tf_op jit(solution)/shard_map/attend_early/pallas_call | solution.py:419
  64.0 0.1 collective-permute-start.4
  64.1 0.5 collective-permute-start.5
  64.6 0.1 collective-permute-start.6
  64.7 0.4 collective-permute-start.7
  65.1 0.0 collective-permute-done.2.refs_1_
  65.1 0.8 collective-permute-done.4.refs_3_
  65.9 0.0 copy-done.4
  65.9 0.0 copy-done.5
  65.9 0.0 copy-done.6
  65.9 0.0 copy-done
  65.9 0.0 copy-done.1
  65.9 0.0 copy-done.2
  65.9 6.3 %mix.1 = (bf16[128,2048]{1,0:T(8,128)(2,1)S(1)}, bf16[512,2048]{1,0:T(8,128)(2,1)}) custom-call(f32[128,896]{1,0:T(8,128)S(1)} %copy-done.2, f32[128,896]{1,0:T(8,128)} %collective-permute-done.2.refs_1_, f32[128,896]{1,0:T(8,128)S(1)} %get-tuple-element.17.refs_2_, f32[128,896]{1,0:T(8,128)S(1)} %collective-permute-done.4.refs_3_, ...), custom_call_target="tpu_custom_call" | custom-call | tf_op jit(solution)/shard_map/mix/pallas_call | solution.py:440
  72.2 24.2 %all-to-all-start.2 = ((bf16[64,8,2048]{2,1,0:T(8,128)(2,1)}), bf16[64,8,2048]{2,1,0:T(8,128)(2,1)S(1)}, u32[]{:S(2)}, u32[]{:S(2)}) async-start(bf16[64,8,2048]{2,1,0:T(8,128)(2,1)} %bitcast.23), calls=%async_computation.2 | async-start | bytes 4194304 | tf_op jit(solution)/shard_map/all_to_all | solution.py:448
  96.4 0.0 collective-permute-done.5.refs_3_
  96.4 0.0 collective-permute-done.6.refs_4_
  96.4 0.0 collective-permute-done.7.refs_5_
  96.4 30.1 %all-to-all-done.2 = bf16[64,8,2048]{2,1,0:T(8,128)(2,1)S(1)} async-done(((bf16[64,8,2048]{2,1,0:T(8,128)(2,1)}), bf16[64,8,2048]{2,1,0:T(8,128)(2,1)S(1)}, u32[]{:S(2)}, u32[]{:S(2)}) %all-to-all-start.2) | async-done | bytes 2097184 | tf_op jit(solution)/shard_map/all_to_all | solution.py:448
  126.5 9.3 %experts.1 = bf16[512,2048]{1,0:T(8,128)(2,1)S(1)} custom-call(bf16[512,2048]{1,0:T(8,128)(2,1)S(1)} %bitcast.15, bf16[2048,512]{1,0:T(8,128)(2,1)} %bitcast.25, bf16[2048,512]{1,0:T(8,128)(2,1)} %bitcast.27, bf16[512,2048]{1,0:T(8,128)(2,1)} %bitcast.29, bf16[2048,512]{1,0:T(8,128)(2,1)} %collective-permute-done.5.refs_3_, ...), custom_call_target="tpu_custom_call" | custom-call | tf_op jit(solution)/shard_map/experts/pallas_call | solution.py:451
  135.8 0.0 copy-start.7
  135.8 35.4 %all_to_all.20 = bf16[64,8,2048]{2,1,0:T(8,128)(2,1)S(1)} all-to-all(bf16[64,8,2048]{2,1,0:T(8,128)(2,1)S(1)} %bitcast.16), channel_id=1, replica_groups=mesh['sp'=64,'tp'=2] {'sp'}, dimensions={0} | all-to-all | bytes 4194304 | tf_op jit(solution)/shard_map/all_to_all | solution.py:461
  171.2 0.0 copy-done.7
  171.2 1.7 pick.1
  (4 shorter events, 0.0 us)
Async XLA Ops:
  2.4 7.9 %collective-permute-start = (bf16[304,128]{1,0:T(8,128)(2,1)S(1)}, bf16[304,128]{1,0:T(8,128)(2,1)S(1)}, u32[]{:S(2)}, u32[]{:S(2)}) collective-permute-start(bf16[304,128]{1,0:T(8,128)(2,1)S(1)} %get-tuple-element.13), channel_id=1, source_target_pairs={{0,64},{2,66},{4,68},{6,70},{8,72},{10,74},{12,76},{14,78},{16,80}... | collective-permute-start | bytes 233480 | tf_op jit(solution)/shard_map/ppermute | solution.py:397
  11.5 26.0 %all-to-all-start = ((bf16[16,304,128]{2,1,0:T(8,128)(2,1)}), bf16[16,304,128]{2,1,0:T(8,128)(2,1)S(1)}, u32[]{:S(2)}, u32[]{:S(2)}) async-start(bf16[16,304,128]{2,1,0:T(8,128)(2,1)} %broadcast_select_fusion), calls=%async_computation | async-start | bytes 2490368 | tf_op jit(solution)/shard_map/all_to_all | solution.py:401
  18.5 24.8 %copy-start.3 = (s32[256]{0:T(256)S(1)}, s32[256]{0:T(256)}, u32[]{:S(2)}) copy-start(s32[256]{0:T(256)} %refs_5_.4) | copy-start | bytes 3076
  18.5 4.9 %collective-permute-start.3 = (bf16[304,128]{1,0:T(8,128)(2,1)S(1)}, bf16[304,128]{1,0:T(8,128)(2,1)S(1)}, u32[]{:S(2)}, u32[]{:S(2)}) collective-permute-start(bf16[304,128]{1,0:T(8,128)(2,1)S(1)} %get-tuple-element.13), channel_id=1, source_target_pairs={{0,32},{2,34},{4,36},{6,38},{8,40},{10,42},{12,44},{14,46},{16,48}... | collective-permute-start | bytes 233480 | tf_op jit(solution)/shard_map/ppermute | solution.py:397
  37.5 5.8 %copy-start.8 = (bf16[16,304,128]{2,1,0:T(8,128)(2,1)}, bf16[16,304,128]{2,1,0:T(8,128)(2,1)S(1)}, u32[]{:S(2)}) copy-start(bf16[16,304,128]{2,1,0:T(8,128)(2,1)S(1)} %all-to-all-done.refs_1_) | copy-start | bytes 3735556
  38.8 22.2 %all-to-all-start.1 = ((bf16[16,304,128]{2,1,0:T(8,128)(2,1)}), bf16[16,304,128]{2,1,0:T(8,128)(2,1)}, u32[]{:S(2)}, u32[]{:S(2)}) async-start(bf16[16,304,128]{2,1,0:T(8,128)(2,1)} %broadcast_in_dim.51), calls=%async_computation.1 | async-start | bytes 2490368 | tf_op jit(solution)/shard_map/all_to_all | solution.py:404
  43.2 2.5 %collective-permute-start.1 = (bf16[256,1664]{1,0:T(8,128)(2,1)S(1)}, bf16[256,1664]{1,0:T(8,128)(2,1)S(1)}, u32[]{:S(2)}, u32[]{:S(2)}) collective-permute-start(bf16[256,1664]{1,0:T(8,128)(2,1)S(1)} %get-tuple-element.14.own_ref.refs_3_.refs_2_), channel_id=1, source_target_pairs={{0,1},{1,0},{2,3},{3,2},{4,5},{5,4},{6,7},{7,6},{8,9},{9,8},{10,11... | collective-permute-start | bytes 2555912 | tf_op jit(solution)/shard_map/ppermute | solution.py:398
  55.5 10.4 %copy-start.4 = (f32[2048]{0:T(1024)S(1)}, f32[2048]{0:T(1024)}, u32[]{:S(2)}) copy-start(f32[2048]{0:T(1024)} %param.23) | copy-start | bytes 24580
  55.5 10.4 %copy-start.5 = (f32[2048]{0:T(1024)S(1)}, f32[2048]{0:T(1024)}, u32[]{:S(2)}) copy-start(f32[2048]{0:T(1024)} %param.24) | copy-start | bytes 24580
  55.5 10.4 %copy-start.6 = (s32[128,2]{0,1:T(2,128)S(1)}, s32[128,2]{0,1:T(2,128)}, u32[]{:S(2)}) copy-start(s32[128,2]{0,1:T(2,128)} %param.25) | copy-start | bytes 3076
  55.5 9.6 %collective-permute-start.2 = (f32[128,896]{1,0:T(8,128)}, f32[128,896]{1,0:T(8,128)}, u32[]{:S(2)}, u32[]{:S(2)}) collective-permute-start(f32[128,896]{1,0:T(8,128)} %get-tuple-element.16), channel_id=1, source_target_pairs={{0,1},{1,0},{2,3},{3,2},{4,5},{5,4},{6,7},{7,6},{8,9},{9,8},{10,11... | collective-permute-start | bytes 1376264 | tf_op jit(solution)/shard_map/ppermute | solution.py:437
  60.9 5.0 %copy-start = (bf16[768,2048]{1,0:T(8,128)(2,1)S(1)}, bf16[768,2048]{1,0:T(8,128)(2,1)}, u32[]{:S(2)}) copy-start(bf16[768,2048]{1,0:T(8,128)(2,1)} %refs_4_.3) | copy-start | bytes 9437188
  60.9 5.0 %copy-start.1 = (bf16[128,2048]{1,0:T(8,128)(2,1)S(1)}, bf16[128,2048]{1,0:T(8,128)(2,1)}, u32[]{:S(2)}) copy-start(bf16[128,2048]{1,0:T(8,128)(2,1)} %refs_5_.5) | copy-start | bytes 1572868
  60.9 5.0 %copy-start.2 = (f32[128,896]{1,0:T(8,128)S(1)}, f32[128,896]{1,0:T(8,128)}, u32[]{:S(2)}) copy-start(f32[128,896]{1,0:T(8,128)} %get-tuple-element.15.refs_0_) | copy-start | bytes 1376260
  64.0 1.9 %collective-permute-start.4 = (f32[128,896]{1,0:T(8,128)S(1)}, f32[128,896]{1,0:T(8,128)S(1)}, u32[]{:S(2)}, u32[]{:S(2)}) collective-permute-start(f32[128,896]{1,0:T(8,128)S(1)} %get-tuple-element.18), channel_id=1, source_target_pairs={{0,1},{1,0},{2,3},{3,2},{4,5},{5,4},{6,7},{7,6},{8,9},{9,8},{10,11... | collective-permute-start | bytes 1376264 | tf_op jit(solution)/shard_map/ppermute | solution.py:437
  64.1 32.3 %collective-permute-start.5 = (bf16[2048,512]{1,0:T(8,128)(2,1)}, bf16[2048,512]{1,0:T(8,128)(2,1)}, u32[]{:S(2)}, u32[]{:S(2)}) collective-permute-start(bf16[2048,512]{1,0:T(8,128)(2,1)} %bitcast.24), channel_id=1, source_target_pairs={{0,1},{1,0},{2,3},{3,2},{4,5},{5,4},{6,7},{7,6},{8,9},{9,8},{10,11... | collective-permute-start | bytes 6291464 | tf_op jit(solution)/shard_map/ppermute | solution.py:450
  64.6 31.8 %collective-permute-start.6 = (bf16[2048,512]{1,0:T(8,128)(2,1)}, bf16[2048,512]{1,0:T(8,128)(2,1)}, u32[]{:S(2)}, u32[]{:S(2)}) collective-permute-start(bf16[2048,512]{1,0:T(8,128)(2,1)} %bitcast.26), channel_id=1, source_target_pairs={{0,1},{1,0},{2,3},{3,2},{4,5},{5,4},{6,7},{7,6},{8,9},{9,8},{10,11... | collective-permute-start | bytes 6291464 | tf_op jit(solution)/shard_map/ppermute | solution.py:450
  64.7 31.7 %collective-permute-start.7 = (bf16[512,2048]{1,0:T(8,128)(2,1)}, bf16[512,2048]{1,0:T(8,128)(2,1)}, u32[]{:S(2)}, u32[]{:S(2)}) collective-permute-start(bf16[512,2048]{1,0:T(8,128)(2,1)} %bitcast.28), channel_id=1, source_target_pairs={{0,1},{1,0},{2,3},{3,2},{4,5},{5,4},{6,7},{7,6},{8,9},{9,8},{10,11... | collective-permute-start | bytes 6291464 | tf_op jit(solution)/shard_map/ppermute | solution.py:450
  72.2 54.3 %all-to-all-start.2 = ((bf16[64,8,2048]{2,1,0:T(8,128)(2,1)}), bf16[64,8,2048]{2,1,0:T(8,128)(2,1)S(1)}, u32[]{:S(2)}, u32[]{:S(2)}) async-start(bf16[64,8,2048]{2,1,0:T(8,128)(2,1)} %bitcast.23), calls=%async_computation.2 | async-start | bytes 4194304 | tf_op jit(solution)/shard_map/all_to_all | solution.py:448
  135.8 35.4 %copy-start.7 = (f32[128,2]{0,1:T(2,128)S(1)}, f32[128,2]{0,1:T(2,128)}, u32[]{:S(2)}) copy-start(f32[128,2]{0,1:T(2,128)} %param.26) | copy-start | bytes 3076

commit v3 on v2

v3 whole, which is shorter than its diff:
```python
import functools
import math

import jax
import jax.numpy as jnp
from jax import lax
from jax.experimental import pallas as pl
from jax.experimental.pallas import tpu as pltpu
from jax.sharding import PartitionSpec as P


D = 2048
NOPE = 64
ROPE = 32
HALF = 128
BLOCK = 256
HEADS = 12
LOCAL_HEADS = 6
PLANE = 16
ROWS = 304
CAPACITY = 8
EXPERTS = 64
CHUNKS = 1
PIECES = 4
AHEAD = 3
DEPTH = CAPACITY // CHUNKS
PART = EXPERTS * DEPTH
SPAN = NOPE + ROPE
QW = LOCAL_HEADS * SPAN
PACK = QW + 4 * BLOCK
STATS = HEADS * NOPE
ROWS_OUT = STATS + 32
epsilon = 1e-06
ATTEND_MIB = 24
LOW = -1e30
SCALE = (NOPE + ROPE) ** -0.5 * math.log2(math.e)
f32 = jnp.float32
bf16 = jnp.bfloat16


def vmem():
    return pl.BlockSpec(memory_space=pltpu.VMEM)


def smem():
    return pl.BlockSpec(memory_space=pltpu.SMEM)


def hbm():
    return pl.BlockSpec(memory_space=pltpu.HBM)


def far(x):
    return pltpu.with_memory_space_constraint(x, pltpu.HBM)


def params(mib):
    return pltpu.CompilerParams(vmem_limit_bytes=mib * 1024 * 1024)


def lanes(rows):
    return lax.broadcasted_iota(jnp.int32, (rows, 128), 1)


def turn(first, second, cosine, sine):
    return first * cosine - second * sine, second * cosine + first * sine


def prep_kernel(*refs):
    inputs, (pay_ref, pack_ref) = refs[:8], refs[8:10]
    held, sems = refs[10:18], refs[18]
    copies = [pltpu.make_async_copy(src, dst, sems.at[i]) for i, (src, dst) in enumerate(zip(inputs, held))]
    for copy in copies:
        copy.start()
    for copy in copies:
        copy.wait()
    q_ref, lat_ref, rope_ref, doc_ref, wk_ref, wv_ref, cos_ref, sin_ref = held
    half = lax.axis_index("tp")
    cosine, sine = cos_ref[...], sin_ref[...]
    mine = pl.ds(pl.multiple_of(half * HALF, HALF), HALF)
    pay_ref[0:128, :] = lat_ref[mine, 0:128]
    pay_ref[128:256, :] = lat_ref[mine, 128:256]
    rope = rope_ref[...].astype(f32)
    turned = jnp.concatenate(turn(rope[:16], rope[16:], cosine, sine), axis=0)
    turned = jnp.where(half == 0, turned[:, :128], turned[:, 128:])
    turned = jnp.concatenate([turned, jnp.zeros((96, 128), f32)], axis=0).T
    packed = turned[0:32, :]
    for c in range(1, 4):
        packed = packed + pltpu.roll(turned[32 * c : 32 * c + 32, :], 32 * c, 1)
    pay_ref[256:288, :] = packed.astype(bf16)
    docs = doc_ref[pl.ds(half, 1), :].astype(f32)
    pay_ref[288:304, :] = jnp.broadcast_to(docs, (16, 128)).astype(bf16)
    lane = lanes(BLOCK)
    for head in range(LOCAL_HEADS):
        start = head * SPAN
        pack_ref[start : start + NOPE, :] = q_ref[start : start + NOPE, :]
        rot = q_ref[start + NOPE : start + SPAN, :].astype(f32)
        rot = jnp.concatenate(turn(rot[:16], rot[16:], cosine, sine), axis=0)
        pack_ref[start + NOPE : start + SPAN, :] = rot.astype(bf16)
    w1 = wk_ref[:, 128:256].astype(f32)
    w2 = wk_ref[:, 256:384].astype(f32)
    r1, r2 = pltpu.roll(w1, 64, 1), pltpu.roll(w2, 64, 1)
    first, second = slice(QW, QW + BLOCK), slice(QW + BLOCK, QW + 2 * BLOCK)
    pack_ref[first, 0:128] = wk_ref[:, 0:128]
    pack_ref[first, 128:256] = jnp.where(lane < 64, w1, 0.0).astype(bf16)
    pack_ref[second, 0:128] = jnp.where(lane < 64, r1, r2).astype(bf16)
    pack_ref[second, 128:256] = jnp.where(lane < 64, r2, 0.0).astype(bf16)
    pack_ref[QW + 2 * BLOCK : QW + 3 * BLOCK, :] = wv_ref[:, 0:256]
    pack_ref[QW + 3 * BLOCK : PACK, 0:128] = wv_ref[:, 256:384]
    pack_ref[QW + 3 * BLOCK : PACK, 128:256] = jnp.zeros((BLOCK, 128), bf16)


def spread_kernel(own_ref, oth_ref, q_ref, v_ref):
    for side, src in enumerate((own_ref, oth_ref)):
        for local in range(LOCAL_HEADS):
            head, at, start = side * LOCAL_HEADS + local, local % 3 * NOPE, local * SPAN
            q_ref[head] = jnp.zeros((256, BLOCK), bf16)
            q_ref[head, at : at + NOPE, :] = src[start : start + NOPE, :]
            q_ref[head, 192 : 192 + ROPE, :] = src[start + NOPE : start + SPAN, :]
        base = QW + 2 * BLOCK
        for panel in range(3):
            rows, cols = base + panel // 2 * BLOCK, panel % 2 * 128
            piece = src[rows : rows + BLOCK, cols : cols + 128].astype(f32).T
            v_ref[side * 384 + panel * 128 : side * 384 + panel * 128 + 128, :] = piece.astype(bf16)


def attend_kernel(late, *refs):
    if late:
        ext_ref, refs = refs[0], refs[1:]
    src_ref, wv_src, q_ref, own_ref, oth_ref, qdoc_ref, doc_ref, mine_ref, theirs_ref = refs[:9]
    k_s, v_s, m_s, l_s, a_s, bias_s, arr_ref, wv_ref, sems = refs[9:]
    fetch = pltpu.make_async_copy(src_ref, arr_ref, sems.at[0])
    fetch.start()
    fetch_wv = pltpu.make_async_copy(wv_src, wv_ref, sems.at[1])
    fetch_wv.start()
    half = lax.axis_index("tp")
    seat = lax.axis_index("sp")
    plane, spot = seat // PLANE, seat % PLANE
    doc_first = doc_ref[0].astype(f32)
    doc_last = doc_ref[BLOCK - 1].astype(f32)
    m_s[...] = jnp.full(m_s.shape, LOW, f32)
    l_s[...] = jnp.zeros(l_s.shape, f32)
    a_s[...] = jnp.zeros(a_s.shape, f32)
    fetch.wait()
    fetch_wv.wait()

    def block_of(i):
        if not late:
            return (plane - 1) * PLANE + i
        return (plane - jnp.where(i <= spot, 0, 2)) * PLANE + i

    def place(block):
        return jnp.where(block >= 0, block * BLOCK + half * HALF, -1)

    groups = [[(arr_ref, 8 * t + b, block_of(8 * t + b)) for b in range(8)] for t in range(2)]
    if late:
        groups.append([(ext_ref, None, (plane - 2) * PLANE + spot)])
    row_lane = lax.broadcasted_iota(jnp.int32, (1, 128), 1)
    code = jnp.zeros((1, 128), f32)
    for t, group in enumerate(groups):
        high = low = None
        for ref, i, block in group:
            docs = (ref[288:304, :] if i is None else ref[i, 288:304, :]).astype(f32)[0:1, :]
            seen = jnp.where(block >= 0, docs, -1.0)
            bound = jnp.where(block == seat, -1.0, seen)
            high = seen if high is None else jnp.maximum(high, seen)
            low = bound if low is None else jnp.minimum(low, bound)
        code = code + jnp.where((row_lane == 127) & (high >= doc_first), float(2 ** (2 * t)), 0.0)
        code = code + jnp.where((row_lane == 0) & (low == doc_last), float(2 ** (2 * t + 1)), 0.0)
    code = jnp.sum(code).astype(jnp.int32)

    def heads(count, masked):
        def side(number, carried):
            first = number * LOCAL_HEADS

            def score(head):
                return jnp.dot(k_s[2 * number + head // 3, :count, :], q_ref[first + head], preferred_element_type=f32)

            following = score(0)
            for head in range(LOCAL_HEADS):
                s = following
                if head + 1 < LOCAL_HEADS:
                    following = score(head + 1)
                at = first + head
                if masked:
                    s = s + bias_s[:count, :]
                old = m_s[at]
                new = jnp.maximum(old, jnp.max(s, axis=0, keepdims=True))
                keep = jnp.exp2((old - new) * SCALE)
                m_s[at] = new
                weights = jnp.exp2((s - new) * SCALE)
                l_s[at] = l_s[at] * keep + jnp.sum(weights, axis=0, keepdims=True)
                rows = pl.ds(pl.multiple_of(at * NOPE, NOPE), NOPE)
                a_s[at] = a_s[at] * keep + jnp.dot(v_s[rows, :count], weights.astype(bf16), preferred_element_type=f32)
            return carried

        lax.fori_loop(0, 2, side, 0)

    def tile(load, blocks, flags):
        panels = len(blocks)
        count = panels * 128
        active = (flags & 1) == 1
        plain = (flags & 2) == 2

        @pl.when(active)
        def _():
            lat = jnp.concatenate(
                [
                    jnp.concatenate([load(b, 0, 128) for b in range(panels)], axis=0),
                    jnp.concatenate([load(b, 128, 256) for b in range(panels)], axis=0),
                ],
                axis=1,
            )
            turned = []
            for b in range(panels):
                r = load(b, 256, 288).astype(f32)
                turned += [pltpu.roll(r, 64, 1), pltpu.roll(r, 32, 1), r, pltpu.roll(r, 96, 1)]
            turned = jnp.concatenate(turned, axis=0)
            wide = lanes(count)
            turned = jnp.where((wide >= 64) & (wide < 96), turned, 0.0)
            for side, src in enumerate((own_ref, oth_ref)):
                for g in range(2):
                    rows = QW + g * BLOCK
                    keys = jnp.dot(lat, src[rows : rows + BLOCK, :], preferred_element_type=f32)
                    k_s[side * 2 + g, :count, 0:128] = keys[:, 0:128].astype(bf16)
                    k_s[side * 2 + g, :count, 128:256] = (keys[:, 128:256] + turned).astype(bf16)
            v_s[:, :count] = lax.dot_general(
                wv_ref[...], lat, (((1,), (1,)), ((), ())), preferred_element_type=f32
            ).astype(bf16)

        if panels > 1:

            @pl.when(active & plain)
            def _():
                heads(count, False)

        @pl.when(active & jnp.logical_not(plain) if panels > 1 else active)
        def _():
            at_query = seat * BLOCK + lax.broadcasted_iota(jnp.int32, (128, BLOCK), 1)
            row = lax.broadcasted_iota(jnp.int32, (128, BLOCK), 0)
            for b in range(panels):
                base = place(blocks[b])
                at_key = jnp.where(base >= 0, base, 1 << 20) + row
                docs = jnp.broadcast_to(load(b, 288, 304).astype(f32)[0:1, :], (128, 128)).T
                same = jnp.concatenate([docs, docs], axis=1) == qdoc_ref[...]
                bias_s[128 * b : 128 * b + 128, :] = jnp.where((at_key <= at_query) & same, 0.0, LOW)
            heads(count, True)

    if late:
        tile(lambda b, lo, hi: ext_ref[lo:hi, :], [groups[2][0][2]], code >> 4)

    def step(number, carried):
        blocks = [block_of(number * 8 + b) for b in range(8)]
        tile(lambda b, lo, hi: arr_ref[number * 8 + b, lo:hi, :], blocks, code >> (2 * number))
        return carried

    lax.fori_loop(0, 2, step, 0)

    def sides(x):
        left, right = x[:, 0:128], x[:, 128:256]
        return jnp.where(half == 0, left, right), jnp.where(half == 0, right, left)

    for head in range(HEADS):
        at = head + jnp.where(half == 0, 0, LOCAL_HEADS if head < LOCAL_HEADS else -LOCAL_HEADS)
        rows = pl.ds(pl.multiple_of(at * NOPE, NOPE), NOPE)
        mine_ref[rows, :], theirs_ref[rows, :] = sides(a_s[head])
        for base, ref in ((STATS, m_s), (STATS + 16, l_s)):
            mine_ref[pl.ds(base + at, 1), :], theirs_ref[pl.ds(base + at, 1), :] = sides(ref[head])


def slots_of(ids):
    expert = lax.broadcasted_iota(jnp.int32, (EXPERTS, HALF), 0)
    named = [(ids[k : k + 1, :] == expert) for k in range(2)]
    counts = named[0].astype(f32) + named[1].astype(f32)
    row = lax.broadcasted_iota(jnp.int32, (HALF, HALF), 0)
    col = lax.broadcasted_iota(jnp.int32, (HALF, HALF), 1)
    earlier = jnp.dot(counts.astype(bf16), (row < col).astype(f32).astype(bf16), preferred_element_type=f32)
    slot = lax.broadcasted_iota(jnp.int32, (PART, HALF), 0)
    picks = []
    for k in range(2):
        rank = jnp.sum(jnp.where(named[k], earlier, 0.0), axis=0, keepdims=True).astype(jnp.int32)
        base = ids[k : k + 1, :] * DEPTH + rank
        chunks = []
        for c in range(CHUNKS):
            here = (rank >= DEPTH * c) & (rank < DEPTH * (c + 1))
            at = jnp.where(here, base - DEPTH * c, -1)
            chunks.append((slot == at).astype(f32).astype(bf16))
        picks.append(chunks)
    return picks


def norm_of(x):
    return lax.rsqrt(jnp.mean(x * x, axis=-1, keepdims=True) + epsilon)


def mix_kernel(*refs):
    parts, (proj_ref, res_ref, mixg_ref, moeg_ref, ids_ref, mid_ref), rest = refs[:4], refs[4:10], refs[10:]
    buf_refs, held, sems = rest[:CHUNKS], rest[CHUNKS], rest[CHUNKS + 1]
    tops = [part[STATS : STATS + HEADS, :] for part in parts]
    top = jnp.maximum(jnp.maximum(tops[0], tops[1]), jnp.maximum(tops[2], tops[3]))
    shares = [jnp.exp2((s - top) * SCALE) for s in tops]
    total = 0.0
    for part, share in zip(parts, shares):
        total = total + share * part[STATS + 16 : STATS + 16 + HEADS, :]
    pieces = []
    for head in range(HEADS):
        rows = slice(head * NOPE, head * NOPE + NOPE)
        value = 0.0
        for part, share in zip(parts, shares):
            value = value + part[rows, :] * share[head : head + 1, :]
        pieces.append((value / total[head : head + 1, :]).astype(bf16))
    attended = jnp.concatenate(pieces, axis=0)
    mix = lax.dot_general(attended, proj_ref[...], (((0,), (0,)), ((), ())), preferred_element_type=f32)
    branch = mix * norm_of(mix) * mixg_ref[...]
    middle = (res_ref[...].astype(f32) + branch).astype(bf16)
    mid_ref[...] = middle
    wide = middle.astype(f32)
    normed = (wide * norm_of(wide) * moeg_ref[...]).astype(bf16)
    picks = slots_of(ids_ref[...])
    copies = []
    for c in range(CHUNKS):
        chosen = picks[0][c] + picks[1][c]
        for r in range(PIECES):
            rows = slice(r * PART // PIECES, (r + 1) * PART // PIECES)
            held[c, rows, :] = jnp.dot(chosen[rows], normed, preferred_element_type=f32).astype(bf16)
            copies.append(pltpu.make_async_copy(held.at[c, rows], buf_refs[c].at[rows], sems.at[c * PIECES + r]))
            copies[-1].start()
    for copy in copies:
        copy.wait()


def expert_kernel(rows_ref, *refs):
    weights, out_ref, held, first_s, sems = refs[:6], refs[6], refs[7:13], refs[13], refs[14]
    copies = [pltpu.make_async_copy(src, dst, sems.at[i]) for i, (src, dst) in enumerate(zip(weights, held))]
    for copy in copies[:AHEAD]:
        copy.start()
    rows = rows_ref[...]

    def ready(i):
        copies[i].wait()
        if i + AHEAD < len(copies):
            copies[i + AHEAD].start()
        return held[i][...]

    for side in range(2):
        gated = jnp.dot(rows, ready(3 * side), preferred_element_type=f32)
        upward = jnp.dot(rows, ready(3 * side + 1), preferred_element_type=f32)
        hidden = (gated / (1.0 + jnp.exp(-gated)) * upward).astype(bf16)
        part = jnp.dot(hidden, ready(3 * side + 2), preferred_element_type=f32).astype(bf16)
        if side == 0:
            first_s[...] = part
        else:
            out_ref[...] = (first_s[...].astype(f32) + part.astype(f32)).astype(bf16)


def pick_kernel(*refs):
    back_refs, (mid_ref, ids_ref, weight_ref, out_ref) = refs[:CHUNKS], refs[CHUNKS:]
    picks = slots_of(ids_ref[...])
    total = mid_ref[...].astype(f32)
    for k in range(2):
        rows = 0.0
        for c in range(CHUNKS):
            rows = rows + lax.dot_general(
                picks[k][c], back_refs[c][...], (((0,), (0,)), ((), ())), preferred_element_type=f32
            )
        column = jnp.broadcast_to(weight_ref[k : k + 1, :], (HALF, HALF)).T
        total = total + rows * column[:, 0:1]
    out_ref[...] = total.astype(bf16)


def local(
    residual,
    queries,
    latent,
    rope_key,
    doc_ids,
    latent_to_key,
    latent_to_value,
    out_proj,
    mix_gain,
    moe_gain,
    expert_ids,
    route_weight,
    gate_weight,
    up_weight,
    down_weight,
):
    sp = lax.axis_size("sp")
    seat = lax.axis_index("sp")
    spot = seat % PLANE
    swap = [(0, 1), (1, 0)]
    frequency = 10000.0 ** (-jnp.arange(16, dtype=f32) / 16)
    positions = seat * BLOCK + jnp.arange(BLOCK, dtype=jnp.int32)
    angles = positions.astype(f32)[None, :] * frequency[:, None]
    inputs = (queries.T, latent, rope_key.T, doc_ids.reshape(2, 128), latent_to_key, latent_to_value, jnp.cos(angles), jnp.sin(angles))
    payload, pack = pl.pallas_call(
        prep_kernel,
        out_shape=(jax.ShapeDtypeStruct((ROWS, 128), bf16), jax.ShapeDtypeStruct((PACK, BLOCK), bf16)),
        in_specs=[hbm()] * 8,
        out_specs=(vmem(), vmem()),
        scratch_shapes=[pltpu.VMEM(x.shape, x.dtype) for x in inputs] + [pltpu.SemaphoreType.DMA((8,))],
        compiler_params=params(8),
        name="prep",
    )(*map(far, inputs))
    before = []
    for k in (1, 2):
        before.append(lax.ppermute(payload, "sp", [(i, i + PLANE * k) for i in range(sp - PLANE * k)]))
    other = lax.ppermute(pack, "tp", swap)
    target = jnp.arange(PLANE, dtype=jnp.int32)[:, None, None]
    groups = [[z * PLANE + i for i in range(PLANE)] for z in range(sp // PLANE)]

    def plane(x):
        return lax.all_to_all(x, "sp", 0, 0, axis_index_groups=groups, tiled=True)

    late = plane(jnp.where(spot <= target, payload[None], before[1][None]))
    fanned = jnp.broadcast_to(before[0][None], (PLANE, ROWS, 128))
    early = plane(fanned)
    query_docs = doc_ids.astype(f32)[None, :]
    spread = pl.pallas_call(
        spread_kernel,
        out_shape=(jax.ShapeDtypeStruct((HEADS, 256, BLOCK), bf16), pltpu.HBM((STATS, 256), bf16)),
        in_specs=[vmem()] * 2,
        out_specs=(vmem(), vmem()),
        compiler_params=params(6),
        name="spread",
    )(pack, other)
    stat = jax.ShapeDtypeStruct((ROWS_OUT, HALF), f32)

    def attend(is_late, *operands):
        mine, theirs = pl.pallas_call(
            functools.partial(attend_kernel, is_late),
            out_shape=(pltpu.HBM((ROWS_OUT, HALF), f32),) * 2 if is_late else (stat, stat),
            in_specs=[vmem()] * (len(operands) - 1) + [hbm()] * 2 + [vmem()] * 4 + [smem()],
            out_specs=(vmem(), vmem()),
            scratch_shapes=[
                pltpu.VMEM((4, 1024, 256), bf16),
                pltpu.VMEM((STATS, 1024), bf16),
                pltpu.VMEM((HEADS, 1, BLOCK), f32),
                pltpu.VMEM((HEADS, 1, BLOCK), f32),
                pltpu.VMEM((HEADS, NOPE, BLOCK), f32),
                pltpu.VMEM((1024, BLOCK), f32),
                pltpu.VMEM((PLANE, ROWS, 128), bf16),
                pltpu.VMEM((STATS, 256), bf16),
                pltpu.SemaphoreType.DMA((2,)),
            ],
            compiler_params=pltpu.CompilerParams(vmem_limit_bytes=ATTEND_MIB * 1024 * 1024),
            name="attend_late" if is_late else "attend_early",
        )(*operands[:-1], far(operands[-1]), far(spread[1]), spread[0], pack, other, query_docs, doc_ids)
        return mine, lax.ppermute(theirs, "tp", swap)

    parts = attend(True, before[1], late) + attend(False, early)
    middle, *buffers = pl.pallas_call(
        mix_kernel,
        out_shape=(jax.ShapeDtypeStruct((HALF, D), bf16),) + (pltpu.HBM((PART, D), bf16),) * CHUNKS,
        in_specs=[vmem()] * 9,
        out_specs=(vmem(),) + (hbm(),) * CHUNKS,
        scratch_shapes=[pltpu.VMEM((CHUNKS, PART, D), bf16), pltpu.SemaphoreType.DMA((CHUNKS * PIECES,))],
        compiler_params=params(16),
        name="mix",
    )(*parts, out_proj, residual, mix_gain[None], moe_gain[None], expert_ids.T)
    own = (gate_weight[0], up_weight[0], down_weight[0])
    swapped = tuple(lax.ppermute(w, "tp", swap) for w in own)

    def cross(x):
        return lax.all_to_all(x.reshape(EXPERTS, DEPTH, D), "sp", 0, 0, tiled=True).reshape(PART, D)

    rows = [cross(buffers[c]) for c in range(CHUNKS)]
    back = []
    for c in range(CHUNKS):
        result = pl.pallas_call(
            expert_kernel,
            out_shape=pltpu.HBM((PART, D), bf16),
            in_specs=[vmem()] + [hbm()] * 6,
            out_specs=vmem(),
            scratch_shapes=[pltpu.VMEM(w.shape, bf16) for w in own * 2]
            + [pltpu.VMEM((PART, D), bf16), pltpu.SemaphoreType.DMA((6,))],
            compiler_params=params(28),
            name="experts",
        )(rows[c], *map(far, own + swapped))
        back.append(cross(result))
    return pl.pallas_call(
        pick_kernel,
        out_shape=jax.ShapeDtypeStruct((HALF, D), bf16),
        in_specs=[vmem()] * (CHUNKS + 3),
        out_specs=vmem(),
        compiler_params=params(10),
        name="pick",
    )(*back, middle, expert_ids.T, route_weight.T)


def solution(mesh):
    in_specs = (
        P(("sp", "tp"), None),
        P("sp", "tp"),
        P("sp", None),
        P("sp", None),
        P("sp"),
        P(None, "tp"),
        P(None, "tp"),
        P(),
        P(),
        P(),
        P(("sp", "tp"), None),
        P(("sp", "tp"), None),
        P("sp", None, "tp"),
        P("sp", None, "tp"),
        P("sp", "tp", None),
    )
    out_specs = P(("sp", "tp"), None)

    return jax.shard_map(local, mesh=mesh, in_specs=in_specs, out_specs=out_specs, check_vma=False)
```

time: 175 us -> 188 us (1.074)
  starting transfers between devices: 46 us -> 61.9 us
  waiting for transfers between devices: 56.3 us -> 52.6 us
  Pallas kernels: 31.6 us -> 33.7 us
    all_to_all x3, starting transfers between devices: 35.6 us -> 51.5 us  [the longest x1 40.1 us: cross(): lax.all_to_all(x.reshape(EXPERTS, DEPTH, D), 'sp', 0, 0, tiled=True)]
    all_to_all x3, waiting for transfers between devices: 49.1 us -> 45.6 us  [the longest x1 30.1 us: cross(): lax.all_to_all(x.reshape(EXPERTS, DEPTH, D), 'sp', 0, 0, tiled=True)]
    pallas_call x2, Pallas kernels: 12.5 us -> 14.9 us  [attend(): pl.pallas_call(functools.partial(attend_kernel, is_late), out_shape=(pltp...]
    pallas_call x1, Pallas kernels: 6.26 us -> 3.8 us  [local(): pl.pallas_call(mix_kernel, out_shape=(jax.ShapeDtypeStruct((HALF, D), bf1...]
    pallas_call x2, Pallas kernels: 9.63 us -> 11.7 us  [the longest x1 10.7 us: local(): pl.pallas_call(expert_kernel, out_shape=pltpu.HBM((PART, D), bf16), in_sp...]
where the time goes in v3:
time: 188 us; the launch traced here: 187 us
  starting transfers between devices  61.9 us (33%)
  waiting for transfers between devices  52.6 us (28%)
  blocking collectives  35.6 us (19%)
  Pallas kernels  33.7 us (18%)
  other arithmetic  1.99 us (1%)
    all_to_all x1, starting transfers between devices, cross(): lax.all_to_all(x.reshape(EXPERTS, DEPTH, D), 'sp', 0, 0, tiled=True)  40.1 us
    all_to_all x1, blocking collectives, cross(): lax.all_to_all(x.reshape(EXPERTS, DEPTH, D), 'sp', 0, 0, tiled=True)  35.6 us
    all_to_all x1, waiting for transfers between devices, cross(): lax.all_to_all(x.reshape(EXPERTS, DEPTH, D), 'sp', 0, 0, tiled=True)  30.1 us
    all_to_all x2, waiting for transfers between devices, plane(): return lax.all_to_all(x, 'sp', 0, 0, axis_index_groups=groups, tiled=True)  15.5 us
    pallas_call x2, Pallas kernels, attend(): pl.pallas_call(functools.partial(attend_kernel, is_late), out_shape=(pltp...  14.9 us
    all_to_all x2, starting transfers between devices, plane(): return lax.all_to_all(x, 'sp', 0, 0, axis_index_groups=groups, tiled=True)  11.4 us
    pallas_call x1, Pallas kernels, local(): pl.pallas_call(expert_kernel, out_shape=pltpu.HBM((PART, D), bf16), in_sp...  10.7 us
    ppermute x2, starting transfers between devices, local(): lax.ppermute(payload, 'sp', [(i, i + PLANE * k) for i in range(sp - PLANE...  8.83 us
  transfers between devices with their start and end apart: 11, of which 7 were waited for; matrix products, arithmetic and copies ran while one was open for 0% of the time, Pallas kernels for 11%

profile of v3, /device:TPU:0, one launch (start us, length us, event | category | flops | bytes accessed | tf_op | source)
XLA Modules:
  0.0 187.3 jit_solution(1709109359384340743)
XLA Ops:
  0.0 0.8 multiply_sine_fusion
  0.8 1.5 prep.1
  2.3 5.9 %collective-permute-start = (bf16[304,128]{1,0:T(8,128)(2,1)S(1)}, bf16[304,128]{1,0:T(8,128)(2,1)S(1)}, u32[]{:S(2)}, u32[]{:S(2)}) collective-permute-start(bf16[304,128]{1,0:T(8,128)(2,1)S(1)} %get-tuple-element.15), channel_id=1, source_target_pairs={{0,64},{2,66},{4,68},{6,70},{8,72},{10,74},{12,76},{14,78},{16,80}... | collective-permute-start | bytes 233480 | tf_op jit(solution)/shard_map/ppermute | solution.py:407
  8.3 2.0 %collective-permute-done.refs_0_ = bf16[304,128]{1,0:T(8,128)(2,1)S(1)} collective-permute-done((bf16[304,128]{1,0:T(8,128)(2,1)S(1)}, bf16[304,128]{1,0:T(8,128)(2,1)S(1)}, u32[]{:S(2)}, u32[]{:S(2)}) %collective-permute-start) | collective-permute-done | bytes 77856 | tf_op jit(solution)/shard_map/ppermute | solution.py:407
  10.2 1.2 broadcast_select_fusion
  11.4 7.0 %all-to-all-start = ((bf16[16,304,128]{2,1,0:T(8,128)(2,1)}), bf16[16,304,128]{2,1,0:T(8,128)(2,1)S(1)}, u32[]{:S(2)}, u32[]{:S(2)}) async-start(bf16[16,304,128]{2,1,0:T(8,128)(2,1)} %broadcast_select_fusion), calls=%async_computation | async-start | bytes 2490368 | tf_op jit(solution)/shard_map/all_to_all | solution.py:413
  18.5 0.0 copy-start.3
  18.5 2.9 %collective-permute-start.3 = (bf16[304,128]{1,0:T(8,128)(2,1)S(1)}, bf16[304,128]{1,0:T(8,128)(2,1)S(1)}, u32[]{:S(2)}, u32[]{:S(2)}) collective-permute-start(bf16[304,128]{1,0:T(8,128)(2,1)S(1)} %get-tuple-element.15), channel_id=1, source_target_pairs={{0,32},{2,34},{4,36},{6,38},{8,40},{10,42},{12,44},{14,46},{16,48}... | collective-permute-start | bytes 233480 | tf_op jit(solution)/shard_map/ppermute | solution.py:407
  21.4 2.0 %collective-permute-done.3 = bf16[304,128]{1,0:T(8,128)(2,1)S(1)} collective-permute-done((bf16[304,128]{1,0:T(8,128)(2,1)S(1)}, bf16[304,128]{1,0:T(8,128)(2,1)S(1)}, u32[]{:S(2)}, u32[]{:S(2)}) %collective-permute-start.3) | collective-permute-done | bytes 77856 | tf_op jit(solution)/shard_map/ppermute | solution.py:407
  23.4 14.0 %all-to-all-done.refs_1_ = bf16[16,304,128]{2,1,0:T(8,128)(2,1)S(1)} async-done(((bf16[16,304,128]{2,1,0:T(8,128)(2,1)}), bf16[16,304,128]{2,1,0:T(8,128)(2,1)S(1)}, u32[]{:S(2)}, u32[]{:S(2)}) %all-to-all-start) | async-done | bytes 1245216 | tf_op jit(solution)/shard_map/all_to_all | solution.py:413
  37.4 0.0 copy-start.8
  37.4 1.3 broadcast_in_dim.48
  38.7 4.4 %all-to-all-start.1 = ((bf16[16,304,128]{2,1,0:T(8,128)(2,1)}), bf16[16,304,128]{2,1,0:T(8,128)(2,1)}, u32[]{:S(2)}, u32[]{:S(2)}) async-start(bf16[16,304,128]{2,1,0:T(8,128)(2,1)} %broadcast_in_dim.48), calls=%async_computation.1 | async-start | bytes 2490368 | tf_op jit(solution)/shard_map/all_to_all | solution.py:413
  43.1 0.0 copy-done.8
  43.2 0.1 collective-permute-start.1
  43.2 0.0 copy-done.3
  43.3 2.3 %collective-permute-done.1.oth_ref.refs_5_.refs_4_ = bf16[1600,256]{1,0:T(8,128)(2,1)S(1)} collective-permute-done((bf16[1600,256]{1,0:T(8,128)(2,1)S(1)}, bf16[1600,256]{1,0:T(8,128)(2,1)S(1)}, u32[]{:S(2)}, u32[]{:S(2)}) %collective-permute-start.1) | collective-permute-done | bytes 819232 | tf_op jit(solution)/shard_map/ppermute | solution.py:408
  45.6 1.0 spread.1
  46.5 12.5 %attend_late.1 = (f32[800,128]{1,0:T(8,128)}, f32[800,128]{1,0:T(8,128)}) custom-call(bf16[304,128]{1,0:T(8,128)(2,1)S(1)} %collective-permute-done.refs_0_, bf16[16,304,128]{2,1,0:T(8,128)(2,1)} %copy-done.8, bf16[768,256]{1,0:T(8,128)(2,1)} %get-tuple-element.17.refs_2_.refs_1_, bf16[12,256,256]{2,1,0:T(8,128)(2,1)S(1)} %get-tuple-element.18.refs_3_.refs_2_, ...), custom_call_target="tpu_custom_call" | custom-call | tf_op jit(solution)/shard_map/attend_late/pallas_call | solution.py:430
  59.0 0.0 copy-start.4
  59.0 0.0 copy-start.5
  59.0 0.0 copy-start.6
  59.0 0.4 collective-permute-start.2
  59.4 1.5 all-to-all-done.1.refs_0_
  60.9 0.0 copy-start
  60.9 0.0 copy-start.1
  60.9 0.0 copy-start.2
  60.9 2.5 %attend_early.1 = (f32[800,128]{1,0:T(8,128)S(1)}, f32[800,128]{1,0:T(8,128)S(1)}) custom-call(bf16[16,304,128]{2,1,0:T(8,128)(2,1)} %all-to-all-done.1.refs_0_, bf16[768,256]{1,0:T(8,128)(2,1)} %get-tuple-element.17.refs_2_.refs_1_, bf16[12,256,256]{2,1,0:T(8,128)(2,1)S(1)} %get-tuple-element.18.refs_3_.refs_2_, ...), custom_call_target="tpu_custom_call" | custom-call | tf_op jit(solution)/shard_map/attend_early/pallas_call | solution.py:430
  63.4 0.1 collective-permute-start.4
  63.5 0.5 collective-permute-start.5
  64.0 0.1 collective-permute-start.6
  64.1 0.4 collective-permute-start.7
  64.5 0.0 collective-permute-done.2.refs_1_
  64.5 0.7 collective-permute-done.4.refs_3_
  65.2 0.0 copy-done.4
  65.2 0.0 copy-done.5
  65.2 0.0 copy-done.6
  65.2 0.0 copy-done
  65.2 0.0 copy-done.1
  65.3 0.0 copy-done.2
  65.3 3.8 %mix.1 = (bf16[128,2048]{1,0:T(8,128)(2,1)S(1)}, bf16[512,2048]{1,0:T(8,128)(2,1)}) custom-call(f32[800,128]{1,0:T(8,128)S(1)} %copy-done.2, f32[800,128]{1,0:T(8,128)} %collective-permute-done.2.refs_1_, f32[800,128]{1,0:T(8,128)S(1)} %get-tuple-element.21.refs_2_, f32[800,128]{1,0:T(8,128)S(1)} %collective-permute-done.4.refs_3_, ...), custom_call_target="tpu_custom_call" | custom-call | tf_op jit(solution)/shard_map/mix/pallas_call | solution.py:452
  69.1 40.1 %all-to-all-start.2 = ((bf16[64,8,2048]{2,1,0:T(8,128)(2,1)}), bf16[64,8,2048]{2,1,0:T(8,128)(2,1)S(1)}, u32[]{:S(2)}, u32[]{:S(2)}) async-start(bf16[64,8,2048]{2,1,0:T(8,128)(2,1)} %bitcast.26), calls=%async_computation.2 | async-start | bytes 4194304 | tf_op jit(solution)/shard_map/all_to_all | solution.py:465
  109.2 0.0 collective-permute-done.5.refs_3_
  109.2 0.0 collective-permute-done.6.refs_4_
  109.2 0.0 collective-permute-done.7.refs_5_
  109.2 30.1 %all-to-all-done.2 = bf16[64,8,2048]{2,1,0:T(8,128)(2,1)S(1)} async-done(((bf16[64,8,2048]{2,1,0:T(8,128)(2,1)}), bf16[64,8,2048]{2,1,0:T(8,128)(2,1)S(1)}, u32[]{:S(2)}, u32[]{:S(2)}) %all-to-all-start.2) | async-done | bytes 2097184 | tf_op jit(solution)/shard_map/all_to_all | solution.py:465
  139.3 10.7 %experts.1 = bf16[512,2048]{1,0:T(8,128)(2,1)} custom-call(bf16[512,2048]{1,0:T(8,128)(2,1)S(1)} %bitcast.16, bf16[2048,512]{1,0:T(8,128)(2,1)} %bitcast.28, bf16[2048,512]{1,0:T(8,128)(2,1)} %bitcast.30, bf16[512,2048]{1,0:T(8,128)(2,1)} %bitcast.32, bf16[2048,512]{1,0:T(8,128)(2,1)} %collective-permute-done.5.refs_3_, ...), custom_call_target="tpu_custom_call" | custom-call | tf_op jit(solution)/shard_map/experts/pallas_call | solution.py:470
  150.1 0.0 copy-start.7
  150.1 35.6 %all_to_all.20 = bf16[64,8,2048]{2,1,0:T(8,128)(2,1)S(1)} all-to-all(bf16[64,8,2048]{2,1,0:T(8,128)(2,1)} %bitcast.25), channel_id=1, replica_groups=mesh['sp'=64,'tp'=2] {'sp'}, dimensions={0} | all-to-all | bytes 4194304 | tf_op jit(solution)/shard_map/all_to_all | solution.py:465
  185.6 0.0 copy-done.7
  185.6 1.7 pick.1
  (4 shorter events, 0.0 us)
Async XLA Ops:
  2.3 7.9 %collective-permute-start = (bf16[304,128]{1,0:T(8,128)(2,1)S(1)}, bf16[304,128]{1,0:T(8,128)(2,1)S(1)}, u32[]{:S(2)}, u32[]{:S(2)}) collective-permute-start(bf16[304,128]{1,0:T(8,128)(2,1)S(1)} %get-tuple-element.15), channel_id=1, source_target_pairs={{0,64},{2,66},{4,68},{6,70},{8,72},{10,74},{12,76},{14,78},{16,80}... | collective-permute-start | bytes 233480 | tf_op jit(solution)/shard_map/ppermute | solution.py:407
  11.4 26.0 %all-to-all-start = ((bf16[16,304,128]{2,1,0:T(8,128)(2,1)}), bf16[16,304,128]{2,1,0:T(8,128)(2,1)S(1)}, u32[]{:S(2)}, u32[]{:S(2)}) async-start(bf16[16,304,128]{2,1,0:T(8,128)(2,1)} %broadcast_select_fusion), calls=%async_computation | async-start | bytes 2490368 | tf_op jit(solution)/shard_map/all_to_all | solution.py:413
  18.5 24.8 %copy-start.3 = (s32[256]{0:T(256)S(1)}, s32[256]{0:T(256)}, u32[]{:S(2)}) copy-start(s32[256]{0:T(256)} %refs_6_.1) | copy-start | bytes 3076
  18.5 4.9 %collective-permute-start.3 = (bf16[304,128]{1,0:T(8,128)(2,1)S(1)}, bf16[304,128]{1,0:T(8,128)(2,1)S(1)}, u32[]{:S(2)}, u32[]{:S(2)}) collective-permute-start(bf16[304,128]{1,0:T(8,128)(2,1)S(1)} %get-tuple-element.15), channel_id=1, source_target_pairs={{0,32},{2,34},{4,36},{6,38},{8,40},{10,42},{12,44},{14,46},{16,48}... | collective-permute-start | bytes 233480 | tf_op jit(solution)/shard_map/ppermute | solution.py:407
  37.4 5.7 %copy-start.8 = (bf16[16,304,128]{2,1,0:T(8,128)(2,1)}, bf16[16,304,128]{2,1,0:T(8,128)(2,1)S(1)}, u32[]{:S(2)}) copy-start(bf16[16,304,128]{2,1,0:T(8,128)(2,1)S(1)} %all-to-all-done.refs_1_) | copy-start | bytes 3735556
  38.7 22.2 %all-to-all-start.1 = ((bf16[16,304,128]{2,1,0:T(8,128)(2,1)}), bf16[16,304,128]{2,1,0:T(8,128)(2,1)}, u32[]{:S(2)}, u32[]{:S(2)}) async-start(bf16[16,304,128]{2,1,0:T(8,128)(2,1)} %broadcast_in_dim.48), calls=%async_computation.1 | async-start | bytes 2490368 | tf_op jit(solution)/shard_map/all_to_all | solution.py:413
  43.2 2.4 %collective-permute-start.1 = (bf16[1600,256]{1,0:T(8,128)(2,1)S(1)}, bf16[1600,256]{1,0:T(8,128)(2,1)S(1)}, u32[]{:S(2)}, u32[]{:S(2)}) collective-permute-start(bf16[1600,256]{1,0:T(8,128)(2,1)S(1)} %get-tuple-element.16.own_ref.refs_4_.refs_3_), channel_id=1, source_target_pairs={{0,1},{1,0},{2,3},{3,2},{4,5},{5,4},{6,7},{7,6},{8,9},{9,8},{10,11... | collective-permute-start | bytes 2457608 | tf_op jit(solution)/shard_map/ppermute | solution.py:408
  59.0 6.2 %copy-start.4 = (f32[2048]{0:T(1024)S(1)}, f32[2048]{0:T(1024)}, u32[]{:S(2)}) copy-start(f32[2048]{0:T(1024)} %param.23) | copy-start | bytes 24580
  59.0 6.2 %copy-start.5 = (f32[2048]{0:T(1024)S(1)}, f32[2048]{0:T(1024)}, u32[]{:S(2)}) copy-start(f32[2048]{0:T(1024)} %param.24) | copy-start | bytes 24580
  59.0 6.2 %copy-start.6 = (s32[128,2]{0,1:T(2,128)S(1)}, s32[128,2]{0,1:T(2,128)}, u32[]{:S(2)}) copy-start(s32[128,2]{0,1:T(2,128)} %param.25) | copy-start | bytes 3076
  59.0 5.5 %collective-permute-start.2 = (f32[800,128]{1,0:T(8,128)}, f32[800,128]{1,0:T(8,128)}, u32[]{:S(2)}, u32[]{:S(2)}) collective-permute-start(f32[800,128]{1,0:T(8,128)} %get-tuple-element.20), channel_id=1, source_target_pairs={{0,1},{1,0},{2,3},{3,2},{4,5},{5,4},{6,7},{7,6},{8,9},{9,8},{10,11... | collective-permute-start | bytes 1228808 | tf_op jit(solution)/shard_map/ppermute | solution.py:449
  60.9 4.3 %copy-start = (bf16[768,2048]{1,0:T(8,128)(2,1)S(1)}, bf16[768,2048]{1,0:T(8,128)(2,1)}, u32[]{:S(2)}) copy-start(bf16[768,2048]{1,0:T(8,128)(2,1)} %refs_4_.3) | copy-start | bytes 9437188
  60.9 4.3 %copy-start.1 = (bf16[128,2048]{1,0:T(8,128)(2,1)S(1)}, bf16[128,2048]{1,0:T(8,128)(2,1)}, u32[]{:S(2)}) copy-start(bf16[128,2048]{1,0:T(8,128)(2,1)} %refs_5_.3) | copy-start | bytes 1572868
  60.9 4.3 %copy-start.2 = (f32[800,128]{1,0:T(8,128)S(1)}, f32[800,128]{1,0:T(8,128)}, u32[]{:S(2)}) copy-start(f32[800,128]{1,0:T(8,128)} %get-tuple-element.19.refs_0_) | copy-start | bytes 1228804
  63.4 1.8 collective-permute-start.4
  63.5 45.7 %collective-permute-start.5 = (bf16[2048,512]{1,0:T(8,128)(2,1)}, bf16[2048,512]{1,0:T(8,128)(2,1)}, u32[]{:S(2)}, u32[]{:S(2)}) collective-permute-start(bf16[2048,512]{1,0:T(8,128)(2,1)} %bitcast.27), channel_id=1, source_target_pairs={{0,1},{1,0},{2,3},{3,2},{4,5},{5,4},{6,7},{7,6},{8,9},{9,8},{10,11... | collective-permute-start | bytes 6291464 | tf_op jit(solution)/shard_map/ppermute | solution.py:462
  64.0 45.2 %collective-permute-start.6 = (bf16[2048,512]{1,0:T(8,128)(2,1)}, bf16[2048,512]{1,0:T(8,128)(2,1)}, u32[]{:S(2)}, u32[]{:S(2)}) collective-permute-start(bf16[2048,512]{1,0:T(8,128)(2,1)} %bitcast.29), channel_id=1, source_target_pairs={{0,1},{1,0},{2,3},{3,2},{4,5},{5,4},{6,7},{7,6},{8,9},{9,8},{10,11... | collective-permute-start | bytes 6291464 | tf_op jit(solution)/shard_map/ppermute | solution.py:462
  64.1 45.1 %collective-permute-start.7 = (bf16[512,2048]{1,0:T(8,128)(2,1)}, bf16[512,2048]{1,0:T(8,128)(2,1)}, u32[]{:S(2)}, u32[]{:S(2)}) collective-permute-start(bf16[512,2048]{1,0:T(8,128)(2,1)} %bitcast.31), channel_id=1, source_target_pairs={{0,1},{1,0},{2,3},{3,2},{4,5},{5,4},{6,7},{7,6},{8,9},{9,8},{10,11... | collective-permute-start | bytes 6291464 | tf_op jit(solution)/shard_map/ppermute | solution.py:462
  69.1 70.2 %all-to-all-start.2 = ((bf16[64,8,2048]{2,1,0:T(8,128)(2,1)}), bf16[64,8,2048]{2,1,0:T(8,128)(2,1)S(1)}, u32[]{:S(2)}, u32[]{:S(2)}) async-start(bf16[64,8,2048]{2,1,0:T(8,128)(2,1)} %bitcast.26), calls=%async_computation.2 | async-start | bytes 4194304 | tf_op jit(solution)/shard_map/all_to_all | solution.py:465
  150.1 35.6 %copy-start.7 = (f32[128,2]{0,1:T(2,128)S(1)}, f32[128,2]{0,1:T(2,128)}, u32[]{:S(2)}) copy-start(f32[128,2]{0,1:T(2,128)} %param.26) | copy-start | bytes 3076

commit v4 on v2

--- a/solution.py
+++ b/solution.py
@@ -7,6 +7,7 @@
 from jax.experimental import pallas as pl
 from jax.experimental.pallas import tpu as pltpu
 from jax.sharding import PartitionSpec as P
+
 
 D = 2048
 NOPE = 64
@@ -28,6 +29,7 @@
 ATTEND_MIB = 24
 LOW = -1e30
 SCALE = (NOPE + ROPE) ** -0.5 * math.log2(math.e)
+PIECES = 4
 f32 = jnp.float32
 bf16 = jnp.bfloat16
 
@@ -303,7 +305,7 @@
 
 
 def mix_kernel(*refs):
-    parts, (proj_ref, res_ref, mixg_ref, moeg_ref, ids_ref, mid_ref, buf_ref) = refs[:4], refs[4:]
+    parts, (proj_ref, res_ref, mixg_ref, moeg_ref, ids_ref, mid_ref, buf_ref, held, sems) = refs[:4], refs[4:]
     lane = lanes(HALF)
     stats = [part[:, 768:896] for part in parts]
     top = jnp.maximum(jnp.maximum(stats[0], stats[1]), jnp.maximum(stats[2], stats[3]))
@@ -326,7 +328,15 @@
     wide = middle.astype(f32)
     normed = (wide * norm_of(wide) * moeg_ref[...]).astype(bf16)
     picks = slots_of(ids_ref[...])
-    buf_ref[...] = jnp.dot(picks[0] + picks[1], normed, preferred_element_type=f32).astype(bf16)
+    chosen = picks[0] + picks[1]
+    copies = []
+    for r in range(PIECES):
+        rows = slice(r * SLOTS // PIECES, (r + 1) * SLOTS // PIECES)
+        held[rows, :] = jnp.dot(chosen[rows], normed, preferred_element_type=f32).astype(bf16)
+        copies.append(pltpu.make_async_copy(held.at[rows], buf_ref.at[rows], sems.at[r]))
+        copies[r].start()
+    for copy in copies:
+        copy.wait()
 
 
 def expert_kernel(rows_ref, *refs):
@@ -394,16 +404,21 @@
         compiler_params=params(8),
         name="prep",
     )(*map(far, inputs))
-    before = [lax.ppermute(payload, "sp", [(i, i + PLANE * k) for i in range(sp - PLANE * k)]) for k in (1, 2)]
+    before = []
+    for k in (1, 2):
+        before.append(lax.ppermute(payload, "sp", [(i, i + PLANE * k) for i in range(sp - PLANE * k)]))
     other = lax.ppermute(pack, "tp", swap)
+    own = (gate_weight[0], up_weight[0], down_weight[0])
+    swapped = tuple(lax.ppermute(w, "tp", swap) for w in own)
     target = jnp.arange(PLANE, dtype=jnp.int32)[:, None, None]
     groups = [[z * PLANE + i for i in range(PLANE)] for z in range(sp // PLANE)]
-    late = lax.all_to_all(
-        jnp.where(spot <= target, payload[None], before[1][None]), "sp", 0, 0, axis_index_groups=groups, tiled=True
-    )
-    early = lax.all_to_all(
-        jnp.broadcast_to(before[0][None], (PLANE, ROWS, 128)), "sp", 0, 0, axis_index_groups=groups, tiled=True
-    )
+
+    def plane(x):
+        return lax.all_to_all(x, "sp", 0, 0, axis_index_groups=groups, tiled=True)
+
+    late = plane(jnp.where(spot <= target, payload[None], before[1][None]))
+    fanned = jnp.broadcast_to(before[0][None], (PLANE, ROWS, 128))
+    early = plane(fanned)
     query_docs = jnp.broadcast_to(doc_ids.astype(f32)[:, None], (BLOCK, 128))
     spread = pl.pallas_call(
         spread_kernel,
@@ -441,13 +456,12 @@
         mix_kernel,
         out_shape=(jax.ShapeDtypeStruct((HALF, D), bf16), pltpu.HBM((SLOTS, D), bf16)),
         in_specs=[vmem()] * 9,
-        out_specs=(vmem(), vmem()),
+        out_specs=(vmem(), hbm()),
+        scratch_shapes=[pltpu.VMEM((SLOTS, D), bf16), pltpu.SemaphoreType.DMA((PIECES,))],
         compiler_params=params(16),
         name="mix",
     )(*parts, out_proj, residual, mix_gain[None], moe_gain[None], expert_ids.T)
     rows = lax.all_to_all(buffer.reshape(EXPERTS, CAPACITY, D), "sp", 0, 0, tiled=True).reshape(SLOTS, D)
-    own = (gate_weight[0], up_weight[0], down_weight[0])
-    swapped = tuple(lax.ppermute(w, "tp", swap) for w in own)
     result = pl.pallas_call(
         expert_kernel,
         out_shape=jax.ShapeDtypeStruct((SLOTS, D), bf16),
@@ -488,4 +502,5 @@
         P("sp", "tp", None),
     )
     out_specs = P(("sp", "tp"), None)
+
     return jax.shard_map(local, mesh=mesh, in_specs=in_specs, out_specs=out_specs, check_vma=False)

time: 175 us -> 175 us (level); the launches traced: 173 us -> 175 us
  starting transfers between devices: 46 us -> 48.2 us
    all_to_all x1, starting transfers between devices: 24.2 us -> 26.3 us  [local(): lax.all_to_all(buffer.reshape(EXPERTS, CAPACITY, D), 'sp', 0, 0, tiled=True)]
where the time goes in v4:
time: 175 us
  waiting for transfers between devices  56.3 us (32%)
  starting transfers between devices  48.2 us (28%)
  blocking collectives  35.3 us (20%)
  Pallas kernels  31.2 us (18%)
  other arithmetic  1.98 us (1%)
    all_to_all x1, blocking collectives, local(): back = lax.all_to_all(result, 'sp', 0, 0, tiled=True).reshape(SLOTS, D)  35.3 us
    all_to_all x1, waiting for transfers between devices, local(): lax.all_to_all(buffer.reshape(EXPERTS, CAPACITY, D), 'sp', 0, 0, tiled=True)  30.1 us
    all_to_all x1, starting transfers between devices, local(): lax.all_to_all(buffer.reshape(EXPERTS, CAPACITY, D), 'sp', 0, 0, tiled=True)  26.3 us
    all_to_all x2, waiting for transfers between devices, plane(): return lax.all_to_all(x, 'sp', 0, 0, axis_index_groups=groups, tiled=True)  19 us
    pallas_call x2, Pallas kernels, attend(): pl.pallas_call(functools.partial(attend_kernel, is_late), out_shape=(pltp...  12.5 us
    all_to_all x2, starting transfers between devices, plane(): return lax.all_to_all(x, 'sp', 0, 0, axis_index_groups=groups, tiled=True)  11.4 us
    pallas_call x1, Pallas kernels, local(): pl.pallas_call(expert_kernel, out_shape=jax.ShapeDtypeStruct((SLOTS, D),...  9.33 us
    ppermute x2, starting transfers between devices, local(): lax.ppermute(payload, 'sp', [(i, i + PLANE * k) for i in range(sp - PLANE...  8.83 us
  transfers between devices with their start and end apart: 11, of which 7 were waited for; matrix products, arithmetic and copies ran while one was open for 0% of the time, Pallas kernels for 11%

profile of v4, /device:TPU:0, one launch (start us, length us, event | category | flops | bytes accessed | tf_op | source)
XLA Modules:
  0.0 174.7 jit_solution(13631631617116588929)
XLA Ops:
  0.0 0.8 multiply_sine_fusion
  0.8 1.6 prep.1
  2.4 5.9 %collective-permute-start = (bf16[304,128]{1,0:T(8,128)(2,1)S(1)}, bf16[304,128]{1,0:T(8,128)(2,1)S(1)}, u32[]{:S(2)}, u32[]{:S(2)}) collective-permute-start(bf16[304,128]{1,0:T(8,128)(2,1)S(1)} %get-tuple-element.13), channel_id=1, source_target_pairs={{0,64},{2,66},{4,68},{6,70},{8,72},{10,74},{12,76},{14,78},{16,80}... | collective-permute-start | bytes 233480 | tf_op jit(solution)/shard_map/ppermute | solution.py:409
  8.3 2.0 %collective-permute-done.refs_0_ = bf16[304,128]{1,0:T(8,128)(2,1)S(1)} collective-permute-done((bf16[304,128]{1,0:T(8,128)(2,1)S(1)}, bf16[304,128]{1,0:T(8,128)(2,1)S(1)}, u32[]{:S(2)}, u32[]{:S(2)}) %collective-permute-start) | collective-permute-done | bytes 77856 | tf_op jit(solution)/shard_map/ppermute | solution.py:409
  10.3 1.2 broadcast_select_fusion
  11.5 7.0 %all-to-all-start = ((bf16[16,304,128]{2,1,0:T(8,128)(2,1)}), bf16[16,304,128]{2,1,0:T(8,128)(2,1)S(1)}, u32[]{:S(2)}, u32[]{:S(2)}) async-start(bf16[16,304,128]{2,1,0:T(8,128)(2,1)} %broadcast_select_fusion), calls=%async_computation | async-start | bytes 2490368 | tf_op jit(solution)/shard_map/all_to_all | solution.py:417
  18.5 0.0 copy-start.3
  18.5 2.9 %collective-permute-start.3 = (bf16[304,128]{1,0:T(8,128)(2,1)S(1)}, bf16[304,128]{1,0:T(8,128)(2,1)S(1)}, u32[]{:S(2)}, u32[]{:S(2)}) collective-permute-start(bf16[304,128]{1,0:T(8,128)(2,1)S(1)} %get-tuple-element.13), channel_id=1, source_target_pairs={{0,32},{2,34},{4,36},{6,38},{8,40},{10,42},{12,44},{14,46},{16,48}... | collective-permute-start | bytes 233480 | tf_op jit(solution)/shard_map/ppermute | solution.py:409
  21.5 2.0 %collective-permute-done.3 = bf16[304,128]{1,0:T(8,128)(2,1)S(1)} collective-permute-done((bf16[304,128]{1,0:T(8,128)(2,1)S(1)}, bf16[304,128]{1,0:T(8,128)(2,1)S(1)}, u32[]{:S(2)}, u32[]{:S(2)}) %collective-permute-start.3) | collective-permute-done | bytes 77856 | tf_op jit(solution)/shard_map/ppermute | solution.py:409
  23.5 14.0 %all-to-all-done.refs_1_ = bf16[16,304,128]{2,1,0:T(8,128)(2,1)S(1)} async-done(((bf16[16,304,128]{2,1,0:T(8,128)(2,1)}), bf16[16,304,128]{2,1,0:T(8,128)(2,1)S(1)}, u32[]{:S(2)}, u32[]{:S(2)}) %all-to-all-start) | async-done | bytes 1245216 | tf_op jit(solution)/shard_map/all_to_all | solution.py:417
  37.5 0.0 copy-start.8
  37.5 1.3 broadcast_in_dim.51
  38.8 4.4 %all-to-all-start.1 = ((bf16[16,304,128]{2,1,0:T(8,128)(2,1)}), bf16[16,304,128]{2,1,0:T(8,128)(2,1)}, u32[]{:S(2)}, u32[]{:S(2)}) async-start(bf16[16,304,128]{2,1,0:T(8,128)(2,1)} %broadcast_in_dim.51), calls=%async_computation.1 | async-start | bytes 2490368 | tf_op jit(solution)/shard_map/all_to_all | solution.py:417
  43.2 0.1 collective-permute-start.1
  43.3 0.0 copy-done.3
  43.3 0.0 copy-done.8
  43.3 2.3 %collective-permute-done.1.oth_ref.refs_4_.refs_3_ = bf16[256,1664]{1,0:T(8,128)(2,1)S(1)} collective-permute-done((bf16[256,1664]{1,0:T(8,128)(2,1)S(1)}, bf16[256,1664]{1,0:T(8,128)(2,1)S(1)}, u32[]{:S(2)}, u32[]{:S(2)}) %collective-permute-start.1) | collective-permute-done | bytes 852000 | tf_op jit(solution)/shard_map/ppermute | solution.py:410
  45.6 0.3 spread.1.refs_2_.refs_1_
  45.9 0.1 broadcast_in_dim.50.refs_5_.refs_4_
  46.0 9.4 %attend_late.1 = (f32[128,896]{1,0:T(8,128)}, f32[128,896]{1,0:T(8,128)}) custom-call(bf16[304,128]{1,0:T(8,128)(2,1)S(1)} %collective-permute-done.refs_0_, bf16[16,304,128]{2,1,0:T(8,128)(2,1)} %copy-done.8, bf16[12,256,256]{2,1,0:T(8,128)(2,1)S(1)} %spread.1.refs_2_.refs_1_, bf16[256,1664]{1,0:T(8,128)(2,1)S(1)} %get-tuple-element.14.own_ref.refs_3_.refs_2_, ...), custom_call_target="tpu_custom_call" | custom-call | tf_op jit(solution)/shard_map/attend_late/pallas_call | solution.py:434
  55.5 0.0 copy-start.4
  55.5 0.0 copy-start.5
  55.5 0.0 copy-start.6
  55.5 0.4 collective-permute-start.2
  55.9 5.0 %all-to-all-done.1.refs_0_ = bf16[16,304,128]{2,1,0:T(8,128)(2,1)} async-done(((bf16[16,304,128]{2,1,0:T(8,128)(2,1)}), bf16[16,304,128]{2,1,0:T(8,128)(2,1)}, u32[]{:S(2)}, u32[]{:S(2)}) %all-to-all-start.1) | async-done | bytes 1245216 | tf_op jit(solution)/shard_map/all_to_all | solution.py:417
  60.9 0.0 copy-start
  60.9 0.0 copy-start.1
  60.9 0.0 copy-start.2
  60.9 3.0 %attend_early.1 = (f32[128,896]{1,0:T(8,128)S(1)}, f32[128,896]{1,0:T(8,128)S(1)}) custom-call(bf16[16,304,128]{2,1,0:T(8,128)(2,1)} %all-to-all-done.1.refs_0_, bf16[12,256,256]{2,1,0:T(8,128)(2,1)S(1)} %spread.1.refs_2_.refs_1_, bf16[256,1664]{1,0:T(8,128)(2,1)S(1)} %get-tuple-element.14.own_ref.refs_3_.refs_2_, ...), custom_call_target="tpu_custom_call" | custom-call | tf_op jit(solution)/shard_map/attend_early/pallas_call | solution.py:434
  64.0 0.1 collective-permute-start.4
  64.1 0.5 collective-permute-start.5
  64.6 0.1 collective-permute-start.6
  64.7 0.4 collective-permute-start.7
  65.1 0.0 collective-permute-done.2.refs_1_
  65.1 0.8 collective-permute-done.4.refs_3_
  65.9 0.0 copy-done.4
  65.9 0.0 copy-done.5
  65.9 0.0 copy-done.6
  65.9 0.0 copy-done
  65.9 0.0 copy-done.1
  65.9 0.0 copy-done.2
  65.9 5.9 %mix.1 = (bf16[128,2048]{1,0:T(8,128)(2,1)S(1)}, bf16[512,2048]{1,0:T(8,128)(2,1)}) custom-call(f32[128,896]{1,0:T(8,128)S(1)} %copy-done.2, f32[128,896]{1,0:T(8,128)} %collective-permute-done.2.refs_1_, f32[128,896]{1,0:T(8,128)S(1)} %get-tuple-element.17.refs_2_, f32[128,896]{1,0:T(8,128)S(1)} %collective-permute-done.4.refs_3_, ...), custom_call_target="tpu_custom_call" | custom-call | tf_op jit(solution)/shard_map/mix/pallas_call | solution.py:455
  71.8 26.3 %all-to-all-start.2 = ((bf16[64,8,2048]{2,1,0:T(8,128)(2,1)}), bf16[64,8,2048]{2,1,0:T(8,128)(2,1)S(1)}, u32[]{:S(2)}, u32[]{:S(2)}) async-start(bf16[64,8,2048]{2,1,0:T(8,128)(2,1)} %bitcast.23), calls=%async_computation.2 | async-start | bytes 4194304 | tf_op jit(solution)/shard_map/all_to_all | solution.py:464
  98.1 0.0 collective-permute-done.5.refs_3_
  98.1 0.0 collective-permute-done.6.refs_4_
  98.1 0.0 collective-permute-done.7.refs_5_
  98.2 30.1 %all-to-all-done.2 = bf16[64,8,2048]{2,1,0:T(8,128)(2,1)S(1)} async-done(((bf16[64,8,2048]{2,1,0:T(8,128)(2,1)}), bf16[64,8,2048]{2,1,0:T(8,128)(2,1)S(1)}, u32[]{:S(2)}, u32[]{:S(2)}) %all-to-all-start.2) | async-done | bytes 2097184 | tf_op jit(solution)/shard_map/all_to_all | solution.py:464
  128.3 9.3 %experts.1 = bf16[512,2048]{1,0:T(8,128)(2,1)S(1)} custom-call(bf16[512,2048]{1,0:T(8,128)(2,1)S(1)} %bitcast.15, bf16[2048,512]{1,0:T(8,128)(2,1)} %bitcast.25, bf16[2048,512]{1,0:T(8,128)(2,1)} %bitcast.27, bf16[512,2048]{1,0:T(8,128)(2,1)} %bitcast.29, bf16[2048,512]{1,0:T(8,128)(2,1)} %collective-permute-done.5.refs_3_, ...), custom_call_target="tpu_custom_call" | custom-call | tf_op jit(solution)/shard_map/experts/pallas_call | solution.py:465
  137.6 0.0 copy-start.7
  137.6 35.3 %all_to_all.20 = bf16[64,8,2048]{2,1,0:T(8,128)(2,1)S(1)} all-to-all(bf16[64,8,2048]{2,1,0:T(8,128)(2,1)S(1)} %bitcast.16), channel_id=1, replica_groups=mesh['sp'=64,'tp'=2] {'sp'}, dimensions={0} | all-to-all | bytes 4194304 | tf_op jit(solution)/shard_map/all_to_all | solution.py:475
  173.0 0.0 copy-done.7
  173.0 1.7 pick.1
  (4 shorter events, 0.0 us)
Async XLA Ops:
  2.4 7.9 %collective-permute-start = (bf16[304,128]{1,0:T(8,128)(2,1)S(1)}, bf16[304,128]{1,0:T(8,128)(2,1)S(1)}, u32[]{:S(2)}, u32[]{:S(2)}) collective-permute-start(bf16[304,128]{1,0:T(8,128)(2,1)S(1)} %get-tuple-element.13), channel_id=1, source_target_pairs={{0,64},{2,66},{4,68},{6,70},{8,72},{10,74},{12,76},{14,78},{16,80}... | collective-permute-start | bytes 233480 | tf_op jit(solution)/shard_map/ppermute | solution.py:409
  11.5 26.0 %all-to-all-start = ((bf16[16,304,128]{2,1,0:T(8,128)(2,1)}), bf16[16,304,128]{2,1,0:T(8,128)(2,1)S(1)}, u32[]{:S(2)}, u32[]{:S(2)}) async-start(bf16[16,304,128]{2,1,0:T(8,128)(2,1)} %broadcast_select_fusion), calls=%async_computation | async-start | bytes 2490368 | tf_op jit(solution)/shard_map/all_to_all | solution.py:417
  18.5 24.8 %copy-start.3 = (s32[256]{0:T(256)S(1)}, s32[256]{0:T(256)}, u32[]{:S(2)}) copy-start(s32[256]{0:T(256)} %refs_5_.4) | copy-start | bytes 3076
  18.5 4.9 %collective-permute-start.3 = (bf16[304,128]{1,0:T(8,128)(2,1)S(1)}, bf16[304,128]{1,0:T(8,128)(2,1)S(1)}, u32[]{:S(2)}, u32[]{:S(2)}) collective-permute-start(bf16[304,128]{1,0:T(8,128)(2,1)S(1)} %get-tuple-element.13), channel_id=1, source_target_pairs={{0,32},{2,34},{4,36},{6,38},{8,40},{10,42},{12,44},{14,46},{16,48}... | collective-permute-start | bytes 233480 | tf_op jit(solution)/shard_map/ppermute | solution.py:409
  37.5 5.8 %copy-start.8 = (bf16[16,304,128]{2,1,0:T(8,128)(2,1)}, bf16[16,304,128]{2,1,0:T(8,128)(2,1)S(1)}, u32[]{:S(2)}) copy-start(bf16[16,304,128]{2,1,0:T(8,128)(2,1)S(1)} %all-to-all-done.refs_1_) | copy-start | bytes 3735556
  38.8 22.2 %all-to-all-start.1 = ((bf16[16,304,128]{2,1,0:T(8,128)(2,1)}), bf16[16,304,128]{2,1,0:T(8,128)(2,1)}, u32[]{:S(2)}, u32[]{:S(2)}) async-start(bf16[16,304,128]{2,1,0:T(8,128)(2,1)} %broadcast_in_dim.51), calls=%async_computation.1 | async-start | bytes 2490368 | tf_op jit(solution)/shard_map/all_to_all | solution.py:417
  43.2 2.5 %collective-permute-start.1 = (bf16[256,1664]{1,0:T(8,128)(2,1)S(1)}, bf16[256,1664]{1,0:T(8,128)(2,1)S(1)}, u32[]{:S(2)}, u32[]{:S(2)}) collective-permute-start(bf16[256,1664]{1,0:T(8,128)(2,1)S(1)} %get-tuple-element.14.own_ref.refs_3_.refs_2_), channel_id=1, source_target_pairs={{0,1},{1,0},{2,3},{3,2},{4,5},{5,4},{6,7},{7,6},{8,9},{9,8},{10,11... | collective-permute-start | bytes 2555912 | tf_op jit(solution)/shard_map/ppermute | solution.py:410
  55.5 10.4 %copy-start.4 = (f32[2048]{0:T(1024)S(1)}, f32[2048]{0:T(1024)}, u32[]{:S(2)}) copy-start(f32[2048]{0:T(1024)} %param.23) | copy-start | bytes 24580
  55.5 10.4 %copy-start.5 = (f32[2048]{0:T(1024)S(1)}, f32[2048]{0:T(1024)}, u32[]{:S(2)}) copy-start(f32[2048]{0:T(1024)} %param.24) | copy-start | bytes 24580
  55.5 10.4 %copy-start.6 = (s32[128,2]{0,1:T(2,128)S(1)}, s32[128,2]{0,1:T(2,128)}, u32[]{:S(2)}) copy-start(s32[128,2]{0,1:T(2,128)} %param.25) | copy-start | bytes 3076
  55.5 9.6 %collective-permute-start.2 = (f32[128,896]{1,0:T(8,128)}, f32[128,896]{1,0:T(8,128)}, u32[]{:S(2)}, u32[]{:S(2)}) collective-permute-start(f32[128,896]{1,0:T(8,128)} %get-tuple-element.16), channel_id=1, source_target_pairs={{0,1},{1,0},{2,3},{3,2},{4,5},{5,4},{6,7},{7,6},{8,9},{9,8},{10,11... | collective-permute-start | bytes 1376264 | tf_op jit(solution)/shard_map/ppermute | solution.py:452
  60.9 5.0 %copy-start = (bf16[768,2048]{1,0:T(8,128)(2,1)S(1)}, bf16[768,2048]{1,0:T(8,128)(2,1)}, u32[]{:S(2)}) copy-start(bf16[768,2048]{1,0:T(8,128)(2,1)} %refs_4_.3) | copy-start | bytes 9437188
  60.9 5.0 %copy-start.1 = (bf16[128,2048]{1,0:T(8,128)(2,1)S(1)}, bf16[128,2048]{1,0:T(8,128)(2,1)}, u32[]{:S(2)}) copy-start(bf16[128,2048]{1,0:T(8,128)(2,1)} %refs_5_.5) | copy-start | bytes 1572868
  60.9 5.0 %copy-start.2 = (f32[128,896]{1,0:T(8,128)S(1)}, f32[128,896]{1,0:T(8,128)}, u32[]{:S(2)}) copy-start(f32[128,896]{1,0:T(8,128)} %get-tuple-element.15.refs_0_) | copy-start | bytes 1376260
  64.0 1.9 %collective-permute-start.4 = (f32[128,896]{1,0:T(8,128)S(1)}, f32[128,896]{1,0:T(8,128)S(1)}, u32[]{:S(2)}, u32[]{:S(2)}) collective-permute-start(f32[128,896]{1,0:T(8,128)S(1)} %get-tuple-element.18), channel_id=1, source_target_pairs={{0,1},{1,0},{2,3},{3,2},{4,5},{5,4},{6,7},{7,6},{8,9},{9,8},{10,11... | collective-permute-start | bytes 1376264 | tf_op jit(solution)/shard_map/ppermute | solution.py:452
  64.1 34.0 %collective-permute-start.5 = (bf16[2048,512]{1,0:T(8,128)(2,1)}, bf16[2048,512]{1,0:T(8,128)(2,1)}, u32[]{:S(2)}, u32[]{:S(2)}) collective-permute-start(bf16[2048,512]{1,0:T(8,128)(2,1)} %bitcast.24), channel_id=1, source_target_pairs={{0,1},{1,0},{2,3},{3,2},{4,5},{5,4},{6,7},{7,6},{8,9},{9,8},{10,11... | collective-permute-start | bytes 6291464 | tf_op jit(solution)/shard_map/ppermute | solution.py:412
  64.6 33.6 %collective-permute-start.6 = (bf16[2048,512]{1,0:T(8,128)(2,1)}, bf16[2048,512]{1,0:T(8,128)(2,1)}, u32[]{:S(2)}, u32[]{:S(2)}) collective-permute-start(bf16[2048,512]{1,0:T(8,128)(2,1)} %bitcast.26), channel_id=1, source_target_pairs={{0,1},{1,0},{2,3},{3,2},{4,5},{5,4},{6,7},{7,6},{8,9},{9,8},{10,11... | collective-permute-start | bytes 6291464 | tf_op jit(solution)/shard_map/ppermute | solution.py:412
  64.7 33.5 %collective-permute-start.7 = (bf16[512,2048]{1,0:T(8,128)(2,1)}, bf16[512,2048]{1,0:T(8,128)(2,1)}, u32[]{:S(2)}, u32[]{:S(2)}) collective-permute-start(bf16[512,2048]{1,0:T(8,128)(2,1)} %bitcast.28), channel_id=1, source_target_pairs={{0,1},{1,0},{2,3},{3,2},{4,5},{5,4},{6,7},{7,6},{8,9},{9,8},{10,11... | collective-permute-start | bytes 6291464 | tf_op jit(solution)/shard_map/ppermute | solution.py:412
  71.8 56.5 %all-to-all-start.2 = ((bf16[64,8,2048]{2,1,0:T(8,128)(2,1)}), bf16[64,8,2048]{2,1,0:T(8,128)(2,1)S(1)}, u32[]{:S(2)}, u32[]{:S(2)}) async-start(bf16[64,8,2048]{2,1,0:T(8,128)(2,1)} %bitcast.23), calls=%async_computation.2 | async-start | bytes 4194304 | tf_op jit(solution)/shard_map/all_to_all | solution.py:464
  137.6 35.4 %copy-start.7 = (f32[128,2]{0,1:T(2,128)S(1)}, f32[128,2]{0,1:T(2,128)}, u32[]{:S(2)}) copy-start(f32[128,2]{0,1:T(2,128)} %param.26) | copy-start | bytes 3076

commit v5 on v4

--- a/solution.py
+++ b/solution.py
@@ -62,15 +62,18 @@
     return first * cosine - second * sine, second * cosine + first * sine
 
 
-def prep_kernel(*refs):
-    inputs, (pay_ref, pack_ref) = refs[:8], refs[8:10]
-    held, sems = refs[10:18], refs[18]
+def fetch_all(inputs, held, sems):
     copies = [pltpu.make_async_copy(src, dst, sems.at[i]) for i, (src, dst) in enumerate(zip(inputs, held))]
     for copy in copies:
         copy.start()
     for copy in copies:
         copy.wait()
-    q_ref, lat_ref, rope_ref, doc_ref, wk_ref, wv_ref, cos_ref, sin_ref = held
+
+
+def prep_kernel(*refs):
+    pay_ref, held, sems = refs[5], refs[6:11], refs[11]
+    fetch_all(refs[:5], held, sems)
+    lat_ref, rope_ref, doc_ref, cos_ref, sin_ref = held
     half = lax.axis_index("tp")
     cosine, sine = cos_ref[...], sin_ref[...]
     mine = pl.ds(pl.multiple_of(half * HALF, HALF), HALF)
@@ -86,6 +89,13 @@
     pay_ref[256:288, :] = packed.astype(bf16)
     docs = doc_ref[pl.ds(half, 1), :].astype(f32)
     pay_ref[288:304, :] = jnp.broadcast_to(docs, (16, 128)).astype(bf16)
+
+
+def pack_kernel(*refs):
+    pack_ref, held, sems = refs[5], refs[6:11], refs[11]
+    fetch_all(refs[:5], held, sems)
+    q_ref, wk_ref, wv_ref, cos_ref, sin_ref = held
+    cosine, sine = cos_ref[...], sin_ref[...]
     lane = lanes(BLOCK)
     for head in range(LOCAL_HEADS):
         start = head * (NOPE + ROPE)
@@ -145,7 +155,11 @@
     def place(block):
         return jnp.where(block >= 0, block * BLOCK + half * HALF, -1)
 
-    groups = [[(arr_ref, 8 * t + b, block_of(8 * t + b)) for b in range(8)] for t in range(2)]
+    wide_tile = 8 if late else 16
+    tiles = PLANE // wide_tile
+    groups = [
+        [(arr_ref, wide_tile * t + b, block_of(wide_tile * t + b)) for b in range(wide_tile)] for t in range(tiles)
+    ]
     if late:
         groups.append([(ext_ref, None, (plane - 2) * PLANE + spot)])
     row_lane = lax.broadcasted_iota(jnp.int32, (1, 128), 1)
@@ -164,22 +178,23 @@
 
     def heads(count, masked):
         panels = count // 128
+        turns = 3 if masked and not late else LOCAL_HEADS
 
         def side(number, carried):
-            first = number * LOCAL_HEADS
+            first = number * turns
 
             def score(head):
                 return lax.dot_general(
                     q_ref[first + head],
-                    k_s[2 * number + head // 3, :count, :],
+                    k_s[turns // 3 * number + head // 3, :count, :],
                     (((1,), (1,)), ((), ())),
                     preferred_element_type=f32,
                 )
 
             following = score(0)
-            for head in range(LOCAL_HEADS):
+            for head in range(turns):
                 s = following
-                if head + 1 < LOCAL_HEADS:
+                if head + 1 < turns:
                     following = score(head + 1)
                 at = first + head
                 parts = [s[:, 128 * b : 128 * b + 128] for b in range(panels)]
@@ -197,7 +212,7 @@
                 a_s[at] = a_s[at] * keep + jnp.dot(rounded, v_s[at, :count, :], preferred_element_type=f32)
             return carried
 
-        lax.fori_loop(0, 2, side, 0)
+        lax.fori_loop(0, HEADS // turns, side, 0)
 
     def tile(load, blocks, flags):
         panels = len(blocks)
@@ -255,11 +270,11 @@
         tile(lambda b, lo, hi: ext_ref[lo:hi, :], [groups[2][0][2]], code >> 4)
 
     def step(number, carried):
-        blocks = [block_of(number * 8 + b) for b in range(8)]
-        tile(lambda b, lo, hi: arr_ref[number * 8 + b, lo:hi, :], blocks, code >> (2 * number))
+        blocks = [block_of(number * wide_tile + b) for b in range(wide_tile)]
+        tile(lambda b, lo, hi: arr_ref[number * wide_tile + b, lo:hi, :], blocks, code >> (2 * number))
         return carried
 
-    lax.fori_loop(0, 2, step, 0)
+    lax.fori_loop(0, tiles, step, 0)
 
     stats = jnp.zeros((BLOCK, 128), f32)
     for head in range(HEADS):
@@ -394,16 +409,21 @@
     frequency = 10000.0 ** (-jnp.arange(16, dtype=f32) / 16)
     positions = seat * BLOCK + jnp.arange(BLOCK, dtype=jnp.int32)
     angles = positions.astype(f32)[None, :] * frequency[:, None]
-    inputs = (queries.T, latent, rope_key.T, doc_ids.reshape(2, 128), latent_to_key, latent_to_value, jnp.cos(angles), jnp.sin(angles))
-    payload, pack = pl.pallas_call(
-        prep_kernel,
-        out_shape=(jax.ShapeDtypeStruct((ROWS, 128), bf16), jax.ShapeDtypeStruct((BLOCK, PACK), bf16)),
-        in_specs=[hbm()] * 8,
-        out_specs=(vmem(), vmem()),
-        scratch_shapes=[pltpu.VMEM(x.shape, x.dtype) for x in inputs] + [pltpu.SemaphoreType.DMA((8,))],
-        compiler_params=params(8),
-        name="prep",
-    )(*map(far, inputs))
+    waves = (jnp.cos(angles), jnp.sin(angles))
+
+    def first(kernel, shape, *inputs):
+        inputs = inputs + waves
+        return pl.pallas_call(
+            kernel,
+            out_shape=jax.ShapeDtypeStruct(shape, bf16),
+            in_specs=[hbm()] * 5,
+            out_specs=vmem(),
+            scratch_shapes=[pltpu.VMEM(x.shape, x.dtype) for x in inputs] + [pltpu.SemaphoreType.DMA((5,))],
+            compiler_params=params(8),
+        )(*map(far, inputs))
+
+    payload = first(prep_kernel, (ROWS, 128), latent, rope_key.T, doc_ids.reshape(2, 128))
+    pack = first(pack_kernel, (BLOCK, PACK), queries.T, latent_to_key, latent_to_value)
     before = []
     for k in (1, 2):
         before.append(lax.ppermute(payload, "sp", [(i, i + PLANE * k) for i in range(sp - PLANE * k)]))
@@ -431,22 +451,23 @@
     stat = jax.ShapeDtypeStruct((HALF, 896), f32)
 
     def attend(is_late, *operands):
+        keys = 1024 if is_late else 2048
         mine, theirs = pl.pallas_call(
             functools.partial(attend_kernel, is_late),
             out_shape=(pltpu.HBM((HALF, 896), f32),) * 2 if is_late else (stat, stat),
             in_specs=[vmem()] * (len(operands) - 1) + [hbm()] + [vmem()] * 4 + [smem()],
             out_specs=(vmem(), vmem()),
             scratch_shapes=[
-                pltpu.VMEM((4, 1024, 256), bf16),
-                pltpu.VMEM((HEADS, 1024, 128), bf16),
+                pltpu.VMEM((4, keys, 256), bf16),
+                pltpu.VMEM((HEADS, keys, 128), bf16),
                 pltpu.VMEM((HEADS, BLOCK, 128), f32),
                 pltpu.VMEM((HEADS, BLOCK, 128), f32),
-                pltpu.VMEM((BLOCK, 1024), f32),
+                pltpu.VMEM((BLOCK, keys), f32),
                 pltpu.VMEM((BLOCK, 896), f32),
                 pltpu.VMEM((PLANE, ROWS, 128), bf16),
                 pltpu.SemaphoreType.DMA(()),
             ],
-            compiler_params=params(ATTEND_MIB),
+            compiler_params=params(ATTEND_MIB if is_late else 44),
             name="attend_late" if is_late else "attend_early",
         )(*operands[:-1], far(operands[-1]), spread, pack, other, query_docs, doc_ids)
         return mine, lax.ppermute(theirs, "tp", swap)

time: 175 us -> 176 us (level)
  no operation moved by 1% of the time
where the time goes in v5:
time: 176 us
  waiting for transfers between devices  55.2 us (31%)
  starting transfers between devices  49.3 us (28%)
  blocking collectives  35.3 us (20%)
  Pallas kernels  32.4 us (18%)
  other arithmetic  1.99 us (1%)
    all_to_all x1, blocking collectives, local(): back = lax.all_to_all(result, 'sp', 0, 0, tiled=True).reshape(SLOTS, D)  35.3 us
    all_to_all x1, waiting for transfers between devices, local(): lax.all_to_all(buffer.reshape(EXPERTS, CAPACITY, D), 'sp', 0, 0, tiled=True)  30.3 us
    all_to_all x1, starting transfers between devices, local(): lax.all_to_all(buffer.reshape(EXPERTS, CAPACITY, D), 'sp', 0, 0, tiled=True)  27.5 us
    all_to_all x2, waiting for transfers between devices, plane(): return lax.all_to_all(x, 'sp', 0, 0, axis_index_groups=groups, tiled=True)  17.8 us
    pallas_call x2, Pallas kernels, attend(): pl.pallas_call(functools.partial(attend_kernel, is_late), out_shape=(pltp...  12.6 us
    all_to_all x2, starting transfers between devices, plane(): return lax.all_to_all(x, 'sp', 0, 0, axis_index_groups=groups, tiled=True)  11.6 us
    pallas_call x1, Pallas kernels, local(): pl.pallas_call(expert_kernel, out_shape=jax.ShapeDtypeStruct((SLOTS, D),...  9.33 us
    ppermute x2, starting transfers between devices, local(): lax.ppermute(payload, 'sp', [(i, i + PLANE * k) for i in range(sp - PLANE...  8.83 us
  transfers between devices with their start and end apart: 11, of which 7 were waited for; matrix products, arithmetic and copies ran while one was open for 0% of the time, Pallas kernels for 11%

profile of v5, /device:TPU:0, one launch (start us, length us, event | category | flops | bytes accessed | tf_op | source)
XLA Modules:
  0.0 175.9 jit_solution(2797784652218910172)
XLA Ops:
  0.0 0.8 multiply_sine_fusion
  0.8 1.1 shard_map.145
  1.9 5.9 %collective-permute-start = (bf16[304,128]{1,0:T(8,128)(2,1)S(1)}, bf16[304,128]{1,0:T(8,128)(2,1)S(1)}, u32[]{:S(2)}, u32[]{:S(2)}) collective-permute-start(bf16[304,128]{1,0:T(8,128)(2,1)S(1)} %shard_map.145), channel_id=1, source_target_pairs={{0,64},{2,66},{4,68},{6,70},{8,72},{10,74},{12,76},{14,78},{16,80}... | collective-permute-start | bytes 233480 | tf_op jit(solution)/shard_map/ppermute | solution.py:429
  7.8 2.0 %collective-permute-done.refs_0_ = bf16[304,128]{1,0:T(8,128)(2,1)S(1)} collective-permute-done((bf16[304,128]{1,0:T(8,128)(2,1)S(1)}, bf16[304,128]{1,0:T(8,128)(2,1)S(1)}, u32[]{:S(2)}, u32[]{:S(2)}) %collective-permute-start) | collective-permute-done | bytes 77856 | tf_op jit(solution)/shard_map/ppermute | solution.py:429
  9.8 1.2 broadcast_select_fusion
  11.0 7.0 %all-to-all-start = ((bf16[16,304,128]{2,1,0:T(8,128)(2,1)}), bf16[16,304,128]{2,1,0:T(8,128)(2,1)S(1)}, u32[]{:S(2)}, u32[]{:S(2)}) async-start(bf16[16,304,128]{2,1,0:T(8,128)(2,1)} %broadcast_select_fusion), calls=%async_computation | async-start | bytes 2490368 | tf_op jit(solution)/shard_map/all_to_all | solution.py:437
  18.1 2.9 %collective-permute-start.3 = (bf16[304,128]{1,0:T(8,128)(2,1)S(1)}, bf16[304,128]{1,0:T(8,128)(2,1)S(1)}, u32[]{:S(2)}, u32[]{:S(2)}) collective-permute-start(bf16[304,128]{1,0:T(8,128)(2,1)S(1)} %shard_map.145), channel_id=1, source_target_pairs={{0,32},{2,34},{4,36},{6,38},{8,40},{10,42},{12,44},{14,46},{16,48}... | collective-permute-start | bytes 233480 | tf_op jit(solution)/shard_map/ppermute | solution.py:429
  21.0 2.0 %collective-permute-done.3 = bf16[304,128]{1,0:T(8,128)(2,1)S(1)} collective-permute-done((bf16[304,128]{1,0:T(8,128)(2,1)S(1)}, bf16[304,128]{1,0:T(8,128)(2,1)S(1)}, u32[]{:S(2)}, u32[]{:S(2)}) %collective-permute-start.3) | collective-permute-done | bytes 77856 | tf_op jit(solution)/shard_map/ppermute | solution.py:429
  23.0 14.0 %all-to-all-done.refs_1_ = bf16[16,304,128]{2,1,0:T(8,128)(2,1)S(1)} async-done(((bf16[16,304,128]{2,1,0:T(8,128)(2,1)}), bf16[16,304,128]{2,1,0:T(8,128)(2,1)S(1)}, u32[]{:S(2)}, u32[]{:S(2)}) %all-to-all-start) | async-done | bytes 1245216 | tf_op jit(solution)/shard_map/all_to_all | solution.py:437
  37.0 0.0 copy-start.8
  37.0 1.3 broadcast_in_dim.51
  38.3 0.0 copy-start.3
  38.4 4.5 %all-to-all-start.1 = ((bf16[16,304,128]{2,1,0:T(8,128)(2,1)}), bf16[16,304,128]{2,1,0:T(8,128)(2,1)}, u32[]{:S(2)}, u32[]{:S(2)}) async-start(bf16[16,304,128]{2,1,0:T(8,128)(2,1)} %broadcast_in_dim.51), calls=%async_computation.1 | async-start | bytes 2490368 | tf_op jit(solution)/shard_map/all_to_all | solution.py:437
  42.9 1.4 shard_map.146.own_ref.refs_3_.refs_2_
  44.3 0.0 copy-done.8
  44.3 0.1 collective-permute-start.1
  44.4 0.0 copy-done.3
  44.4 2.3 %collective-permute-done.1.oth_ref.refs_4_.refs_3_ = bf16[256,1664]{1,0:T(8,128)(2,1)S(1)} collective-permute-done((bf16[256,1664]{1,0:T(8,128)(2,1)S(1)}, bf16[256,1664]{1,0:T(8,128)(2,1)S(1)}, u32[]{:S(2)}, u32[]{:S(2)}) %collective-permute-start.1) | collective-permute-done | bytes 852000 | tf_op jit(solution)/shard_map/ppermute | solution.py:430
  46.8 0.3 spread.1.refs_2_.refs_1_
  47.1 0.1 broadcast_in_dim.50.refs_5_.refs_4_
  47.2 9.4 %attend_late.1 = (f32[128,896]{1,0:T(8,128)}, f32[128,896]{1,0:T(8,128)}) custom-call(bf16[304,128]{1,0:T(8,128)(2,1)S(1)} %collective-permute-done.refs_0_, bf16[16,304,128]{2,1,0:T(8,128)(2,1)} %copy-done.8, bf16[12,256,256]{2,1,0:T(8,128)(2,1)S(1)} %spread.1.refs_2_.refs_1_, bf16[256,1664]{1,0:T(8,128)(2,1)S(1)} %shard_map.146.own_ref.refs_3_.refs_2_, ...), custom_call_target="tpu_custom_call" | custom-call | tf_op jit(solution)/shard_map/attend_late/pallas_call | solution.py:455
  56.6 0.0 copy-start.4
  56.6 0.0 copy-start.5
  56.6 0.0 copy-start.6
  56.6 0.2 collective-permute-start.2
  56.9 3.8 %all-to-all-done.1.refs_0_ = bf16[16,304,128]{2,1,0:T(8,128)(2,1)} async-done(((bf16[16,304,128]{2,1,0:T(8,128)(2,1)}), bf16[16,304,128]{2,1,0:T(8,128)(2,1)}, u32[]{:S(2)}, u32[]{:S(2)}) %all-to-all-start.1) | async-done | bytes 1245216 | tf_op jit(solution)/shard_map/all_to_all | solution.py:437
  60.6 0.0 copy-start
  60.6 0.0 copy-start.1
  60.6 0.0 copy-start.2
  60.6 3.2 %attend_early.1 = (f32[128,896]{1,0:T(8,128)S(1)}, f32[128,896]{1,0:T(8,128)S(1)}) custom-call(bf16[16,304,128]{2,1,0:T(8,128)(2,1)} %all-to-all-done.1.refs_0_, bf16[12,256,256]{2,1,0:T(8,128)(2,1)S(1)} %spread.1.refs_2_.refs_1_, bf16[256,1664]{1,0:T(8,128)(2,1)S(1)} %shard_map.146.own_ref.refs_3_.refs_2_, ...), custom_call_target="tpu_custom_call" | custom-call | tf_op jit(solution)/shard_map/attend_early/pallas_call | solution.py:455
  63.8 0.1 collective-permute-start.4
  63.9 0.5 collective-permute-start.5
  64.4 0.1 collective-permute-start.6
  64.5 0.4 collective-permute-start.7
  64.9 0.0 collective-permute-done.2.refs_1_
  64.9 0.8 collective-permute-done.4.refs_3_
  65.7 0.0 copy-done.4
  65.7 0.0 copy-done.5
  65.7 0.0 copy-done.6
  65.7 0.0 copy-done
  65.8 0.0 copy-done.1
  65.8 0.0 copy-done.2
  65.8 5.9 %mix.1 = (bf16[128,2048]{1,0:T(8,128)(2,1)S(1)}, bf16[512,2048]{1,0:T(8,128)(2,1)}) custom-call(f32[128,896]{1,0:T(8,128)S(1)} %copy-done.2, f32[128,896]{1,0:T(8,128)} %collective-permute-done.2.refs_1_, f32[128,896]{1,0:T(8,128)S(1)} %get-tuple-element.13.refs_2_, f32[128,896]{1,0:T(8,128)S(1)} %collective-permute-done.4.refs_3_, ...), custom_call_target="tpu_custom_call" | custom-call | tf_op jit(solution)/shard_map/mix/pallas_call | solution.py:476
  71.7 27.5 %all-to-all-start.2 = ((bf16[64,8,2048]{2,1,0:T(8,128)(2,1)}), bf16[64,8,2048]{2,1,0:T(8,128)(2,1)S(1)}, u32[]{:S(2)}, u32[]{:S(2)}) async-start(bf16[64,8,2048]{2,1,0:T(8,128)(2,1)} %bitcast.23), calls=%async_computation.2 | async-start | bytes 4194304 | tf_op jit(solution)/shard_map/all_to_all | solution.py:485
  99.1 0.0 collective-permute-done.5.refs_3_
  99.2 0.0 collective-permute-done.6.refs_4_
  99.2 0.0 collective-permute-done.7.refs_5_
  99.2 30.3 %all-to-all-done.2 = bf16[64,8,2048]{2,1,0:T(8,128)(2,1)S(1)} async-done(((bf16[64,8,2048]{2,1,0:T(8,128)(2,1)}), bf16[64,8,2048]{2,1,0:T(8,128)(2,1)S(1)}, u32[]{:S(2)}, u32[]{:S(2)}) %all-to-all-start.2) | async-done | bytes 2097184 | tf_op jit(solution)/shard_map/all_to_all | solution.py:485
  129.5 9.3 %experts.1 = bf16[512,2048]{1,0:T(8,128)(2,1)S(1)} custom-call(bf16[512,2048]{1,0:T(8,128)(2,1)S(1)} %bitcast.15, bf16[2048,512]{1,0:T(8,128)(2,1)} %bitcast.25, bf16[2048,512]{1,0:T(8,128)(2,1)} %bitcast.27, bf16[512,2048]{1,0:T(8,128)(2,1)} %bitcast.29, bf16[2048,512]{1,0:T(8,128)(2,1)} %collective-permute-done.5.refs_3_, ...), custom_call_target="tpu_custom_call" | custom-call | tf_op jit(solution)/shard_map/experts/pallas_call | solution.py:486
  138.9 0.0 copy-start.7
  138.9 35.3 %all_to_all.20 = bf16[64,8,2048]{2,1,0:T(8,128)(2,1)S(1)} all-to-all(bf16[64,8,2048]{2,1,0:T(8,128)(2,1)S(1)} %bitcast.16), channel_id=1, replica_groups=mesh['sp'=64,'tp'=2] {'sp'}, dimensions={0} | all-to-all | bytes 4194304 | tf_op jit(solution)/shard_map/all_to_all | solution.py:496
  174.2 0.0 copy-done.7
  174.2 1.7 pick.1
  (4 shorter events, 0.0 us)
Async XLA Ops:
  1.9 7.9 %collective-permute-start = (bf16[304,128]{1,0:T(8,128)(2,1)S(1)}, bf16[304,128]{1,0:T(8,128)(2,1)S(1)}, u32[]{:S(2)}, u32[]{:S(2)}) collective-permute-start(bf16[304,128]{1,0:T(8,128)(2,1)S(1)} %shard_map.145), channel_id=1, source_target_pairs={{0,64},{2,66},{4,68},{6,70},{8,72},{10,74},{12,76},{14,78},{16,80}... | collective-permute-start | bytes 233480 | tf_op jit(solution)/shard_map/ppermute | solution.py:429
  11.0 26.0 %all-to-all-start = ((bf16[16,304,128]{2,1,0:T(8,128)(2,1)}), bf16[16,304,128]{2,1,0:T(8,128)(2,1)S(1)}, u32[]{:S(2)}, u32[]{:S(2)}) async-start(bf16[16,304,128]{2,1,0:T(8,128)(2,1)} %broadcast_select_fusion), calls=%async_computation | async-start | bytes 2490368 | tf_op jit(solution)/shard_map/all_to_all | solution.py:437
  18.1 4.9 %collective-permute-start.3 = (bf16[304,128]{1,0:T(8,128)(2,1)S(1)}, bf16[304,128]{1,0:T(8,128)(2,1)S(1)}, u32[]{:S(2)}, u32[]{:S(2)}) collective-permute-start(bf16[304,128]{1,0:T(8,128)(2,1)S(1)} %shard_map.145), channel_id=1, source_target_pairs={{0,32},{2,34},{4,36},{6,38},{8,40},{10,42},{12,44},{14,46},{16,48}... | collective-permute-start | bytes 233480 | tf_op jit(solution)/shard_map/ppermute | solution.py:429
  37.0 7.3 %copy-start.8 = (bf16[16,304,128]{2,1,0:T(8,128)(2,1)}, bf16[16,304,128]{2,1,0:T(8,128)(2,1)S(1)}, u32[]{:S(2)}) copy-start(bf16[16,304,128]{2,1,0:T(8,128)(2,1)S(1)} %all-to-all-done.refs_1_) | copy-start | bytes 3735556
  38.3 6.1 %copy-start.3 = (s32[256]{0:T(256)S(1)}, s32[256]{0:T(256)}, u32[]{:S(2)}) copy-start(s32[256]{0:T(256)} %refs_5_.2) | copy-start | bytes 3076
  38.4 22.3 %all-to-all-start.1 = ((bf16[16,304,128]{2,1,0:T(8,128)(2,1)}), bf16[16,304,128]{2,1,0:T(8,128)(2,1)}, u32[]{:S(2)}, u32[]{:S(2)}) async-start(bf16[16,304,128]{2,1,0:T(8,128)(2,1)} %broadcast_in_dim.51), calls=%async_computation.1 | async-start | bytes 2490368 | tf_op jit(solution)/shard_map/all_to_all | solution.py:437
  44.3 2.5 %collective-permute-start.1 = (bf16[256,1664]{1,0:T(8,128)(2,1)S(1)}, bf16[256,1664]{1,0:T(8,128)(2,1)S(1)}, u32[]{:S(2)}, u32[]{:S(2)}) collective-permute-start(bf16[256,1664]{1,0:T(8,128)(2,1)S(1)} %shard_map.146.own_ref.refs_3_.refs_2_), channel_id=1, source_target_pairs={{0,1},{1,0},{2,3},{3,2},{4,5},{5,4},{6,7},{7,6},{8,9},{9,8},{10,11... | collective-permute-start | bytes 2555912 | tf_op jit(solution)/shard_map/ppermute | solution.py:430
  56.6 9.1 %copy-start.4 = (f32[2048]{0:T(1024)S(1)}, f32[2048]{0:T(1024)}, u32[]{:S(2)}) copy-start(f32[2048]{0:T(1024)} %param.23) | copy-start | bytes 24580
  56.6 9.1 %copy-start.5 = (f32[2048]{0:T(1024)S(1)}, f32[2048]{0:T(1024)}, u32[]{:S(2)}) copy-start(f32[2048]{0:T(1024)} %param.24) | copy-start | bytes 24580
  56.6 9.1 %copy-start.6 = (s32[128,2]{0,1:T(2,128)S(1)}, s32[128,2]{0,1:T(2,128)}, u32[]{:S(2)}) copy-start(s32[128,2]{0,1:T(2,128)} %param.25) | copy-start | bytes 3076
  56.6 8.3 %collective-permute-start.2 = (f32[128,896]{1,0:T(8,128)}, f32[128,896]{1,0:T(8,128)}, u32[]{:S(2)}, u32[]{:S(2)}) collective-permute-start(f32[128,896]{1,0:T(8,128)} %get-tuple-element.12), channel_id=1, source_target_pairs={{0,1},{1,0},{2,3},{3,2},{4,5},{5,4},{6,7},{7,6},{8,9},{9,8},{10,11... | collective-permute-start | bytes 1376264 | tf_op jit(solution)/shard_map/ppermute | solution.py:473
  60.6 5.1 %copy-start = (bf16[768,2048]{1,0:T(8,128)(2,1)S(1)}, bf16[768,2048]{1,0:T(8,128)(2,1)}, u32[]{:S(2)}) copy-start(bf16[768,2048]{1,0:T(8,128)(2,1)} %refs_4_.1) | copy-start | bytes 9437188
  60.6 5.1 %copy-start.1 = (bf16[128,2048]{1,0:T(8,128)(2,1)S(1)}, bf16[128,2048]{1,0:T(8,128)(2,1)}, u32[]{:S(2)}) copy-start(bf16[128,2048]{1,0:T(8,128)(2,1)} %refs_5_.3) | copy-start | bytes 1572868
  60.6 5.1 %copy-start.2 = (f32[128,896]{1,0:T(8,128)S(1)}, f32[128,896]{1,0:T(8,128)}, u32[]{:S(2)}) copy-start(f32[128,896]{1,0:T(8,128)} %get-tuple-element.11.refs_0_) | copy-start | bytes 1376260
  63.8 1.9 %collective-permute-start.4 = (f32[128,896]{1,0:T(8,128)S(1)}, f32[128,896]{1,0:T(8,128)S(1)}, u32[]{:S(2)}, u32[]{:S(2)}) collective-permute-start(f32[128,896]{1,0:T(8,128)S(1)} %get-tuple-element.14), channel_id=1, source_target_pairs={{0,1},{1,0},{2,3},{3,2},{4,5},{5,4},{6,7},{7,6},{8,9},{9,8},{10,11... | collective-permute-start | bytes 1376264 | tf_op jit(solution)/shard_map/ppermute | solution.py:473
  63.9 35.2 %collective-permute-start.5 = (bf16[2048,512]{1,0:T(8,128)(2,1)}, bf16[2048,512]{1,0:T(8,128)(2,1)}, u32[]{:S(2)}, u32[]{:S(2)}) collective-permute-start(bf16[2048,512]{1,0:T(8,128)(2,1)} %bitcast.24), channel_id=1, source_target_pairs={{0,1},{1,0},{2,3},{3,2},{4,5},{5,4},{6,7},{7,6},{8,9},{9,8},{10,11... | collective-permute-start | bytes 6291464 | tf_op jit(solution)/shard_map/ppermute | solution.py:432
  64.4 34.7 %collective-permute-start.6 = (bf16[2048,512]{1,0:T(8,128)(2,1)}, bf16[2048,512]{1,0:T(8,128)(2,1)}, u32[]{:S(2)}, u32[]{:S(2)}) collective-permute-start(bf16[2048,512]{1,0:T(8,128)(2,1)} %bitcast.26), channel_id=1, source_target_pairs={{0,1},{1,0},{2,3},{3,2},{4,5},{5,4},{6,7},{7,6},{8,9},{9,8},{10,11... | collective-permute-start | bytes 6291464 | tf_op jit(solution)/shard_map/ppermute | solution.py:432
  64.5 34.6 %collective-permute-start.7 = (bf16[512,2048]{1,0:T(8,128)(2,1)}, bf16[512,2048]{1,0:T(8,128)(2,1)}, u32[]{:S(2)}, u32[]{:S(2)}) collective-permute-start(bf16[512,2048]{1,0:T(8,128)(2,1)} %bitcast.28), channel_id=1, source_target_pairs={{0,1},{1,0},{2,3},{3,2},{4,5},{5,4},{6,7},{7,6},{8,9},{9,8},{10,11... | collective-permute-start | bytes 6291464 | tf_op jit(solution)/shard_map/ppermute | solution.py:432
  71.7 57.9 %all-to-all-start.2 = ((bf16[64,8,2048]{2,1,0:T(8,128)(2,1)}), bf16[64,8,2048]{2,1,0:T(8,128)(2,1)S(1)}, u32[]{:S(2)}, u32[]{:S(2)}) async-start(bf16[64,8,2048]{2,1,0:T(8,128)(2,1)} %bitcast.23), calls=%async_computation.2 | async-start | bytes 4194304 | tf_op jit(solution)/shard_map/all_to_all | solution.py:485
  138.9 35.4 %copy-start.7 = (f32[128,2]{0,1:T(2,128)S(1)}, f32[128,2]{0,1:T(2,128)}, u32[]{:S(2)}) copy-start(f32[128,2]{0,1:T(2,128)} %param.26) | copy-start | bytes 3076
